TPU v7x, 32 devices: a whole 2x2x4 slice. The times are simulated.
32 devices in a mesh: sp: 8 (over z, y), tp: 4 (over x, core).
Axes of the slice: x: 2, y: 2, z: 4, core: 2. Of those that a mesh axis runs over, the one named last changes fastest.
Arguments:
- tokens: bfloat16 [8192, 2048], P('sp'), may hold values from -6 to 6
- norm_gain: bfloat16 [2048], replicated, may hold values from 0.099609375 to 1.8984375
- query_weight: bfloat16 [2048, 2048], P(None, 'tp'), may hold values from -0.125 to 0.125
- key_weight: bfloat16 [2048, 512], P(None, 'tp'), may hold values from -0.125 to 0.125
- value_weight: bfloat16 [2048, 512], P(None, 'tp'), may hold values from -0.125 to 0.125
- query_gain: float32 [64], replicated, may hold values from 1 to 14
- key_gain: float32 [64], replicated, may hold values from 1 to 14
- sink_logit: float32 [32], P('tp'), may hold values from 4 to 10
- gate_weight: bfloat16 [2048, 4096], P(None, 'tp'), may hold values from -0.125 to 0.125
- inner_weight: bfloat16 [2048, 4096], P(None, 'tp'), may hold values from -0.125 to 0.125
- input_map: bfloat16 [2048, 1024], P(None, 'tp'), may hold values from -0.125 to 0.125
- output_map: bfloat16 [2048, 1024], P(None, 'tp'), may hold values from -0.125 to 0.125
- step_weight: bfloat16 [2048, 2, 64], P(None, None, 'tp'), may hold values from -0.125 to 0.125
- conv_inner: bfloat16 [5, 4096], P(None, 'tp'), may hold values from -2.5 to 2.5
- conv_pair: bfloat16 [5, 2, 1024], P(None, None, 'tp'), may hold values from -2.5 to 2.5
- decay_rate: float32 [2, 64], P(None, 'tp'), may hold values from 3.6621094e-06 to 0.05
- decay_jump: float32 [8192, 2, 64], P('sp', None, 'tp'), may hold values from -1.4001709 to 0
- inner_gain: bfloat16 [4096], P('tp'), may hold values from 0.099609375 to 1.8984375
- attn_out_weight: bfloat16 [2048, 2048], P('tp'), may hold values from -0.25 to 0.25
- ssm_out_weight: bfloat16 [4096, 2048], P('tp'), may hold values from -0.09375 to 0.09375
Outputs:
- mixed: bfloat16 [8192, 2048], P(('sp', 'tp'))
All inputs are finite; a program needn't handle non-finite values.
Results may differ from a plain program's by a relative error of at most 0.025.
The roundings to bfloat16 on the way count: a program that leaves them out, or rounds other values in their place, can miss the bound.
Values may be sent and summed in bfloat16 or wider, within the bound.
A program may use at most 128 MiB of HBM per device.

v0:
```python
import functools

import jax
import jax.numpy as jnp
from jax import lax
from jax.experimental import pallas as pl
from jax.experimental.pallas import tpu as pltpu
from jax.sharding import PartitionSpec as P

STATE_SIZE = 128
WINDOW = 128
CHUNK = 128
HALO = 16

NORM_EPS = 1e-05
ROPE_BASE = 500000.0
NEG_FILL = -1e30


def extended(block, sides, width):
    for axis, dim in sides:
        count = lax.axis_size(axis)
        forward = [(i, i + 1) for i in range(count - 1)]
        backward = [(target, source) for source, target in forward]
        low = lax.ppermute(
            lax.slice_in_dim(block, block.shape[dim] - width, None, axis=dim), axis, forward
        )
        high = lax.ppermute(lax.slice_in_dim(block, 0, width, axis=dim), axis, backward)
        block = jnp.concatenate([low, block, high], axis=dim)
    return block


def rms_rows(values, scales):
    return values * lax.rsqrt(jnp.mean(values * values, axis=-1, keepdims=True) + NORM_EPS) * scales


def rotate(head_rows, positions):
    head_size = head_rows.shape[-1]
    half_size = head_size // 2
    frequency = ROPE_BASE ** (-jnp.arange(0, head_size, 2, dtype=jnp.float32) / head_size)
    angles = positions.astype(jnp.float32)[:, None] * frequency
    cosine = jnp.cos(angles)[:, None, :]
    sine_part = jnp.sin(angles)[:, None, :]
    first_half = head_rows[..., :half_size]
    second_half = head_rows[..., half_size:]
    return jnp.concatenate(
        [
            first_half * cosine - second_half * sine_part,
            second_half * cosine + first_half * sine_part,
        ],
        axis=-1,
    )


def spread(factor, width):
    heads = factor.shape[1]
    row = lax.broadcasted_iota(jnp.int32, (heads, width), 0)
    column = lax.broadcasted_iota(jnp.int32, (heads, width), 1)
    head_size = width // heads
    ones = jnp.where(
        (column >= row * head_size) & (column < (row + 1) * head_size), 1.0, 0.0
    ).astype(jnp.bfloat16)
    return jnp.dot(factor.astype(jnp.bfloat16), ones, preferred_element_type=jnp.float32)


def exact_dot(a, b):
    return jnp.dot(a, b, precision=lax.Precision.HIGHEST, preferred_element_type=jnp.float32)


def triangle(size, lower):
    row = lax.broadcasted_iota(jnp.int32, (size, size), 0)
    column = lax.broadcasted_iota(jnp.int32, (size, size), 1)
    return jnp.where(row >= column if lower else row <= column, 1.0, 0.0)


def states_kernel(
    tap_count, inner, maps, rows_ref, taps_ref, ldf_ref, ldb_ref, stf_ref, stb_ref,
    act_ref, freshf_ref, freshb_ref, endf_ref, endb_ref, spare, reach,
):
    step = pl.program_id(0)
    size = act_ref.shape[0]
    start = pl.multiple_of(step * size, size)
    spare[...] = rows_ref[pl.ds(start, size + 2 * HALO), :].astype(jnp.float32)
    first = HALO - tap_count // 2
    filtered = spare[first : first + size, :] * taps_ref[0:1, :]
    for k in range(1, tap_count):
        filtered = filtered + spare[first + k : first + k + size, :] * taps_ref[k : k + 1, :]
    activated = filtered / (1.0 + jnp.exp(-filtered))
    act_ref[...] = activated.astype(jnp.bfloat16)
    signal = activated[:, :inner]
    ldf, ldb = ldf_ref[...], ldb_ref[...]
    cumf = exact_dot(triangle(size, True), ldf)
    cumb = exact_dot(triangle(size, False), ldb)
    wf = jnp.exp(cumf[size - 1 : size] - cumf) * stf_ref[...]
    wb = jnp.exp(cumb[0:1] - cumb) * stb_ref[...]
    xf = (signal * spread(wf, inner)).astype(jnp.bfloat16)
    xb = (signal * spread(wb, inner)).astype(jnp.bfloat16)
    totf = spread(jnp.exp(jnp.broadcast_to(cumf[size - 1 : size], (8, ldf.shape[1]))), inner)[0:1]
    totb = spread(jnp.exp(jnp.broadcast_to(cumb[0:1], (8, ldb.shape[1]))), inner)[0:1]

    @pl.when(step == 0)
    def _():
        endf_ref[...] = jnp.zeros_like(endf_ref)
        endb_ref[...] = jnp.zeros_like(endb_ref)
        reach[...] = jnp.ones_like(reach)

    groups = maps // STATE_SIZE
    width = inner // groups
    for g in range(groups):
        entry = activated[:, inner + g * STATE_SIZE : inner + (g + 1) * STATE_SIZE]
        entry = jnp.transpose(entry).astype(jnp.bfloat16)
        cols = slice(g * width, (g + 1) * width)
        ff = jnp.dot(entry, xf[:, cols], preferred_element_type=jnp.float32)
        fb = jnp.dot(entry, xb[:, cols], preferred_element_type=jnp.float32)
        freshf_ref[0, :, cols] = ff
        freshb_ref[0, :, cols] = fb
        endf_ref[:, cols] = endf_ref[:, cols] * totf[:, cols] + ff
        endb_ref[:, cols] = endb_ref[:, cols] + reach[0:1, cols] * fb
    reach[...] = reach[...] * totb


def outputs_kernel(
    head_size, inner, maps, act_ref, ldf_ref, ldb_ref, stf_ref, stb_ref, ldft_ref, ldbt_ref,
    stft_ref, stbt_ref, ldball_ref, freshf_ref, freshb_ref, inf_ref, inb_ref, gate_ref, gain_ref,
    out_ref, carryf, enterb, y,
):
    step = pl.program_id(0)
    chunks = pl.num_programs(0)
    size = act_ref.shape[0]
    heads = inner // head_size

    @pl.when(step == 0)
    def _():
        carryf[...] = inf_ref[...]
        enterb[chunks - 1] = inb_ref[...]

        @pl.loop(0, chunks - 1)
        def _(k):
            at = chunks - 1 - k
            part = ldball_ref[pl.ds(pl.multiple_of(at * size, size), size), :]
            tot = jnp.exp(jnp.sum(part, axis=0, keepdims=True))
            tot = spread(jnp.broadcast_to(tot, (8, heads)), inner)[0:1]
            enterb[at - 1] = enterb[at] * tot + freshb_ref[at]

    lower, upper = triangle(size, True), triangle(size, False)
    cumf = exact_dot(lower, ldf_ref[...])
    cumb = exact_dot(upper, ldb_ref[...])
    cumft = exact_dot(ldft_ref[...], upper)
    cumbt = exact_dot(ldbt_ref[...], lower)
    stft, stbt = stft_ref[...], stbt_ref[...]
    row = lax.broadcasted_iota(jnp.int32, (size, size), 0)
    column = lax.broadcasted_iota(jnp.int32, (size, size), 1)
    is_lower, is_diagonal = row >= column, row == column
    groups = maps // STATE_SIZE
    width = inner // groups
    group_heads = heads // groups
    expf = spread(jnp.exp(cumf), inner)
    expb = spread(jnp.exp(cumb), inner)
    lane = lax.broadcasted_iota(jnp.int32, (size, 2 * head_size), 1)
    for g in range(groups):
        cols = slice(g * width, (g + 1) * width)
        entry = act_ref[:, inner + g * STATE_SIZE : inner + (g + 1) * STATE_SIZE]
        leave = act_ref[:, inner + maps + g * STATE_SIZE : inner + maps + (g + 1) * STATE_SIZE]
        crossed = lax.dot_general(
            leave, entry, (((1,), (1,)), ((), ())), preferred_element_type=jnp.float32
        )
        y[:, cols] = (
            jnp.dot(leave, carryf[:, cols].astype(jnp.bfloat16), preferred_element_type=jnp.float32)
            * expf[:, cols]
            + jnp.dot(
                leave, enterb[step, :, cols].astype(jnp.bfloat16),
                preferred_element_type=jnp.float32,
            )
            * expb[:, cols]
        )
        for pair in range(group_heads // 2):
            mats = []
            base = g * group_heads + 2 * pair
            for h in (base, base + 1):
                gap = jnp.where(
                    is_lower,
                    cumf[:, h : h + 1] - cumft[h : h + 1, :],
                    cumb[:, h : h + 1] - cumbt[h : h + 1, :],
                )
                sf, sb = stft[h : h + 1, :], stbt[h : h + 1, :]
                amount = jnp.where(is_diagonal, sf + sb, jnp.where(is_lower, sf, sb))
                mats.append((crossed * jnp.exp(gap) * amount).astype(jnp.bfloat16))
            two = slice(base * head_size, (base + 2) * head_size)
            x = act_ref[:, two]
            zero = jnp.zeros_like(x)
            stacked = jnp.concatenate(
                [jnp.where(lane < head_size, x, zero), jnp.where(lane < head_size, zero, x)], axis=0
            )
            y[:, two] += jnp.dot(
                jnp.concatenate(mats, axis=1), stacked, preferred_element_type=jnp.float32
            )
        gate = gate_ref[:, cols].astype(jnp.float32)
        mixed = y[:, cols] * (gate / (1.0 + jnp.exp(-gate)))
        scale = lax.rsqrt(jnp.mean(mixed * mixed, axis=1, keepdims=True) + NORM_EPS)
        out_ref[:, cols] = (mixed * scale * gain_ref[:, cols]).astype(jnp.bfloat16)
    totf = spread(jnp.exp(jnp.broadcast_to(cumf[size - 1 : size], (8, heads))), inner)[0:1]
    carryf[...] = carryf[...] * totf + freshf_ref[0]


def attend_kernel(head_size, key_heads, place_ref, sink_ref, query_ref, rim_ref, out_ref):
    step = pl.program_id(0)
    size = query_ref.shape[0]
    reach = size + 2 * WINDOW
    heads = query_ref.shape[1] // head_size
    ratio = heads // key_heads
    start = pl.multiple_of(step * size, size)
    row = lax.broadcasted_iota(jnp.int32, (size, reach), 0)
    column = lax.broadcasted_iota(jnp.int32, (size, reach), 1)
    key_pos = place_ref[0] + step * size - WINDOW + column
    allowed = (
        (column >= row) & (column <= row + 2 * WINDOW) & (key_pos >= 0) & (key_pos < place_ref[1])
    )
    scale = head_size ** (-0.5)
    for k in range(key_heads):
        keys = rim_ref[pl.ds(start, reach), k * head_size : (k + 1) * head_size]
        values = rim_ref[
            pl.ds(start, reach), (key_heads + k) * head_size : (key_heads + k + 1) * head_size
        ]
        for r in range(ratio):
            h = k * ratio + r
            cols = slice(h * head_size, (h + 1) * head_size)
            scores = lax.dot_general(
                query_ref[:, cols], keys, (((1,), (1,)), ((), ())),
                preferred_element_type=jnp.float32,
            )
            scores = jnp.where(allowed, scores * scale, NEG_FILL)
            sink = sink_ref[h]
            ceiling = jnp.maximum(jnp.max(scores, axis=1, keepdims=True), sink)
            raised = jnp.exp(scores - ceiling)
            bottom = jnp.sum(raised, axis=1, keepdims=True) + jnp.exp(sink - ceiling)
            weights = (raised * (1.0 / bottom)).astype(jnp.bfloat16)
            out_ref[:, cols] = jnp.dot(
                weights, values, preferred_element_type=jnp.float32
            ).astype(jnp.bfloat16)


def attend(query, rimmed, sink_logit, seq_first, seq_total, head_size, key_heads):
    rows, width = query.shape
    block = WINDOW
    place = jnp.stack([jnp.int32(seq_first), jnp.int32(seq_total)])
    return pl.pallas_call(
        functools.partial(attend_kernel, head_size, key_heads),
        grid=(rows // block,),
        in_specs=[
            pl.BlockSpec(memory_space=pltpu.SMEM),
            pl.BlockSpec(memory_space=pltpu.SMEM),
            pl.BlockSpec((block, width), lambda i: (i, 0)),
            pl.BlockSpec(rimmed.shape, lambda i: (0, 0)),
        ],
        out_specs=pl.BlockSpec((block, width), lambda i: (i, 0)),
        out_shape=jax.ShapeDtypeStruct((rows, width), jnp.bfloat16),
        cost_estimate=pl.CostEstimate(
            flops=4 * rows * 3 * WINDOW * width, bytes_accessed=4 * rows * width,
            transcendentals=rows * 3 * WINDOW * width // head_size,
        ),
        name="attend",
    )(place, sink_logit, query, rimmed)


def chunk_states(rimmed, taps, tap_count, inner, maps, decay, step):
    rows = rimmed.shape[0] - 2 * HALO
    total, heads, chunks = rimmed.shape[1], decay[0].shape[1], rows // CHUNK
    small = pl.BlockSpec((CHUNK, heads), lambda i: (i, 0))
    fresh = pl.BlockSpec((1, STATE_SIZE, inner), lambda i: (i, 0, 0))
    end = pl.BlockSpec((STATE_SIZE, inner), lambda i: (0, 0))
    fresh_shape = jax.ShapeDtypeStruct((chunks, STATE_SIZE, inner), jnp.float32)
    end_shape = jax.ShapeDtypeStruct((STATE_SIZE, inner), jnp.float32)
    return pl.pallas_call(
        functools.partial(states_kernel, tap_count, inner, maps),
        grid=(chunks,),
        in_specs=[
            pl.BlockSpec(rimmed.shape, lambda i: (0, 0)),
            pl.BlockSpec(taps.shape, lambda i: (0, 0)),
            small, small, small, small,
        ],
        out_specs=[pl.BlockSpec((CHUNK, total), lambda i: (i, 0)), fresh, fresh, end, end],
        out_shape=[
            jax.ShapeDtypeStruct((rows, total), jnp.bfloat16),
            fresh_shape, fresh_shape, end_shape, end_shape,
        ],
        scratch_shapes=[
            pltpu.VMEM((CHUNK + 2 * HALO, total), jnp.float32),
            pltpu.VMEM((8, inner), jnp.float32),
        ],
        cost_estimate=pl.CostEstimate(
            flops=8 * rows * inner * STATE_SIZE, bytes_accessed=16 * rows * inner,
            transcendentals=rows * total,
        ),
        name="chunk_states",
    )(rimmed, taps, *decay, *step)


def chunk_outputs(head_size, inner, maps, act, decay, step, fresh, incoming, gate, gain):
    rows, total = act.shape
    heads, chunks = decay[0].shape[1], rows // CHUNK
    small = pl.BlockSpec((CHUNK, heads), lambda i: (i, 0))
    turned = pl.BlockSpec((heads, CHUNK), lambda i: (0, i))
    whole = pl.BlockSpec((STATE_SIZE, inner), lambda i: (0, 0))
    return pl.pallas_call(
        functools.partial(outputs_kernel, head_size, inner, maps),
        grid=(chunks,),
        in_specs=[
            pl.BlockSpec((CHUNK, total), lambda i: (i, 0)),
            small, small, small, small, turned, turned, turned, turned,
            pl.BlockSpec((rows, heads), lambda i: (0, 0)),
            pl.BlockSpec((1, STATE_SIZE, inner), lambda i: (i, 0, 0)),
            pl.BlockSpec((chunks, STATE_SIZE, inner), lambda i: (0, 0, 0)),
            whole, whole,
            pl.BlockSpec((CHUNK, inner), lambda i: (i, 0)),
            pl.BlockSpec((1, inner), lambda i: (0, 0)),
        ],
        out_specs=pl.BlockSpec((CHUNK, inner), lambda i: (i, 0)),
        out_shape=jax.ShapeDtypeStruct((rows, inner), jnp.bfloat16),
        scratch_shapes=[
            pltpu.VMEM((STATE_SIZE, inner), jnp.float32),
            pltpu.VMEM((chunks, STATE_SIZE, inner), jnp.float32),
            pltpu.VMEM((CHUNK, inner), jnp.float32),
        ],
        cost_estimate=pl.CostEstimate(
            flops=8 * rows * inner * STATE_SIZE, bytes_accessed=16 * rows * inner,
            transcendentals=rows * CHUNK * heads,
        ),
        name="chunk_outputs",
    )(
        act, *decay, *step, decay[0].T, decay[1].T, step[0].T, step[1].T, decay[1],
        fresh[0], fresh[1], incoming[0], incoming[1], gate, gain,
    )


def entering_state(end, total, axis, head_size, reverse):
    count = lax.axis_size(axis)
    states = end.shape[0]

    def moved(packet, distance):
        pairs = [(i, i + distance) for i in range(count - distance)]
        if reverse:
            pairs = [(target, source) for source, target in pairs]
        return lax.ppermute(packet, axis, pairs)

    decay = jnp.broadcast_to(jnp.repeat(jnp.exp(total), head_size)[None, :], (16, end.shape[1]))
    packet = jnp.concatenate([end, decay], axis=0).astype(jnp.bfloat16)
    packet = moved(packet, 1)
    distance = 1
    held = packet.astype(jnp.float32)
    while distance < count - 1:
        arrived = moved(held.astype(jnp.bfloat16), distance).astype(jnp.float32)
        factor = held[states : states + 1]
        added = jnp.concatenate([held[:states], jnp.zeros_like(held[states:])], axis=0)
        held = added + factor * arrived
        distance *= 2
    return held[:states]


def local(
    tokens,
    norm_gain,
    query_weight,
    key_weight,
    value_weight,
    query_gain,
    key_gain,
    sink_logit,
    gate_weight,
    inner_weight,
    input_map,
    output_map,
    step_weight,
    conv_inner,
    conv_pair,
    decay_rate,
    decay_jump,
    inner_gain,
    attn_out_weight,
    ssm_out_weight,
):
    row_total = tokens.shape[0]
    seq_total = row_total * lax.axis_size("sp")
    seq_first = lax.axis_index("sp") * row_total
    positions = seq_first + jnp.arange(row_total, dtype=jnp.int32)
    normed = rms_rows(tokens.astype(jnp.float32), norm_gain.astype(jnp.float32)).astype(
        jnp.bfloat16
    )

    def project(weight):
        result = jnp.dot(normed, weight, preferred_element_type=jnp.float32)
        return lax.optimization_barrier(result.astype(jnp.bfloat16))

    head_size = query_gain.shape[0]
    query = project(query_weight).reshape(row_total, -1, head_size)
    keyed = project(key_weight).reshape(row_total, -1, head_size)
    value = project(value_weight)
    query = rotate(rms_rows(query.astype(jnp.float32), query_gain), positions).astype(jnp.bfloat16)
    keyed = rotate(rms_rows(keyed.astype(jnp.float32), key_gain), positions).astype(jnp.bfloat16)
    key_heads = keyed.shape[1]
    packed = jnp.concatenate([keyed.reshape(row_total, -1), value], axis=1)
    rimmed_keys = extended(packed, (("sp", 0),), WINDOW)
    inner_rows = project(inner_weight)
    inner_width = inner_rows.shape[1]
    map_width = input_map.shape[1]
    carried_in = jnp.concatenate([inner_rows, project(input_map), project(output_map)], axis=1)
    tap_count = conv_inner.shape[0]
    conv_table = jnp.concatenate([conv_inner, conv_pair.reshape(tap_count, -1)], axis=1).astype(
        jnp.float32
    )
    rimmed_rows = extended(carried_in, (("sp", 0),), HALO)
    step_rows = project(step_weight.reshape(step_weight.shape[0], -1))
    step = jax.nn.softplus(step_rows.astype(jnp.float32))
    log_decay = -decay_rate.reshape(1, -1) * step + decay_jump.reshape(row_total, -1)
    heads_here = inner_width // head_size
    steps = (step[:, :heads_here], step[:, heads_here:])
    decays = (log_decay[:, :heads_here], log_decay[:, heads_here:])
    act, fresh_forward, fresh_backward, end_forward, end_backward = chunk_states(
        rimmed_rows, conv_table, tap_count, inner_width, map_width, decays, steps
    )
    from_lower = entering_state(end_forward, jnp.sum(decays[0], axis=0), "sp", head_size, False)
    from_higher = entering_state(end_backward, jnp.sum(decays[1], axis=0), "sp", head_size, True)
    attn_out = attend(
        query.reshape(row_total, -1), rimmed_keys, sink_logit, seq_first, seq_total, head_size,
        key_heads,
    )
    gate_rows = project(gate_weight)
    ssm_out = chunk_outputs(
        head_size, inner_width, map_width, act, decays, steps, (fresh_forward, fresh_backward),
        (from_lower, from_higher), gate_rows, inner_gain.astype(jnp.float32)[None, :],
    )
    partial_sum = jnp.dot(attn_out, attn_out_weight, preferred_element_type=jnp.float32)
    partial_sum = partial_sum + jnp.dot(ssm_out, ssm_out_weight, preferred_element_type=jnp.float32)
    rounded = lax.optimization_barrier(partial_sum.astype(jnp.bfloat16))
    return lax.psum_scatter(
        rounded.astype(jnp.float32).astype(jnp.bfloat16), "tp", scatter_dimension=0, tiled=True
    )


def solution(mesh):
    in_specs = (
        P("sp", None),
        P(),
        P(None, "tp"),
        P(None, "tp"),
        P(None, "tp"),
        P(),
        P(),
        P("tp"),
        P(None, "tp"),
        P(None, "tp"),
        P(None, "tp"),
        P(None, "tp"),
        P(None, None, "tp"),
        P(None, "tp"),
        P(None, None, "tp"),
        P(None, "tp"),
        P("sp", None, "tp"),
        P("tp"),
        P("tp", None),
        P("tp", None),
    )
    out_specs = P(("sp", "tp"), None)
    return jax.shard_map(local, mesh=mesh, in_specs=in_specs, out_specs=out_specs, check_vma=False)
```

profile of v0, /device:TPU:0, one launch (start us, length us, event | category | flops | bytes accessed | tf_op | source)
XLA Modules:
  0.0 268.3 jit_solution(17870361738169149206)
XLA Ops:
  6.6 3.2 %fusion = f32[1024]{0:T(1024)S(1)} fusion(bf16[1024,2048]{1,0:T(8,128)(2,1)} %param.20), kind=kLoop, calls=%fused_computation.2 | loop fusion | flops 6290432 | bytes 4198400 | tf_op jit(solution)/shard_map/reduce_sum | solution.py:34
  9.8 3.3 %fusion.2 = bf16[1024,2048]{1,0:T(8,128)(2,1)S(1)} fusion(bf16[1024,2048]{1,0:T(8,128)(2,1)} %param.20, f32[2048]{0:T(1024)S(1)} %convert_element_type.116, f32[1024]{0:T(1024)S(1)} %add_rsqrt_fusion.2), kind=kLoop, calls=%fused_computation.4 | loop fusion | flops 8388608 | bytes 8400896 | tf_op jit(solution)/shard_map/convert_element_type | solution.py:385
  13.1 1.2 convolution_convert_fusion.5
  15.1 1.2 convolution_convert_fusion.6
  18.2 5.8 %collective-permute-start = (bf16[128,256]{1,0:T(8,128)(2,1)}, bf16[128,256]{1,0:T(8,128)(2,1)}, u32[]{:S(2)}, u32[]{:S(2)}) collective-permute-start(bf16[128,256]{1,0:T(8,128)(2,1)} %get-tuple-element.31), channel_id=1, source_target_pairs={{0,4},{4,8},{8,12},{12,16},{16,20},{20,24},{24,28},{1,5},{5,9},{9,... | collective-permute-start | bytes 196616 | tf_op jit(solution)/shard_map/ppermute | solution.py:25
  24.0 1.3 collective-permute-start.1
  25.3 3.7 %convolution_convert_fusion.3 = bf16[1024,256]{1,0:T(8,128)(2,1)S(1)} fusion(bf16[1024,2048]{1,0:T(8,128)(2,1)} %copy-done.1, bf16[2048,256]{1,0:T(8,128)(2,1)} %param.31), kind=kOutput, calls=%fused_computation.13 | convolution fusion | flops 1074003968 | bytes 5767168 | tf_op jit(solution)/shard_map/dot_general | solution.py:390
  29.1 1.2 convolution_convert_fusion.4
  31.3 4.7 %convolution_convert_fusion.1 = bf16[1024,1024]{1,0:T(8,128)(2,1)S(1)} fusion(bf16[1024,2048]{1,0:T(8,128)(2,1)S(1)} %copy-done.2, bf16[2048,1024]{1,0:T(8,128)(2,1)S(1)} %copy-done.22), kind=kOutput, calls=%fused_computation.10 | convolution fusion | flops 4296015872 | bytes 10485760 | tf_op jit(solution)/shard_map/dot_general | solution.py:390
  36.0 1.3 copy-done.5
  38.0 5.2 %collective-permute-start.2 = (bf16[16,1536]{1,0:T(8,128)(2,1)}, bf16[16,1536]{1,0:T(8,128)(2,1)}, u32[]{:S(2)}, u32[]{:S(2)}) collective-permute-start(bf16[16,1536]{1,0:T(8,128)(2,1)} %get-tuple-element.25), channel_id=1, source_target_pairs={{0,4},{4,8},{8,12},{12,16},{16,20},{20,24},{24,28},{1,5},{5,9},{9,... | collective-permute-start | bytes 147464 | tf_op jit(solution)/shard_map/ppermute | solution.py:25
  43.1 1.5 collective-permute-start.3
  45.3 1.9 copy.42
  47.2 4.2 %convolution_convert_fusion.7 = bf16[1024,32]{0,1:T(8,128)(2,1)} fusion(bf16[1024,2048]{1,0:T(8,128)(2,1)} %copy-done.1, bf16[2048,32]{0,1:T(8,128)(2,1)} %bitcast.52), kind=kOutput, calls=%fused_computation.17 | convolution fusion | flops 134250496 | bytes 4390912 | tf_op jit(solution)/shard_map/dot_general | solution.py:390
  51.4 1.7 copy.41
  53.1 6.3 %convolution_convert_fusion.2 = bf16[1024,512]{1,0:T(8,128)(2,1)} fusion(bf16[1024,2048]{1,0:T(8,128)(2,1)} %copy-done.1, bf16[2048,512]{1,0:T(8,128)(2,1)} %param.22), kind=kOutput, calls=%fused_computation.12 | convolution fusion | flops 2148007936 | bytes 7340032 | tf_op jit(solution)/shard_map/dot_general | solution.py:390
  59.4 5.7 %convolution_convert_fusion.gate_ref = bf16[1024,1024]{1,0:T(8,128)(2,1)} fusion(bf16[1024,2048]{1,0:T(8,128)(2,1)S(1)} %copy-done.3, bf16[2048,1024]{1,0:T(8,128)(2,1)S(1)} %copy-done.23), kind=kOutput, calls=%fused_computation.9 | convolution fusion | flops 4296015872 | bytes 10485760 | tf_op jit(solution)/shard_map/dot_general | solution.py:390
  65.5 2.3 slice_bitcast_fusion
  68.5 2.6 copy.37
  71.4 4.1 %pad_maximum_fusion.rows_ref = bf16[1056,1536]{1,0:T(8,128)(2,1)} fusion(bf16[16,1536]{1,0:T(8,128)(2,1)} %collective-permute-done.3, bf16[1024,256]{1,0:T(8,128)(2,1)S(1)} %convolution_convert_fusion.3, bf16[1024,256]{1,0:T(8,128)(2,1)S(1)} %convolution_convert_fusion.4, bf16[1024,1024]{1,0:T(8,128)(2,1)} %copy-done.5, ...), kind=kLoop, calls=%fused_computation.6 | loop fusion | flops 16220160 | bytes 6488064 | tf_op jit(solution)/shard_map/concatenate | solution.py:29
  75.5 17.9 %chunk_states.1 = (bf16[1024,1536]{1,0:T(8,128)(2,1)}, f32[8,128,1024]{2,1,0:T(8,128)}, f32[8,128,1024]{2,1,0:T(8,128)}, f32[128,1024]{1,0:T(8,128)}, f32[128,1024]{1,0:T(8,128)}) custom-call(bf16[1056,1536]{1,0:T(8,128)(2,1)} %pad_maximum_fusion.rows_ref, f32[5,1536]{1,0:T(8,128)} %maximum_convert_fusion.taps_ref, f32[1024,16]{1,0:T(8,128)} %get-tuple-element.51.ldf_ref, ...), custom_call_target="tpu_custom_call" | custom-call | flops 1073741824 | bytes 16777216 | tf_op jit(solution)/shard_map/chunk_states/pallas_call | solution.py:273
  93.4 1.2 convert.33
  94.6 1.1 convert.35
  95.8 1.3 collective-permute-start.8
  97.1 5.3 %collective-permute-start.4 = (bf16[144,1024]{1,0:T(8,128)(2,1)S(1)}, bf16[144,1024]{1,0:T(8,128)(2,1)S(1)}, u32[]{:S(2)}, u32[]{:S(2)}) collective-permute-start(bf16[144,1024]{1,0:T(8,128)(2,1)S(1)} %pad_maximum_fusion.3), channel_id=1, source_target_pairs={{0,4},{4,8},{8,12},{12,16},{16,20},{20,24},{24,28},{1,5},{5,9},{9,... | collective-permute-start | bytes 884744 | tf_op jit(solution)/shard_map/ppermute | solution.py:343
  102.8 3.4 %collective-permute-done.8 = bf16[144,1024]{1,0:T(8,128)(2,1)S(1)} collective-permute-done((bf16[144,1024]{1,0:T(8,128)(2,1)S(1)}, bf16[144,1024]{1,0:T(8,128)(2,1)S(1)}, u32[]{:S(2)}, u32[]{:S(2)}) %collective-permute-start.8) | collective-permute-done | bytes 294944 | tf_op jit(solution)/shard_map/ppermute | solution.py:343
  106.2 1.3 collective-permute-start.9
  107.5 5.2 %collective-permute-done.4 = bf16[144,1024]{1,0:T(8,128)(2,1)S(1)} collective-permute-done((bf16[144,1024]{1,0:T(8,128)(2,1)S(1)}, bf16[144,1024]{1,0:T(8,128)(2,1)S(1)}, u32[]{:S(2)}, u32[]{:S(2)}) %collective-permute-start.4) | collective-permute-done | bytes 294944 | tf_op jit(solution)/shard_map/ppermute | solution.py:343
  112.7 4.4 %collective-permute-start.5 = (bf16[144,1024]{1,0:T(8,128)(2,1)S(1)}, bf16[144,1024]{1,0:T(8,128)(2,1)S(1)}, u32[]{:S(2)}, u32[]{:S(2)}) collective-permute-start(bf16[144,1024]{1,0:T(8,128)(2,1)S(1)} %collective-permute-done.4), channel_id=1, source_target_pairs={{0,4},{4,8},{8,12},{12,16},{16,20},{20,24},{24,28},{1,5},{5,9},{9,... | collective-permute-start | bytes 884744 | tf_op jit(solution)/shard_map/ppermute | solution.py:343
  117.6 9.5 %collective-permute-done.5 = bf16[144,1024]{1,0:T(8,128)(2,1)S(1)} collective-permute-done((bf16[144,1024]{1,0:T(8,128)(2,1)S(1)}, bf16[144,1024]{1,0:T(8,128)(2,1)S(1)}, u32[]{:S(2)}, u32[]{:S(2)}) %collective-permute-start.5) | collective-permute-done | bytes 294944 | tf_op jit(solution)/shard_map/ppermute | solution.py:343
  127.1 1.4 fusion.10
  128.5 1.3 collective-permute-start.10
  129.8 6.0 %collective-permute-start.6 = (bf16[144,1024]{1,0:T(8,128)(2,1)}, bf16[144,1024]{1,0:T(8,128)(2,1)}, u32[]{:S(2)}, u32[]{:S(2)}) collective-permute-start(bf16[144,1024]{1,0:T(8,128)(2,1)} %get-tuple-element.49), channel_id=1, source_target_pairs={{0,8},{4,12},{8,16},{12,20},{16,24},{20,28},{1,9},{5,13},{9,17},{1... | collective-permute-start | bytes 884744 | tf_op jit(solution)/shard_map/ppermute | solution.py:343
  136.9 1.3 copy.40.query_ref
  138.2 1.9 copy.46.stbt_ref
  140.1 1.8 copy.45.stft_ref
  141.9 1.8 copy.44.ldbt_ref
  143.7 1.8 copy.43.ldft_ref
  147.7 2.7 %fusion.9 = (bf16[144,1024]{1,0:T(8,128)(2,1)}, f32[144,1024]{1,0:T(8,128)S(1)}, bf16[144,1024]{1,0:T(8,128)(2,1)}, f32[144,1024]{1,0:T(8,128)}) fusion(bf16[144,1024]{1,0:T(8,128)(2,1)} %collective-permute-done.10, f32[1024]{0:T(1024)S(1)} %bitcast.58, f32[144,1024]{1,0:T(8,128)} %get-tuple-element.20, pred[144]{0:T(512)(128)(4,1)S(1)} %copy-done.15, ...), kind=kLoop, calls=%fused_computation.66 | loop fusion | flops 1474560 | bytes 3547280 | tf_op jit(solution)/shard_map/convert_element_type | solution.py:351
  150.4 1.3 collective-permute-start.11
  151.7 6.9 %collective-permute-start.7 = (bf16[144,1024]{1,0:T(8,128)(2,1)}, bf16[144,1024]{1,0:T(8,128)(2,1)}, u32[]{:S(2)}, u32[]{:S(2)}) collective-permute-start(bf16[144,1024]{1,0:T(8,128)(2,1)} %get-tuple-element.47), channel_id=1, source_target_pairs={{0,16},{4,20},{8,24},{12,28},{1,17},{5,21},{9,25},{13,29},{2,18},{... | collective-permute-start | bytes 884744 | tf_op jit(solution)/shard_map/ppermute | solution.py:343
  158.6 1.8 pad_maximum_fusion.2.rim_ref
  160.4 26.0 %attend.1 = bf16[1024,512]{1,0:T(8,128)(2,1)} custom-call(s32[2]{0:T(128)} %pad_add_fusion.place_ref, f32[8]{0:T(128)} %sink_ref.1, bf16[1024,512]{1,0:T(8,128)(2,1)} %copy.40.query_ref, bf16[1280,256]{1,0:T(8,128)(2,1)} %pad_maximum_fusion.2.rim_ref), custom_call_target="tpu_custom_call" | custom-call | flops 805306368 | bytes 2097152 | tf_op jit(solution)/shard_map/attend/pallas_call | solution.py:246
  186.5 2.2 fusion.7
  188.7 17.9 %chunk_outputs.1 = bf16[1024,1024]{1,0:T(8,128)(2,1)} custom-call(bf16[1024,1536]{1,0:T(8,128)(2,1)} %get-tuple-element.10.act_ref, f32[1024,16]{1,0:T(8,128)} %get-tuple-element.51.ldf_ref, f32[1024,16]{1,0:T(8,128)} %get-tuple-element.52.ldb_ref.ldball_ref, f32[1024,16]{1,0:T(8,128)} %get-tuple-element.39.stf_ref, f32[1024,16]{1,0:T(8,128)} %get-tuple-element.38.stb_ref, ...), custom_call_target="tpu_custom_call" | custom-call | flops 1073741824 | bytes 16777216 | tf_op jit(solution)/shard_map/chunk_outputs/pallas_call | solution.py:304
  206.6 7.0 %fusion.13 = f32[1024,2048]{1,0:T(8,128)S(1)} fusion(bf16[1024,1024]{1,0:T(8,128)(2,1)} %chunk_outputs.1, bf16[1024,2048]{1,0:T(8,128)(2,1)} %param.39), kind=kOutput, calls=%fused_computation.70 | convolution fusion | flops 4294967296 | bytes 14680064 | tf_op jit(solution)/shard_map/dot_general | solution.py:432
  213.6 4.3 %add_convert_fusion = bf16[1024,2048]{1,0:T(8,128)(2,1)} fusion(f32[1024,2048]{1,0:T(8,128)S(1)} %fusion.13, bf16[1024,512]{1,0:T(8,128)(2,1)S(1)} %copy-done.27, bf16[512,2048]{1,0:T(8,128)(2,1)S(1)} %copy-done), kind=kOutput, calls=%fused_computation.5 | convolution fusion | flops 2151677952 | bytes 15728640 | tf_op jit(solution)/shard_map/dot_general | solution.py:431
  218.0 43.5 %reduce-scatter.2.cloned.1.call-done = bf16[256,2048]{1,0:T(8,128)(2,1)} async-done(((bf16[1024,2048]{1,0:T(8,128)(2,1)}), bf16[256,2048]{1,0:T(8,128)(2,1)}) %reduce-scatter.2.cloned.1.call-update) | async-done | bytes 1048592 | tf_op jit(solution)/shard_map/reduce_scatter | solution.py:434
  (108 shorter events, 10.2 us)
Async XLA Ops:
  6.5 207.1 %copy-start = (bf16[512,2048]{1,0:T(8,128)(2,1)S(1)}, bf16[512,2048]{1,0:T(8,128)(2,1)}, u32[]{:S(2)}) copy-start(bf16[512,2048]{1,0:T(8,128)(2,1)} %param.38) | copy-start | bytes 6291460
  6.5 3.3 %copy-start.16 = (bf16[2048]{0:T(1024)(128)(2,1)S(1)}, bf16[2048]{0:T(1024)(128)(2,1)}, u32[]{:S(2)}) copy-start(bf16[2048]{0:T(1024)(128)(2,1)} %param.21) | copy-start | bytes 12292
  6.5 254.9 %reduce-scatter.2.cloned.1.call-start = ((), (), s32[]{:S(2)}) async-start(), calls=%async_computation.1 | async-start | bytes 5242880 | tf_op jit(solution)/shard_map/reduce_scatter | solution.py:434
  9.8 3.3 %copy-start.25 = (bf16[2048,128]{1,0:T(8,128)(2,1)S(1)}, bf16[2048,128]{1,0:T(8,128)(2,1)}, u32[]{:S(2)}) copy-start(bf16[2048,128]{1,0:T(8,128)(2,1)} %param.24) | copy-start | bytes 1572868
  13.1 2.0 copy-start.1
  13.1 2.0 copy-start.26
  15.1 2.4 copy-start.10
  15.1 2.0 copy-start.19
  17.1 8.2 %copy-start.8 = (f32[1024,32]{0,1:T(8,128)}, f32[1024,32]{0,1:T(8,128)S(1)}, u32[]{:S(2)}) copy-start(f32[1024,32]{0,1:T(8,128)S(1)} %get-tuple-element.44) | copy-start | bytes 393220
  17.5 11.5 %copy-start.2 = (bf16[1024,2048]{1,0:T(8,128)(2,1)S(1)}, bf16[1024,2048]{1,0:T(8,128)(2,1)}, u32[]{:S(2)}) copy-start(bf16[1024,2048]{1,0:T(8,128)(2,1)} %copy-done.1) | copy-start | bytes 12582916
  17.6 11.5 %copy-start.24 = (bf16[2048,256]{1,0:T(8,128)(2,1)S(1)}, bf16[2048,256]{1,0:T(8,128)(2,1)}, u32[]{:S(2)}) copy-start(bf16[2048,256]{1,0:T(8,128)(2,1)} %param.30) | copy-start | bytes 3145732
  18.2 140.4 %collective-permute-start = (bf16[128,256]{1,0:T(8,128)(2,1)}, bf16[128,256]{1,0:T(8,128)(2,1)}, u32[]{:S(2)}, u32[]{:S(2)}) collective-permute-start(bf16[128,256]{1,0:T(8,128)(2,1)} %get-tuple-element.31), channel_id=1, source_target_pairs={{0,4},{4,8},{8,12},{12,16},{16,20},{20,24},{24,28},{1,5},{5,9},{9,... | collective-permute-start | bytes 196616 | tf_op jit(solution)/shard_map/ppermute | solution.py:25
  24.0 134.6 %collective-permute-start.1 = (bf16[128,256]{1,0:T(8,128)(2,1)}, bf16[128,256]{1,0:T(8,128)(2,1)}, u32[]{:S(2)}, u32[]{:S(2)}) collective-permute-start(bf16[128,256]{1,0:T(8,128)(2,1)} %get-tuple-element.32), channel_id=1, source_target_pairs={{4,0},{8,4},{12,8},{16,12},{20,16},{24,20},{28,24},{5,1},{9,5},{13... | collective-permute-start | bytes 196616 | tf_op jit(solution)/shard_map/ppermute | solution.py:28
  29.1 2.2 copy-start.22
  31.3 13.3 %copy-start.18 = (f32[2,16]{1,0:T(2,128)S(1)}, f32[2,16]{1,0:T(2,128)}, u32[]{:S(2)}) copy-start(f32[2,16]{1,0:T(2,128)} %param.35) | copy-start | bytes 388
  31.3 14.0 %copy-start.14 = (bf16[5,2,256]{2,1,0:T(2,128)(2,1)S(1)}, bf16[5,2,256]{2,1,0:T(2,128)(2,1)}, u32[]{:S(2)}) copy-start(bf16[5,2,256]{2,1,0:T(2,128)(2,1)} %param.34) | copy-start | bytes 15364
  36.0 1.4 copy-start.5
  38.0 33.4 %collective-permute-start.2 = (bf16[16,1536]{1,0:T(8,128)(2,1)}, bf16[16,1536]{1,0:T(8,128)(2,1)}, u32[]{:S(2)}, u32[]{:S(2)}) collective-permute-start(bf16[16,1536]{1,0:T(8,128)(2,1)} %get-tuple-element.25), channel_id=1, source_target_pairs={{0,4},{4,8},{8,12},{12,16},{16,20},{20,24},{24,28},{1,5},{5,9},{9,... | collective-permute-start | bytes 147464 | tf_op jit(solution)/shard_map/ppermute | solution.py:25
  43.1 28.3 %collective-permute-start.3 = (bf16[16,1536]{1,0:T(8,128)(2,1)}, bf16[16,1536]{1,0:T(8,128)(2,1)}, u32[]{:S(2)}, u32[]{:S(2)}) collective-permute-start(bf16[16,1536]{1,0:T(8,128)(2,1)} %get-tuple-element.26), channel_id=1, source_target_pairs={{4,0},{8,4},{12,8},{16,12},{20,16},{24,20},{28,24},{5,1},{9,5},{13... | collective-permute-start | bytes 147464 | tf_op jit(solution)/shard_map/ppermute | solution.py:28
  53.1 6.3 %copy-start.3 = (bf16[1024,2048]{1,0:T(8,128)(2,1)S(1)}, bf16[1024,2048]{1,0:T(8,128)(2,1)}, u32[]{:S(2)}) copy-start(bf16[1024,2048]{1,0:T(8,128)(2,1)} %copy-done.1) | copy-start | bytes 12582916
  53.1 6.3 %copy-start.23 = (bf16[2048,1024]{1,0:T(8,128)(2,1)S(1)}, bf16[2048,1024]{1,0:T(8,128)(2,1)}, u32[]{:S(2)}) copy-start(bf16[2048,1024]{1,0:T(8,128)(2,1)} %param.28) | copy-start | bytes 12582916
  59.4 5.7 %copy-start.7 = (f32[1024,32]{1,0:T(8,128)S(1)}, f32[1024,32]{1,0:T(8,128)}, u32[]{:S(2)}) copy-start(f32[1024,32]{1,0:T(8,128)} %copy.42) | copy-start | bytes 393220
  59.4 5.7 %copy-start.12 = (bf16[1024,32]{1,0:T(8,128)(2,1)S(1)}, bf16[1024,32]{1,0:T(8,128)(2,1)}, u32[]{:S(2)}) copy-start(bf16[1024,32]{1,0:T(8,128)(2,1)} %copy.41) | copy-start | bytes 196612
  59.4 5.7 %copy-start.21 = (f32[32]{0:T(128)S(1)}, f32[32]{0:T(128)}, u32[]{:S(2)}) copy-start(f32[32]{0:T(128)} %neg.25) | copy-start | bytes 388
  65.1 2.7 %copy-start.13 = (bf16[5,1024]{1,0:T(8,128)(2,1)S(1)}, bf16[5,1024]{1,0:T(8,128)(2,1)}, u32[]{:S(2)}) copy-start(bf16[5,1024]{1,0:T(8,128)(2,1)} %param.33) | copy-start | bytes 30724
  75.5 41.6 %copy-start.20 = (f32[64]{0:T(128)S(1)}, f32[64]{0:T(128)}, u32[]{:S(2)}) copy-start(f32[64]{0:T(128)} %param.25) | copy-start | bytes 772
  93.4 9.1 %copy-start.4 = (f32[1024,512]{0,1:T(8,128)S(1)}, f32[1024,512]{0,1:T(8,128)}, u32[]{:S(2)}) copy-start(f32[1024,512]{0,1:T(8,128)} %copy.37) | copy-start | bytes 6291460
  94.6 32.5 %copy-start.15 = (pred[144]{0:T(512)(128)(4,1)S(1)}, pred[144]{0:T(512)(128)(4,1)}, u32[]{:S(2)}) copy-start(pred[144]{0:T(512)(128)(4,1)} %constant.39.clone.1) | copy-start | bytes 436
  95.8 10.5 %collective-permute-start.8 = (bf16[144,1024]{1,0:T(8,128)(2,1)S(1)}, bf16[144,1024]{1,0:T(8,128)(2,1)S(1)}, u32[]{:S(2)}, u32[]{:S(2)}) collective-permute-start(bf16[144,1024]{1,0:T(8,128)(2,1)S(1)} %pad_maximum_fusion.4), channel_id=1, source_target_pairs={{4,0},{8,4},{12,8},{16,12},{20,16},{24,20},{28,24},{5,1},{9,5},{13... | collective-permute-start | bytes 884744 | tf_op jit(solution)/shard_map/ppermute | solution.py:343
  97.1 38.7 %copy-start.9 = (f32[1024,32]{0,1:T(8,128)S(1)}, f32[1024,32]{0,1:T(8,128)}, u32[]{:S(2)}) copy-start(f32[1024,32]{0,1:T(8,128)} %copy-done.8) | copy-start | bytes 393220
  97.1 15.6 %collective-permute-start.4 = (bf16[144,1024]{1,0:T(8,128)(2,1)S(1)}, bf16[144,1024]{1,0:T(8,128)(2,1)S(1)}, u32[]{:S(2)}, u32[]{:S(2)}) collective-permute-start(bf16[144,1024]{1,0:T(8,128)(2,1)S(1)} %pad_maximum_fusion.3), channel_id=1, source_target_pairs={{0,4},{4,8},{8,12},{12,16},{16,20},{20,24},{24,28},{1,5},{5,9},{9,... | collective-permute-start | bytes 884744 | tf_op jit(solution)/shard_map/ppermute | solution.py:343
  106.2 11.4 %collective-permute-start.9 = (bf16[144,1024]{1,0:T(8,128)(2,1)S(1)}, bf16[144,1024]{1,0:T(8,128)(2,1)S(1)}, u32[]{:S(2)}, u32[]{:S(2)}) collective-permute-start(bf16[144,1024]{1,0:T(8,128)(2,1)S(1)} %collective-permute-done.8), channel_id=1, source_target_pairs={{4,0},{8,4},{12,8},{16,12},{20,16},{24,20},{28,24},{5,1},{9,5},{13... | collective-permute-start | bytes 884744 | tf_op jit(solution)/shard_map/ppermute | solution.py:343
  112.7 14.4 %collective-permute-start.5 = (bf16[144,1024]{1,0:T(8,128)(2,1)S(1)}, bf16[144,1024]{1,0:T(8,128)(2,1)S(1)}, u32[]{:S(2)}, u32[]{:S(2)}) collective-permute-start(bf16[144,1024]{1,0:T(8,128)(2,1)S(1)} %collective-permute-done.4), channel_id=1, source_target_pairs={{0,4},{4,8},{8,12},{12,16},{16,20},{20,24},{24,28},{1,5},{5,9},{9,... | collective-permute-start | bytes 884744 | tf_op jit(solution)/shard_map/ppermute | solution.py:343
  117.6 18.6 %copy-start.17 = (bf16[1024]{0:T(1024)(128)(2,1)S(1)}, bf16[1024]{0:T(1024)(128)(2,1)}, u32[]{:S(2)}) copy-start(bf16[1024]{0:T(1024)(128)(2,1)} %param.37) | copy-start | bytes 6148
  128.5 19.2 %collective-permute-start.10 = (bf16[144,1024]{1,0:T(8,128)(2,1)}, bf16[144,1024]{1,0:T(8,128)(2,1)}, u32[]{:S(2)}, u32[]{:S(2)}) collective-permute-start(bf16[144,1024]{1,0:T(8,128)(2,1)} %get-tuple-element.19), channel_id=1, source_target_pairs={{8,0},{12,4},{16,8},{20,12},{24,16},{28,20},{9,1},{13,5},{17,9},{2... | collective-permute-start | bytes 884744 | tf_op jit(solution)/shard_map/ppermute | solution.py:343
  129.8 17.9 %collective-permute-start.6 = (bf16[144,1024]{1,0:T(8,128)(2,1)}, bf16[144,1024]{1,0:T(8,128)(2,1)}, u32[]{:S(2)}, u32[]{:S(2)}) collective-permute-start(bf16[144,1024]{1,0:T(8,128)(2,1)} %get-tuple-element.49), channel_id=1, source_target_pairs={{0,8},{4,12},{8,16},{12,20},{16,24},{20,28},{1,9},{5,13},{9,17},{1... | collective-permute-start | bytes 884744 | tf_op jit(solution)/shard_map/ppermute | solution.py:343
  138.2 20.4 %copy-start.11 = (bf16[1024,128]{1,0:T(8,128)(2,1)S(1)}, bf16[1024,128]{1,0:T(8,128)(2,1)}, u32[]{:S(2)}) copy-start(bf16[1024,128]{1,0:T(8,128)(2,1)} %copy-done.10) | copy-start | bytes 786436
  150.4 36.1 %collective-permute-start.11 = (bf16[144,1024]{1,0:T(8,128)(2,1)}, bf16[144,1024]{1,0:T(8,128)(2,1)}, u32[]{:S(2)}, u32[]{:S(2)}) collective-permute-start(bf16[144,1024]{1,0:T(8,128)(2,1)} %get-tuple-element.17), channel_id=1, source_target_pairs={{16,0},{20,4},{24,8},{28,12},{17,1},{21,5},{25,9},{29,13},{18,2},{... | collective-permute-start | bytes 884744 | tf_op jit(solution)/shard_map/ppermute | solution.py:343
  151.7 34.8 %collective-permute-start.7 = (bf16[144,1024]{1,0:T(8,128)(2,1)}, bf16[144,1024]{1,0:T(8,128)(2,1)}, u32[]{:S(2)}, u32[]{:S(2)}) collective-permute-start(bf16[144,1024]{1,0:T(8,128)(2,1)} %get-tuple-element.47), channel_id=1, source_target_pairs={{0,16},{4,20},{8,24},{12,28},{1,17},{5,21},{9,25},{13,29},{2,18},{... | collective-permute-start | bytes 884744 | tf_op jit(solution)/shard_map/ppermute | solution.py:343
  160.4 26.0 %copy-start.6 = (f32[144,1024]{1,0:T(8,128)S(1)}, f32[144,1024]{1,0:T(8,128)}, u32[]{:S(2)}) copy-start(f32[144,1024]{1,0:T(8,128)} %get-tuple-element.48) | copy-start | bytes 1769476
  206.6 7.0 %copy-start.27 = (bf16[1024,512]{1,0:T(8,128)(2,1)S(1)}, bf16[1024,512]{1,0:T(8,128)(2,1)}, u32[]{:S(2)}) copy-start(bf16[1024,512]{1,0:T(8,128)(2,1)} %attend.1) | copy-start | bytes 3145732
Sparse Core Ops, SparseCore 0:
  218.1 43.3 reduce-scatter.1
where the time goes:
time: 269 us; the launch traced here: 268 us
  Pallas kernels  61.8 us (23%)
  waiting for transfers between devices  61.6 us (23%)
  starting transfers between devices  41.5 us (15%)
  matrix products  39.7 us (15%)
  other arithmetic  28.9 us (11%)
  local copies, waits for them, and re-layouts  20.8 us (8%)
  between operations  14 us (5%)
    reduce_scatter x1, waiting for transfers between devices, local(): lax.psum_scatter(rounded.astype(jnp.float32).astype(jnp.bfloat16), 'tp',...  43.5 us
    dot_general x8, matrix products, project(): result = jnp.dot(normed, weight, preferred_element_type=jnp.float32)  28.3 us
    ppermute x8, starting transfers between devices, moved(): return lax.ppermute(packet, axis, pairs)  27.8 us
    pallas_call x1, Pallas kernels, attend(): pl.pallas_call(functools.partial(attend_kernel, head_size, key_heads), gr...  26 us
    ppermute x8, waiting for transfers between devices, moved(): return lax.ppermute(packet, axis, pairs)  18.1 us
    pallas_call x1, Pallas kernels, chunk_outputs(): pl.pallas_call(functools.partial(outputs_kernel, head_size, inner, maps),...  17.9 us
    pallas_call x1, Pallas kernels, chunk_states(): pl.pallas_call(functools.partial(states_kernel, tap_count, inner, maps),...  17.9 us
    ppermute x2, starting transfers between devices, extended(): lax.ppermute(lax.slice_in_dim(block, block.shape[dim] - width, None, axis...  11 us
  transfers between devices with their start and end apart: 13, of which 4 were waited for; matrix products, arithmetic and copies ran while one was open for 23% of the time, Pallas kernels for 16%

commit v1 on v0

--- a/solution.py
+++ b/solution.py
@@ -15,6 +15,8 @@
 NORM_EPS = 1e-05
 ROPE_BASE = 500000.0
 NEG_FILL = -1e30
+PIECE = 256
+MESH = pl.DeviceIdType.MESH
 
 
 def extended(block, sides, width):
@@ -262,6 +264,126 @@
     )(place, sink_logit, query, rimmed)
 
 
+def combine_kernel(
+    count, attn_ref, ssm_ref, attn_w_ref, ssm_w_ref, out_ref, acc, own, mate_out, mate_in,
+    far_out, far_in, mate_send, mate_recv, far_send, far_recv,
+):
+    me = lax.axis_index("tp")
+    core = lax.rem(me, 2)
+    chip = lax.div(me, 2)
+    chips = count // 2
+    mate = me + 1 - 2 * core
+    rows = out_ref.shape[0]
+    pieces, width = own.shape[1], own.shape[3]
+
+    def chip_of(slot):
+        return lax.rem(chip + 1 + slot, chips)
+
+    def to_mate(slot, j):
+        return pltpu.make_async_remote_copy(
+            src_ref=mate_out.at[slot, j], dst_ref=mate_in.at[slot, j],
+            send_sem=mate_send.at[slot, j], recv_sem=mate_recv.at[slot, j],
+            device_id={"tp": mate}, device_id_type=MESH,
+        )
+
+    def to_far(slot, j):
+        return pltpu.make_async_remote_copy(
+            src_ref=far_out.at[slot, j], dst_ref=far_in.at[slot, j],
+            send_sem=far_send.at[slot, j], recv_sem=far_recv.at[slot, j],
+            device_id={"tp": 2 * chip_of(slot) + core}, device_id_type=MESH,
+        )
+
+    barrier = pltpu.get_barrier_semaphore()
+    pl.semaphore_signal(barrier, inc=1, device_id={"tp": mate}, device_id_type=MESH)
+    for slot in range(chips - 1):
+        pl.semaphore_signal(
+            barrier, inc=1, device_id={"tp": 2 * chip_of(slot) + core}, device_id_type=MESH
+        )
+    pl.semaphore_wait(barrier, chips)
+
+    def compute(slot, j):
+        cols = pl.ds(pl.multiple_of(j * width, width), width)
+        first = pl.multiple_of(chip_of(slot) * 2 * rows, rows)
+        span = pl.ds(first, 2 * rows)
+        acc[...] = jnp.dot(
+            attn_ref[span, :], attn_w_ref[:, cols], preferred_element_type=jnp.float32
+        ) + jnp.dot(ssm_ref[span, :], ssm_w_ref[:, cols], preferred_element_type=jnp.float32)
+        other = acc[pl.ds(pl.multiple_of((1 - core) * rows, rows), rows), :]
+        mate_out[slot, j] = other.astype(jnp.bfloat16)
+        to_mate(slot, j).start()
+        mine = acc[pl.ds(pl.multiple_of(core * rows, rows), rows), :]
+        own[slot, j] = mine.astype(jnp.bfloat16)
+
+    def forward(slot, j):
+        to_mate(slot, j).wait_recv()
+        far_out[slot, j] = (
+            own[slot, j].astype(jnp.float32) + mate_in[slot, j].astype(jnp.float32)
+        ).astype(jnp.bfloat16)
+        to_far(slot, j).start()
+
+    last = chips - 1
+    for slot in range(chips):
+        compute(slot, 0)
+        if slot > 0:
+            forward(slot - 1, pieces - 1)
+
+        @pl.loop(1, pieces)
+        def _(j, slot=slot):
+            compute(slot, j)
+            if slot < last:
+                forward(slot, j - 1)
+
+    @pl.loop(0, pieces)
+    def _(j):
+        to_mate(last, j).wait_recv()
+        total = own[last, j].astype(jnp.float32) + mate_in[last, j].astype(jnp.float32)
+        for slot in range(last):
+            to_far(slot, j).wait_recv()
+            total = total + far_in[slot, j].astype(jnp.float32)
+        out_ref[:, pl.ds(pl.multiple_of(j * width, width), width)] = total.astype(jnp.bfloat16)
+
+    @pl.loop(0, pieces)
+    def _(j):
+        for slot in range(chips):
+            to_mate(slot, j).wait_send()
+        for slot in range(last):
+            to_far(slot, j).wait_send()
+
+
+def combine(attn_out, ssm_out, attn_weight, ssm_weight):
+    count = lax.axis_size("tp")
+    chips = count // 2
+    total, width = attn_out.shape[0], attn_weight.shape[1]
+    rows = total // count
+    pieces = width // PIECE
+    far = max(chips - 1, 1)
+    vmem = pl.BlockSpec(memory_space=pltpu.VMEM)
+    depth = attn_out.shape[1] + ssm_out.shape[1]
+    return pl.pallas_call(
+        functools.partial(combine_kernel, count),
+        in_specs=[vmem] * 4,
+        out_specs=vmem,
+        out_shape=jax.ShapeDtypeStruct((rows, width), jnp.bfloat16),
+        scratch_shapes=[
+            pltpu.VMEM((2 * rows, PIECE), jnp.float32),
+            pltpu.VMEM((chips, pieces, rows, PIECE), jnp.bfloat16),
+            pltpu.VMEM((chips, pieces, rows, PIECE), jnp.bfloat16),
+            pltpu.VMEM((chips, pieces, rows, PIECE), jnp.bfloat16),
+            pltpu.VMEM((far, pieces, rows, PIECE), jnp.bfloat16),
+            pltpu.VMEM((far, pieces, rows, PIECE), jnp.bfloat16),
+            pltpu.SemaphoreType.DMA((chips, pieces)),
+            pltpu.SemaphoreType.DMA((chips, pieces)),
+            pltpu.SemaphoreType.DMA((far, pieces)),
+            pltpu.SemaphoreType.DMA((far, pieces)),
+        ],
+        compiler_params=pltpu.CompilerParams(collective_id=3, has_side_effects=True),
+        cost_estimate=pl.CostEstimate(
+            flops=2 * total * depth * width, bytes_accessed=2 * depth * width, transcendentals=0
+        ),
+        name="combine",
+    )(attn_out, ssm_out, attn_weight, ssm_weight)
+
+
 def chunk_states(rimmed, taps, tap_count, inner, maps, decay, step):
     rows = rimmed.shape[0] - 2 * HALO
     total, heads, chunks = rimmed.shape[1], decay[0].shape[1], rows // CHUNK
@@ -428,12 +550,7 @@
         head_size, inner_width, map_width, act, decays, steps, (fresh_forward, fresh_backward),
         (from_lower, from_higher), gate_rows, inner_gain.astype(jnp.float32)[None, :],
     )
-    partial_sum = jnp.dot(attn_out, attn_out_weight, preferred_element_type=jnp.float32)
-    partial_sum = partial_sum + jnp.dot(ssm_out, ssm_out_weight, preferred_element_type=jnp.float32)
-    rounded = lax.optimization_barrier(partial_sum.astype(jnp.bfloat16))
-    return lax.psum_scatter(
-        rounded.astype(jnp.float32).astype(jnp.bfloat16), "tp", scatter_dimension=0, tiled=True
-    )
+    return combine(attn_out, ssm_out, attn_out_weight, ssm_out_weight)
 
 
 def solution(mesh):

time: 269 us -> 228 us (0.85)
  waiting for transfers between devices: 61.6 us -> 18.2 us
  Pallas kernels: 61.8 us -> 94.5 us
  between operations: 14 us -> 0.63 us
  matrix products: 39.7 us -> 27.7 us
  other arithmetic: 28.9 us -> 26 us
    reduce_scatter x1 -> x0, waiting for transfers between devices: 43.5 us -> none  [local(): lax.psum_scatter(rounded.astype(jnp.float32).astype(jnp.bfloat16), 'tp',...]
    pallas_call x0 -> x1, Pallas kernels: none -> 32.8 us  [combine(): pl.pallas_call(functools.partial(combine_kernel, count), in_specs=[vmem]...]
    dot_general x2 -> x0, matrix products: 11.3 us -> none  [the longest x1 7.01 us: local(): jnp.dot(ssm_out, ssm_out_weight, preferred_element_type=jnp.float32)]
    unnamed x57 -> x56, local copies, waits for them, and re-layouts: 3.09 us -> 5.82 us
  transfers between devices with their start and end apart: 13 -> 12, of which waited for: 4 -> 3; matrix products, arithmetic and copies ran while one was open for 23% -> 25% of each run, Pallas kernels for 16% -> 19%
where the time goes in v1:
time: 228 us; the launch traced here: 227 us
  Pallas kernels  94.5 us (41%)
  starting transfers between devices  40.4 us (18%)
  matrix products  27.7 us (12%)
  other arithmetic  26 us (11%)
  local copies, waits for them, and re-layouts  19.8 us (9%)
  waiting for transfers between devices  18.2 us (8%)
    pallas_call x1, Pallas kernels, combine(): pl.pallas_call(functools.partial(combine_kernel, count), in_specs=[vmem]...  32.8 us
    dot_general x8, matrix products, project(): result = jnp.dot(normed, weight, preferred_element_type=jnp.float32)  27.7 us
    ppermute x8, starting transfers between devices, moved(): return lax.ppermute(packet, axis, pairs)  26.7 us
    pallas_call x1, Pallas kernels, attend(): pl.pallas_call(functools.partial(attend_kernel, head_size, key_heads), gr...  26 us
    ppermute x8, waiting for transfers between devices, moved(): return lax.ppermute(packet, axis, pairs)  18.2 us
    pallas_call x1, Pallas kernels, chunk_outputs(): pl.pallas_call(functools.partial(outputs_kernel, head_size, inner, maps),...  17.9 us
    pallas_call x1, Pallas kernels, chunk_states(): pl.pallas_call(functools.partial(states_kernel, tap_count, inner, maps),...  17.9 us
    ppermute x2, starting transfers between devices, extended(): lax.ppermute(lax.slice_in_dim(block, block.shape[dim] - width, None, axis...  10.9 us
  transfers between devices with their start and end apart: 12, of which 3 were waited for; matrix products, arithmetic and copies ran while one was open for 25% of the time, Pallas kernels for 19%

profile of v1, /device:TPU:0, one launch (start us, length us, event | category | flops | bytes accessed | tf_op | source)
XLA Modules:
  0.0 227.3 jit_solution(12572334040749609487)
XLA Ops:
  0.0 3.2 %fusion = f32[1024]{0:T(1024)S(1)} fusion(bf16[1024,2048]{1,0:T(8,128)(2,1)} %param.20), kind=kLoop, calls=%fused_computation.2 | loop fusion | flops 6290432 | bytes 4198400 | tf_op jit(solution)/shard_map/reduce_sum | solution.py:36
  3.3 3.3 %fusion.2 = bf16[1024,2048]{1,0:T(8,128)(2,1)S(1)} fusion(bf16[1024,2048]{1,0:T(8,128)(2,1)} %param.20, f32[2048]{0:T(1024)S(1)} %convert_element_type.111, f32[1024]{0:T(1024)S(1)} %add_rsqrt_fusion.2), kind=kLoop, calls=%fused_computation.4 | loop fusion | flops 8388608 | bytes 8400896 | tf_op jit(solution)/shard_map/convert_element_type | solution.py:507
  6.6 1.2 convolution_convert_fusion.5
  8.5 1.2 convolution_convert_fusion.6
  12.1 5.8 %collective-permute-start = (bf16[128,256]{1,0:T(8,128)(2,1)}, bf16[128,256]{1,0:T(8,128)(2,1)}, u32[]{:S(2)}, u32[]{:S(2)}) collective-permute-start(bf16[128,256]{1,0:T(8,128)(2,1)} %get-tuple-element.39), channel_id=1, source_target_pairs={{0,4},{4,8},{8,12},{12,16},{16,20},{20,24},{24,28},{1,5},{5,9},{9,... | collective-permute-start | bytes 196616 | tf_op jit(solution)/shard_map/ppermute | solution.py:27
  17.9 1.3 collective-permute-start.1
  19.2 3.7 %convolution_convert_fusion.3 = bf16[1024,256]{1,0:T(8,128)(2,1)S(1)} fusion(bf16[1024,2048]{1,0:T(8,128)(2,1)} %copy-done.2, bf16[2048,256]{1,0:T(8,128)(2,1)} %param.31), kind=kOutput, calls=%fused_computation.12 | convolution fusion | flops 1074003968 | bytes 5767168 | tf_op jit(solution)/shard_map/dot_general | solution.py:512
  22.9 1.2 convolution_convert_fusion.4
  24.2 0.9 copy-done.22
  25.1 4.7 %convolution_convert_fusion.1 = bf16[1024,1024]{1,0:T(8,128)(2,1)S(1)} fusion(bf16[1024,2048]{1,0:T(8,128)(2,1)S(1)} %copy-done.3, bf16[2048,1024]{1,0:T(8,128)(2,1)S(1)} %copy-done.22), kind=kOutput, calls=%fused_computation.9 | convolution fusion | flops 4296015872 | bytes 10485760 | tf_op jit(solution)/shard_map/dot_general | solution.py:512
  29.8 1.4 copy-done.5
  31.8 5.2 %collective-permute-start.2 = (bf16[16,1536]{1,0:T(8,128)(2,1)}, bf16[16,1536]{1,0:T(8,128)(2,1)}, u32[]{:S(2)}, u32[]{:S(2)}) collective-permute-start(bf16[16,1536]{1,0:T(8,128)(2,1)} %get-tuple-element.25), channel_id=1, source_target_pairs={{0,4},{4,8},{8,12},{12,16},{16,20},{20,24},{24,28},{1,5},{5,9},{9,... | collective-permute-start | bytes 147464 | tf_op jit(solution)/shard_map/ppermute | solution.py:27
  37.0 1.5 collective-permute-start.3
  39.2 1.9 copy.42
  41.1 4.2 %convolution_convert_fusion.7 = bf16[1024,32]{0,1:T(8,128)(2,1)} fusion(bf16[1024,2048]{1,0:T(8,128)(2,1)} %copy-done.2, bf16[2048,32]{0,1:T(8,128)(2,1)} %bitcast.48), kind=kOutput, calls=%fused_computation.16 | convolution fusion | flops 134250496 | bytes 4390912 | tf_op jit(solution)/shard_map/dot_general | solution.py:512
  45.2 1.7 copy.41
  46.9 5.6 %convolution_convert_fusion.2 = bf16[1024,512]{1,0:T(8,128)(2,1)} fusion(bf16[1024,2048]{1,0:T(8,128)(2,1)} %copy-done.2, bf16[2048,512]{1,0:T(8,128)(2,1)S(1)} %copy-done), kind=kOutput, calls=%fused_computation.11 | convolution fusion | flops 2148007936 | bytes 7340032 | tf_op jit(solution)/shard_map/dot_general | solution.py:512
  52.6 5.7 %convolution_convert_fusion.gate_ref = bf16[1024,1024]{1,0:T(8,128)(2,1)} fusion(bf16[1024,2048]{1,0:T(8,128)(2,1)S(1)} %copy-done.4, bf16[2048,1024]{1,0:T(8,128)(2,1)S(1)} %copy-done.23), kind=kOutput, calls=%fused_computation.8 | convolution fusion | flops 4296015872 | bytes 10485760 | tf_op jit(solution)/shard_map/dot_general | solution.py:512
  58.6 2.3 %slice_bitcast_fusion = (f32[16,1024]{0,1:T(8,128)}, f32[1024,16]{1,0:T(8,128)}, f32[1024,16]{1,0:T(8,128)}, f32[16,1024]{0,1:T(8,128)}, f32[1024,16]{1,0:T(8,12...) fusion(f32[1024,32]{1,0:T(8,128)S(1)} %get-tuple-element.41, ...), kind=kLoop, calls=%fused_computation.59 | loop fusion | flops 32736 | bytes 786560 | tf_op jit(solution)/shard_map/transpose | solution.py:452
  61.6 1.5 copy.37
  63.4 4.1 %pad_maximum_fusion.rows_ref = bf16[1056,1536]{1,0:T(8,128)(2,1)} fusion(bf16[16,1536]{1,0:T(8,128)(2,1)} %collective-permute-done.3, bf16[1024,256]{1,0:T(8,128)(2,1)S(1)} %convolution_convert_fusion.3, bf16[1024,256]{1,0:T(8,128)(2,1)S(1)} %convolution_convert_fusion.4, bf16[1024,1024]{1,0:T(8,128)(2,1)} %copy-done.5, ...), kind=kLoop, calls=%fused_computation.5 | loop fusion | flops 16220160 | bytes 6488064 | tf_op jit(solution)/shard_map/concatenate | solution.py:31
  67.5 17.9 %chunk_states.1 = (bf16[1024,1536]{1,0:T(8,128)(2,1)}, f32[8,128,1024]{2,1,0:T(8,128)}, f32[8,128,1024]{2,1,0:T(8,128)}, f32[128,1024]{1,0:T(8,128)}, f32[128,1024]{1,0:T(8,128)}) custom-call(bf16[1056,1536]{1,0:T(8,128)(2,1)} %pad_maximum_fusion.rows_ref, f32[5,1536]{1,0:T(8,128)} %maximum_convert_fusion.taps_ref, f32[1024,16]{1,0:T(8,128)} %get-tuple-element.51.ldf_ref, ...), custom_call_target="tpu_custom_call" | custom-call | flops 1073741824 | bytes 16777216 | tf_op jit(solution)/shard_map/chunk_states/pallas_call | solution.py:395
  85.4 1.1 convert.33
  86.4 1.1 convert.35
  87.6 1.3 collective-permute-start.8
  88.9 5.3 %collective-permute-start.4 = (bf16[144,1024]{1,0:T(8,128)(2,1)S(1)}, bf16[144,1024]{1,0:T(8,128)(2,1)S(1)}, u32[]{:S(2)}, u32[]{:S(2)}) collective-permute-start(bf16[144,1024]{1,0:T(8,128)(2,1)S(1)} %pad_maximum_fusion.3), channel_id=1, source_target_pairs={{0,4},{4,8},{8,12},{12,16},{16,20},{20,24},{24,28},{1,5},{5,9},{9,... | collective-permute-start | bytes 884744 | tf_op jit(solution)/shard_map/ppermute | solution.py:465
  94.6 3.4 %collective-permute-done.8 = bf16[144,1024]{1,0:T(8,128)(2,1)S(1)} collective-permute-done((bf16[144,1024]{1,0:T(8,128)(2,1)S(1)}, bf16[144,1024]{1,0:T(8,128)(2,1)S(1)}, u32[]{:S(2)}, u32[]{:S(2)}) %collective-permute-start.8) | collective-permute-done | bytes 294944 | tf_op jit(solution)/shard_map/ppermute | solution.py:465
  98.0 1.3 collective-permute-start.9
  99.3 5.2 %collective-permute-done.4 = bf16[144,1024]{1,0:T(8,128)(2,1)S(1)} collective-permute-done((bf16[144,1024]{1,0:T(8,128)(2,1)S(1)}, bf16[144,1024]{1,0:T(8,128)(2,1)S(1)}, u32[]{:S(2)}, u32[]{:S(2)}) %collective-permute-start.4) | collective-permute-done | bytes 294944 | tf_op jit(solution)/shard_map/ppermute | solution.py:465
  104.5 4.4 %collective-permute-start.5 = (bf16[144,1024]{1,0:T(8,128)(2,1)S(1)}, bf16[144,1024]{1,0:T(8,128)(2,1)S(1)}, u32[]{:S(2)}, u32[]{:S(2)}) collective-permute-start(bf16[144,1024]{1,0:T(8,128)(2,1)S(1)} %collective-permute-done.4), channel_id=1, source_target_pairs={{0,4},{4,8},{8,12},{12,16},{16,20},{20,24},{24,28},{1,5},{5,9},{9,... | collective-permute-start | bytes 884744 | tf_op jit(solution)/shard_map/ppermute | solution.py:465
  109.4 9.6 %collective-permute-done.5 = bf16[144,1024]{1,0:T(8,128)(2,1)S(1)} collective-permute-done((bf16[144,1024]{1,0:T(8,128)(2,1)S(1)}, bf16[144,1024]{1,0:T(8,128)(2,1)S(1)}, u32[]{:S(2)}, u32[]{:S(2)}) %collective-permute-start.5) | collective-permute-done | bytes 294944 | tf_op jit(solution)/shard_map/ppermute | solution.py:465
  119.0 1.2 fusion.10
  120.2 1.3 collective-permute-start.10
  121.5 6.2 %collective-permute-start.6 = (bf16[144,1024]{1,0:T(8,128)(2,1)}, bf16[144,1024]{1,0:T(8,128)(2,1)}, u32[]{:S(2)}, u32[]{:S(2)}) collective-permute-start(bf16[144,1024]{1,0:T(8,128)(2,1)} %get-tuple-element.49), channel_id=1, source_target_pairs={{0,8},{4,12},{8,16},{12,20},{16,24},{20,28},{1,9},{5,13},{9,17},{1... | collective-permute-start | bytes 884744 | tf_op jit(solution)/shard_map/ppermute | solution.py:465
  128.7 1.3 copy.40.query_ref
  130.0 1.8 copy.46.stbt_ref
  131.8 1.8 copy.45.stft_ref
  133.6 1.8 copy.44.ldbt_ref
  135.5 0.8 copy.43.ldft_ref
  136.9 1.3 fusion.9
  138.2 1.3 collective-permute-start.11
  139.5 5.7 %collective-permute-start.7 = (bf16[144,1024]{1,0:T(8,128)(2,1)S(1)}, bf16[144,1024]{1,0:T(8,128)(2,1)S(1)}, u32[]{:S(2)}, u32[]{:S(2)}) collective-permute-start(bf16[144,1024]{1,0:T(8,128)(2,1)S(1)} %get-tuple-element.47), channel_id=1, source_target_pairs={{0,16},{4,20},{8,24},{12,28},{1,17},{5,21},{9,25},{13,29},{2,18},{... | collective-permute-start | bytes 884744 | tf_op jit(solution)/shard_map/ppermute | solution.py:465
  145.3 1.8 pad_maximum_fusion.2.rim_ref
  147.1 26.0 %attend.1.attn_ref = bf16[1024,512]{1,0:T(8,128)(2,1)} custom-call(s32[2]{0:T(128)} %pad_add_fusion.place_ref, f32[8]{0:T(128)} %sink_ref.1, bf16[1024,512]{1,0:T(8,128)(2,1)} %copy.40.query_ref, bf16[1280,256]{1,0:T(8,128)(2,1)} %pad_maximum_fusion.2.rim_ref), custom_call_target="tpu_custom_call" | custom-call | flops 805306368 | bytes 2097152 | tf_op jit(solution)/shard_map/attend/pallas_call | solution.py:248
  173.1 1.2 fusion.7
  174.3 17.9 %chunk_outputs.1.ssm_ref = bf16[1024,1024]{1,0:T(8,128)(2,1)} custom-call(bf16[1024,1536]{1,0:T(8,128)(2,1)} %get-tuple-element.10.act_ref, f32[1024,16]{1,0:T(8,128)} %get-tuple-element.51.ldf_ref, f32[1024,16]{1,0:T(8,128)} %get-tuple-element.52.ldb_ref.ldball_ref, f32[1024,16]{1,0:T(8,128)} %get-tuple-element.37.stf_ref, ...), custom_call_target="tpu_custom_call" | custom-call | flops 1073741824 | bytes 16777216 | tf_op jit(solution)/shard_map/chunk_outputs/pallas_call | solution.py:426
  192.2 32.8 %combine.1 = bf16[256,2048]{1,0:T(8,128)(2,1)} custom-call(bf16[1024,512]{1,0:T(8,128)(2,1)} %attend.1.attn_ref, bf16[1024,1024]{1,0:T(8,128)(2,1)} %chunk_outputs.1.ssm_ref, bf16[512,2048]{1,0:T(8,128)(2,1)} %attn_w_ref.1, bf16[1024,2048]{1,0:T(8,128)(2,1)} %ssm_w_ref.1), custom_call_target="tpu_custom_call" | custom-call | flops 6442450944 | bytes 6291456 | tf_op jit(solution)/shard_map/combine/pallas_call | solution.py:362
  225.0 2.3 %copy.49 = bf16[256,2048]{1,0:T(8,128)(2,1)} copy(bf16[256,2048]{1,0:T(8,128)(2,1)} %combine.1) | data formatting | bytes 2097152
  (103 shorter events, 8.1 us)
Async XLA Ops:
  0.0 46.9 %copy-start = (bf16[2048,512]{1,0:T(8,128)(2,1)S(1)}, bf16[2048,512]{1,0:T(8,128)(2,1)}, u32[]{:S(2)}) copy-start(bf16[2048,512]{1,0:T(8,128)(2,1)} %param.22) | copy-start | bytes 6291460
  0.0 3.3 %copy-start.16 = (bf16[2048]{0:T(1024)(128)(2,1)S(1)}, bf16[2048]{0:T(1024)(128)(2,1)}, u32[]{:S(2)}) copy-start(bf16[2048]{0:T(1024)(128)(2,1)} %param.21) | copy-start | bytes 12292
  3.3 3.3 %copy-start.25 = (bf16[2048,128]{1,0:T(8,128)(2,1)S(1)}, bf16[2048,128]{1,0:T(8,128)(2,1)}, u32[]{:S(2)}) copy-start(bf16[2048,128]{1,0:T(8,128)(2,1)} %param.24) | copy-start | bytes 1572868
  6.6 2.0 copy-start.2
  6.6 2.0 copy-start.26
  8.5 2.9 %copy-start.10 = (bf16[1024,128]{1,0:T(8,128)(2,1)}, bf16[1024,128]{1,0:T(8,128)(2,1)S(1)}, u32[]{:S(2)}) copy-start(bf16[1024,128]{1,0:T(8,128)(2,1)S(1)} %convolution_convert_fusion.5) | copy-start | bytes 786436
  8.5 2.0 copy-start.19
  10.6 0.7 copy-start.8
  11.4 11.5 %copy-start.3 = (bf16[1024,2048]{1,0:T(8,128)(2,1)S(1)}, bf16[1024,2048]{1,0:T(8,128)(2,1)}, u32[]{:S(2)}) copy-start(bf16[1024,2048]{1,0:T(8,128)(2,1)} %copy-done.2) | copy-start | bytes 12582916
  11.4 11.5 %copy-start.24 = (bf16[2048,256]{1,0:T(8,128)(2,1)S(1)}, bf16[2048,256]{1,0:T(8,128)(2,1)}, u32[]{:S(2)}) copy-start(bf16[2048,256]{1,0:T(8,128)(2,1)} %param.30) | copy-start | bytes 3145732
  12.1 133.1 %collective-permute-start = (bf16[128,256]{1,0:T(8,128)(2,1)}, bf16[128,256]{1,0:T(8,128)(2,1)}, u32[]{:S(2)}, u32[]{:S(2)}) collective-permute-start(bf16[128,256]{1,0:T(8,128)(2,1)} %get-tuple-element.39), channel_id=1, source_target_pairs={{0,4},{4,8},{8,12},{12,16},{16,20},{20,24},{24,28},{1,5},{5,9},{9,... | collective-permute-start | bytes 196616 | tf_op jit(solution)/shard_map/ppermute | solution.py:27
  17.9 127.4 %collective-permute-start.1 = (bf16[128,256]{1,0:T(8,128)(2,1)}, bf16[128,256]{1,0:T(8,128)(2,1)}, u32[]{:S(2)}, u32[]{:S(2)}) collective-permute-start(bf16[128,256]{1,0:T(8,128)(2,1)} %get-tuple-element.40), channel_id=1, source_target_pairs={{4,0},{8,4},{12,8},{16,12},{20,16},{24,20},{28,24},{5,1},{9,5},{13... | collective-permute-start | bytes 196616 | tf_op jit(solution)/shard_map/ppermute | solution.py:30
  22.9 2.2 copy-start.22
  25.1 13.3 %copy-start.18 = (f32[2,16]{1,0:T(2,128)S(1)}, f32[2,16]{1,0:T(2,128)}, u32[]{:S(2)}) copy-start(f32[2,16]{1,0:T(2,128)} %param.35) | copy-start | bytes 388
  25.1 14.0 %copy-start.14 = (bf16[5,2,256]{2,1,0:T(2,128)(2,1)S(1)}, bf16[5,2,256]{2,1,0:T(2,128)(2,1)}, u32[]{:S(2)}) copy-start(bf16[5,2,256]{2,1,0:T(2,128)(2,1)} %param.34) | copy-start | bytes 15364
  29.8 1.4 copy-start.5
  31.8 31.6 %collective-permute-start.2 = (bf16[16,1536]{1,0:T(8,128)(2,1)}, bf16[16,1536]{1,0:T(8,128)(2,1)}, u32[]{:S(2)}, u32[]{:S(2)}) collective-permute-start(bf16[16,1536]{1,0:T(8,128)(2,1)} %get-tuple-element.25), channel_id=1, source_target_pairs={{0,4},{4,8},{8,12},{12,16},{16,20},{20,24},{24,28},{1,5},{5,9},{9,... | collective-permute-start | bytes 147464 | tf_op jit(solution)/shard_map/ppermute | solution.py:27
  37.0 26.4 %collective-permute-start.3 = (bf16[16,1536]{1,0:T(8,128)(2,1)}, bf16[16,1536]{1,0:T(8,128)(2,1)}, u32[]{:S(2)}, u32[]{:S(2)}) collective-permute-start(bf16[16,1536]{1,0:T(8,128)(2,1)} %get-tuple-element.26), channel_id=1, source_target_pairs={{4,0},{8,4},{12,8},{16,12},{20,16},{24,20},{28,24},{5,1},{9,5},{13... | collective-permute-start | bytes 147464 | tf_op jit(solution)/shard_map/ppermute | solution.py:30
  46.9 5.6 %copy-start.4 = (bf16[1024,2048]{1,0:T(8,128)(2,1)S(1)}, bf16[1024,2048]{1,0:T(8,128)(2,1)}, u32[]{:S(2)}) copy-start(bf16[1024,2048]{1,0:T(8,128)(2,1)} %copy-done.2) | copy-start | bytes 12582916
  46.9 5.6 %copy-start.23 = (bf16[2048,1024]{1,0:T(8,128)(2,1)S(1)}, bf16[2048,1024]{1,0:T(8,128)(2,1)}, u32[]{:S(2)}) copy-start(bf16[2048,1024]{1,0:T(8,128)(2,1)} %param.28) | copy-start | bytes 12582916
  52.5 5.7 %copy-start.6 = (f32[1024,32]{1,0:T(8,128)S(1)}, f32[1024,32]{1,0:T(8,128)}, u32[]{:S(2)}) copy-start(f32[1024,32]{1,0:T(8,128)} %copy.42) | copy-start | bytes 393220
  52.5 5.7 %copy-start.12 = (bf16[1024,32]{1,0:T(8,128)(2,1)S(1)}, bf16[1024,32]{1,0:T(8,128)(2,1)}, u32[]{:S(2)}) copy-start(bf16[1024,32]{1,0:T(8,128)(2,1)} %copy.41) | copy-start | bytes 196612
  52.6 5.7 %copy-start.21 = (f32[32]{0:T(128)S(1)}, f32[32]{0:T(128)}, u32[]{:S(2)}) copy-start(f32[32]{0:T(128)} %neg.25) | copy-start | bytes 388
  58.3 2.6 %copy-start.13 = (bf16[5,1024]{1,0:T(8,128)(2,1)S(1)}, bf16[5,1024]{1,0:T(8,128)(2,1)}, u32[]{:S(2)}) copy-start(bf16[5,1024]{1,0:T(8,128)(2,1)} %param.33) | copy-start | bytes 30724
  67.5 41.4 %copy-start.20 = (f32[64]{0:T(128)S(1)}, f32[64]{0:T(128)}, u32[]{:S(2)}) copy-start(f32[64]{0:T(128)} %param.25) | copy-start | bytes 772
  86.4 32.5 %copy-start.15 = (pred[144]{0:T(512)(128)(4,1)S(1)}, pred[144]{0:T(512)(128)(4,1)}, u32[]{:S(2)}) copy-start(pred[144]{0:T(512)(128)(4,1)} %constant.39.clone.1) | copy-start | bytes 436
  87.6 10.4 %collective-permute-start.8 = (bf16[144,1024]{1,0:T(8,128)(2,1)S(1)}, bf16[144,1024]{1,0:T(8,128)(2,1)S(1)}, u32[]{:S(2)}, u32[]{:S(2)}) collective-permute-start(bf16[144,1024]{1,0:T(8,128)(2,1)S(1)} %pad_maximum_fusion.4), channel_id=1, source_target_pairs={{4,0},{8,4},{12,8},{16,12},{20,16},{24,20},{28,24},{5,1},{9,5},{13... | collective-permute-start | bytes 884744 | tf_op jit(solution)/shard_map/ppermute | solution.py:465
  88.9 38.7 %copy-start.9 = (f32[1024,32]{0,1:T(8,128)S(1)}, f32[1024,32]{0,1:T(8,128)}, u32[]{:S(2)}) copy-start(f32[1024,32]{0,1:T(8,128)} %copy-done.8) | copy-start | bytes 393220
  88.9 15.5 %collective-permute-start.4 = (bf16[144,1024]{1,0:T(8,128)(2,1)S(1)}, bf16[144,1024]{1,0:T(8,128)(2,1)S(1)}, u32[]{:S(2)}, u32[]{:S(2)}) collective-permute-start(bf16[144,1024]{1,0:T(8,128)(2,1)S(1)} %pad_maximum_fusion.3), channel_id=1, source_target_pairs={{0,4},{4,8},{8,12},{12,16},{16,20},{20,24},{24,28},{1,5},{5,9},{9,... | collective-permute-start | bytes 884744 | tf_op jit(solution)/shard_map/ppermute | solution.py:465
  98.0 11.4 %collective-permute-start.9 = (bf16[144,1024]{1,0:T(8,128)(2,1)S(1)}, bf16[144,1024]{1,0:T(8,128)(2,1)S(1)}, u32[]{:S(2)}, u32[]{:S(2)}) collective-permute-start(bf16[144,1024]{1,0:T(8,128)(2,1)S(1)} %collective-permute-done.8), channel_id=1, source_target_pairs={{4,0},{8,4},{12,8},{16,12},{20,16},{24,20},{28,24},{5,1},{9,5},{13... | collective-permute-start | bytes 884744 | tf_op jit(solution)/shard_map/ppermute | solution.py:465
  104.5 14.5 %collective-permute-start.5 = (bf16[144,1024]{1,0:T(8,128)(2,1)S(1)}, bf16[144,1024]{1,0:T(8,128)(2,1)S(1)}, u32[]{:S(2)}, u32[]{:S(2)}) collective-permute-start(bf16[144,1024]{1,0:T(8,128)(2,1)S(1)} %collective-permute-done.4), channel_id=1, source_target_pairs={{0,4},{4,8},{8,12},{12,16},{16,20},{20,24},{24,28},{1,5},{5,9},{9,... | collective-permute-start | bytes 884744 | tf_op jit(solution)/shard_map/ppermute | solution.py:465
  109.3 18.6 %copy-start.17 = (bf16[1024]{0:T(1024)(128)(2,1)S(1)}, bf16[1024]{0:T(1024)(128)(2,1)}, u32[]{:S(2)}) copy-start(bf16[1024]{0:T(1024)(128)(2,1)} %param.37) | copy-start | bytes 6148
  120.2 16.7 %collective-permute-start.10 = (bf16[144,1024]{1,0:T(8,128)(2,1)}, bf16[144,1024]{1,0:T(8,128)(2,1)}, u32[]{:S(2)}, u32[]{:S(2)}) collective-permute-start(bf16[144,1024]{1,0:T(8,128)(2,1)} %get-tuple-element.19), channel_id=1, source_target_pairs={{8,0},{12,4},{16,8},{20,12},{24,16},{28,20},{9,1},{13,5},{17,9},{2... | collective-permute-start | bytes 884744 | tf_op jit(solution)/shard_map/ppermute | solution.py:465
  121.5 14.0 %copy-start.7 = (f32[16,1024]{0,1:T(8,128)S(1)}, f32[16,1024]{0,1:T(8,128)}, u32[]{:S(2)}) copy-start(f32[16,1024]{0,1:T(8,128)} %get-tuple-element.54) | copy-start | bytes 196612
  121.5 15.4 %collective-permute-start.6 = (bf16[144,1024]{1,0:T(8,128)(2,1)}, bf16[144,1024]{1,0:T(8,128)(2,1)}, u32[]{:S(2)}, u32[]{:S(2)}) collective-permute-start(bf16[144,1024]{1,0:T(8,128)(2,1)} %get-tuple-element.49), channel_id=1, source_target_pairs={{0,8},{4,12},{8,16},{12,20},{16,24},{20,28},{1,9},{5,13},{9,17},{1... | collective-permute-start | bytes 884744 | tf_op jit(solution)/shard_map/ppermute | solution.py:465
  128.6 16.6 %copy-start.11 = (bf16[1024,128]{1,0:T(8,128)(2,1)S(1)}, bf16[1024,128]{1,0:T(8,128)(2,1)}, u32[]{:S(2)}) copy-start(bf16[1024,128]{1,0:T(8,128)(2,1)} %copy-done.10) | copy-start | bytes 786436
  138.2 34.9 %collective-permute-start.11 = (bf16[144,1024]{1,0:T(8,128)(2,1)S(1)}, bf16[144,1024]{1,0:T(8,128)(2,1)S(1)}, u32[]{:S(2)}, u32[]{:S(2)}) collective-permute-start(bf16[144,1024]{1,0:T(8,128)(2,1)S(1)} %get-tuple-element.17), channel_id=1, source_target_pairs={{16,0},{20,4},{24,8},{28,12},{17,1},{21,5},{25,9},{29,13},{18,2},{... | collective-permute-start | bytes 884744 | tf_op jit(solution)/shard_map/ppermute | solution.py:465
  139.5 33.6 %collective-permute-start.7 = (bf16[144,1024]{1,0:T(8,128)(2,1)S(1)}, bf16[144,1024]{1,0:T(8,128)(2,1)S(1)}, u32[]{:S(2)}, u32[]{:S(2)}) collective-permute-start(bf16[144,1024]{1,0:T(8,128)(2,1)S(1)} %get-tuple-element.47), channel_id=1, source_target_pairs={{0,16},{4,20},{8,24},{12,28},{1,17},{5,21},{9,25},{13,29},{2,18},{... | collective-permute-start | bytes 884744 | tf_op jit(solution)/shard_map/ppermute | solution.py:465
  192.2 35.1 %copy-start.1 = (bf16[2048,512]{1,0:T(8,128)(2,1)S(1)}, bf16[2048,512]{1,0:T(8,128)(2,1)}, u32[]{:S(2)}) copy-start(bf16[2048,512]{1,0:T(8,128)(2,1)} %param.22) | copy-start | bytes 6291460

commit v2 on v1

--- a/solution.py
+++ b/solution.py
@@ -16,6 +16,7 @@
 ROPE_BASE = 500000.0
 NEG_FILL = -1e30
 PIECE = 256
+PACK_ROWS = 16
 MESH = pl.DeviceIdType.MESH
 
 
@@ -77,7 +78,7 @@
 
 def states_kernel(
     tap_count, inner, maps, rows_ref, taps_ref, ldf_ref, ldb_ref, stf_ref, stb_ref,
-    act_ref, freshf_ref, freshb_ref, endf_ref, endb_ref, spare, reach,
+    act_ref, freshf_ref, freshb_ref, packf_ref, packb_ref, spare, reach, endf_ref, endb_ref, logs,
 ):
     step = pl.program_id(0)
     size = act_ref.shape[0]
@@ -105,6 +106,7 @@
         endf_ref[...] = jnp.zeros_like(endf_ref)
         endb_ref[...] = jnp.zeros_like(endb_ref)
         reach[...] = jnp.ones_like(reach)
+        logs[...] = jnp.zeros_like(logs)
 
     groups = maps // STATE_SIZE
     width = inner // groups
@@ -119,11 +121,23 @@
         endf_ref[:, cols] = endf_ref[:, cols] * totf[:, cols] + ff
         endb_ref[:, cols] = endb_ref[:, cols] + reach[0:1, cols] * fb
     reach[...] = reach[...] * totb
+    logs[0] = logs[0] + cumf[size - 1 : size]
+    logs[1] = logs[1] + cumb[0:1]
+
+    @pl.when(step == pl.num_programs(0) - 1)
+    def _():
+        half = inner // 2
+        for d, (end_ref, pack_ref) in enumerate(((endf_ref, packf_ref), (endb_ref, packb_ref))):
+            decay = spread(jnp.exp(logs[d]), inner).astype(jnp.bfloat16)
+            for side in range(2):
+                cols = slice(side * half, (side + 1) * half)
+                pack_ref[side, :STATE_SIZE, :] = end_ref[:, cols].astype(jnp.bfloat16)
+                pack_ref[side, STATE_SIZE:, :] = jnp.concatenate([decay, decay], axis=0)[:, cols]
 
 
 def outputs_kernel(
     head_size, inner, maps, act_ref, ldf_ref, ldb_ref, stf_ref, stb_ref, ldft_ref, ldbt_ref,
-    stft_ref, stbt_ref, ldball_ref, freshf_ref, freshb_ref, inf_ref, inb_ref, gate_ref, gain_ref,
+    stft_ref, stbt_ref, ldball_ref, freshf_ref, freshb_ref, enter_ref, gate_ref, gain_ref,
     out_ref, carryf, enterb, y,
 ):
     step = pl.program_id(0)
@@ -133,8 +147,10 @@
 
     @pl.when(step == 0)
     def _():
-        carryf[...] = inf_ref[...]
-        enterb[chunks - 1] = inb_ref[...]
+        half = inner // 2
+        for side in range(2):
+            carryf[:, side * half : (side + 1) * half] = enter_ref[0, side]
+            enterb[chunks - 1, :, side * half : (side + 1) * half] = enter_ref[1, side]
 
         @pl.loop(0, chunks - 1)
         def _(k):
@@ -204,64 +220,195 @@
     carryf[...] = carryf[...] * totf + freshf_ref[0]
 
 
-def attend_kernel(head_size, key_heads, place_ref, sink_ref, query_ref, rim_ref, out_ref):
-    step = pl.program_id(0)
-    size = query_ref.shape[0]
-    reach = size + 2 * WINDOW
+def middle_kernel(
+    head_size, key_heads, count, sink_ref, query_ref, rim_ref, packf_ref, packb_ref, out_ref,
+    enter_ref, scores, raised, bottoms, flipped, turned, bias, mate_in, pair_out, pair_in, gathered,
+    reach, back_out, back_in, mate_send, mate_recv, pair_send, pair_recv, back_send, back_recv,
+):
+    me = lax.axis_index("sp")
+    parity = lax.rem(me, 2)
+    place = lax.div(me, 2)
+    pairs = count // 2
+    mate = me + 1 - 2 * parity
+    is_even = parity == 0
+    packs = (packf_ref, packb_ref)
+    states = STATE_SIZE
+
+    def copy(source, target, sends, receives, device):
+        return pltpu.make_async_remote_copy(
+            src_ref=source, dst_ref=target, send_sem=sends, recv_sem=receives,
+            device_id={"sp": device}, device_id_type=MESH,
+        )
+
+    def to_mate(d):
+        return copy(
+            packs[d].at[1 - parity], mate_in.at[d], mate_send.at[d], mate_recv.at[d], mate
+        )
+
+    def to_pair(d, k):
+        device = me + 2 * k if d == 0 else me - 2 * k
+        return copy(
+            pair_out.at[d], pair_in.at[d, k - 1], pair_send.at[d, k - 1], pair_recv.at[d, k - 1],
+            device,
+        )
+
+    def back_to_mate(d):
+        return copy(back_out.at[d], back_in.at[d], back_send.at[d], back_recv.at[d], mate)
+
+    def sends_to(d, k):
+        return place + k < pairs if d == 0 else place - k >= 0
+
+    def hears_from(d, k):
+        return place - k >= 0 if d == 0 else place + k < pairs
+
+    barrier = pltpu.get_barrier_semaphore()
+    pl.semaphore_signal(barrier, inc=1, device_id={"sp": mate}, device_id_type=MESH)
+    for k in range(1, pairs):
+        other = lax.rem(me + 2 * k, count)
+        pl.semaphore_signal(barrier, inc=1, device_id={"sp": other}, device_id_type=MESH)
+    pl.semaphore_wait(barrier, pairs)
+    for d in range(2):
+        to_mate(d).start()
+
+    def even_and_odd(d):
+        own, other = packs[d][parity].astype(jnp.float32), mate_in[d].astype(jnp.float32)
+        return jnp.where(is_even, own, other), jnp.where(is_even, other, own)
+
+    def join_pair():
+        for d in range(2):
+            to_mate(d).wait_recv()
+            even, odd = even_and_odd(d)
+            near, far = (odd, even) if d == 0 else (even, odd)
+            decay = near[states : states + 1]
+            pair_out[d, :states, :] = (near[:states] + decay * far[:states]).astype(jnp.bfloat16)
+            pair_out[d, states:, :] = (near[states:] * far[states:]).astype(jnp.bfloat16)
+        for k in range(1, pairs):
+            for d in range(2):
+                @pl.when(sends_to(d, k))
+                def _(d=d, k=k):
+                    to_pair(d, k).start()
+
+    def join_all():
+        gathered[...] = jnp.zeros_like(gathered)
+        reach[...] = jnp.ones_like(reach)
+        for k in range(1, pairs):
+            for d in range(2):
+                @pl.when(hears_from(d, k))
+                def _(d=d, k=k):
+                    to_pair(d, k).wait_recv()
+                    came = pair_in[d, k - 1].astype(jnp.float32)
+                    gathered[d] = gathered[d] + reach[d, 0:1] * came[:states]
+                    reach[d] = reach[d] * came[states : states + 8]
+        for d in range(2):
+            even, odd = even_and_odd(d)
+            base = even if d == 0 else odd
+            plain = gathered[d]
+            moved = base[:states] + base[states : states + 1] * plain
+            plain_is_mine = is_even if d == 0 else jnp.logical_not(is_even)
+            enter_ref[d, parity] = jnp.where(plain_is_mine, plain, moved)
+            back_out[d] = jnp.where(plain_is_mine, moved, plain).astype(jnp.bfloat16)
+            back_to_mate(d).start()
+
+    rows, block = query_ref.shape[0], WINDOW
+    span = block + 2 * WINDOW
+    blocks = rows // block
     heads = query_ref.shape[1] // head_size
     ratio = heads // key_heads
-    start = pl.multiple_of(step * size, size)
-    row = lax.broadcasted_iota(jnp.int32, (size, reach), 0)
-    column = lax.broadcasted_iota(jnp.int32, (size, reach), 1)
-    key_pos = place_ref[0] + step * size - WINDOW + column
-    allowed = (
-        (column >= row) & (column <= row + 2 * WINDOW) & (key_pos >= 0) & (key_pos < place_ref[1])
-    )
+    values_at = key_heads * head_size
+    flipped[...] = jnp.transpose(rim_ref[:, values_at:])
     scale = head_size ** (-0.5)
-    for k in range(key_heads):
-        keys = rim_ref[pl.ds(start, reach), k * head_size : (k + 1) * head_size]
-        values = rim_ref[
-            pl.ds(start, reach), (key_heads + k) * head_size : (key_heads + k + 1) * head_size
-        ]
-        for r in range(ratio):
-            h = k * ratio + r
-            cols = slice(h * head_size, (h + 1) * head_size)
-            scores = lax.dot_general(
-                query_ref[:, cols], keys, (((1,), (1,)), ((), ())),
+    key_row = lax.broadcasted_iota(jnp.int32, (span, block), 0)
+    query_col = lax.broadcasted_iota(jnp.int32, (span, block), 1)
+    in_band = (key_row >= query_col) & (key_row <= query_col + 2 * WINDOW)
+
+    @pl.loop(0, blocks)
+    def _(step):
+        @pl.when(step == (3 * blocks) // 8)
+        def _():
+            join_pair()
+
+        @pl.when(step == (7 * blocks) // 8)
+        def _():
+            join_all()
+
+        start = pl.multiple_of(step * block, block)
+        position = me * rows + start - WINDOW + key_row
+        bias[...] = jnp.where(
+            in_band & (position >= 0) & (position < count * rows), 0.0, NEG_FILL
+        )
+        tops = []
+        for h in range(heads):
+            k = h // ratio
+            scores[h] = lax.dot_general(
+                rim_ref[pl.ds(start, span), k * head_size : (k + 1) * head_size],
+                query_ref[pl.ds(start, block), h * head_size : (h + 1) * head_size],
+                (((1,), (1,)), ((), ())), preferred_element_type=jnp.float32,
+            ) * scale + bias[...]
+        for h in range(heads):
+            top = jnp.maximum(jnp.max(scores[h], axis=0, keepdims=True), sink_ref[h])
+            lifted = jnp.exp(scores[h] - top)
+            bottoms[h : h + 1] = jnp.sum(lifted, axis=0, keepdims=True) + jnp.exp(sink_ref[h] - top)
+            raised[h] = lifted.astype(jnp.bfloat16)
+        for h in range(heads):
+            k = h // ratio
+            turned[h * head_size : (h + 1) * head_size, :] = jnp.dot(
+                flipped[k * head_size : (k + 1) * head_size, pl.ds(start, span)], raised[h],
                 preferred_element_type=jnp.float32,
-            )
-            scores = jnp.where(allowed, scores * scale, NEG_FILL)
-            sink = sink_ref[h]
-            ceiling = jnp.maximum(jnp.max(scores, axis=1, keepdims=True), sink)
-            raised = jnp.exp(scores - ceiling)
-            bottom = jnp.sum(raised, axis=1, keepdims=True) + jnp.exp(sink - ceiling)
-            weights = (raised * (1.0 / bottom)).astype(jnp.bfloat16)
-            out_ref[:, cols] = jnp.dot(
-                weights, values, preferred_element_type=jnp.float32
-            ).astype(jnp.bfloat16)
-
-
-def attend(query, rimmed, sink_logit, seq_first, seq_total, head_size, key_heads):
+            ) * (1.0 / bottoms[h : h + 1])
+        out_ref[pl.ds(start, block), :] = jnp.transpose(turned[...]).astype(jnp.bfloat16)
+
+    for d in range(2):
+        back_to_mate(d).wait_recv()
+        enter_ref[d, 1 - parity] = back_in[d].astype(jnp.float32)
+    for d in range(2):
+        to_mate(d).wait_send()
+        back_to_mate(d).wait_send()
+        for k in range(1, pairs):
+            @pl.when(sends_to(d, k))
+            def _(d=d, k=k):
+                to_pair(d, k).wait_send()
+
+
+def middle(query, rimmed, sink_logit, pack_forward, pack_backward, head_size, key_heads):
     rows, width = query.shape
-    block = WINDOW
-    place = jnp.stack([jnp.int32(seq_first), jnp.int32(seq_total)])
+    heads = width // head_size
+    count = lax.axis_size("sp")
+    hops = max(count // 2 - 1, 1)
+    _, depth, half = pack_forward.shape
+    span = 3 * WINDOW
+    vmem = pl.BlockSpec(memory_space=pltpu.VMEM)
+    dma = pltpu.SemaphoreType.DMA
     return pl.pallas_call(
-        functools.partial(attend_kernel, head_size, key_heads),
-        grid=(rows // block,),
-        in_specs=[
-            pl.BlockSpec(memory_space=pltpu.SMEM),
-            pl.BlockSpec(memory_space=pltpu.SMEM),
-            pl.BlockSpec((block, width), lambda i: (i, 0)),
-            pl.BlockSpec(rimmed.shape, lambda i: (0, 0)),
-        ],
-        out_specs=pl.BlockSpec((block, width), lambda i: (i, 0)),
-        out_shape=jax.ShapeDtypeStruct((rows, width), jnp.bfloat16),
+        functools.partial(middle_kernel, head_size, key_heads, count),
+        in_specs=[pl.BlockSpec(memory_space=pltpu.SMEM), vmem, vmem, vmem, vmem],
+        out_specs=[vmem, vmem],
+        out_shape=[
+            jax.ShapeDtypeStruct((rows, width), jnp.bfloat16),
+            jax.ShapeDtypeStruct((2, 2, STATE_SIZE, half), jnp.float32),
+        ],
+        scratch_shapes=[
+            pltpu.VMEM((heads, span, WINDOW), jnp.float32),
+            pltpu.VMEM((heads, span, WINDOW), jnp.bfloat16),
+            pltpu.VMEM((heads, WINDOW), jnp.float32),
+            pltpu.VMEM((key_heads * head_size, rimmed.shape[0]), jnp.bfloat16),
+            pltpu.VMEM((width, WINDOW), jnp.float32),
+            pltpu.VMEM((span, WINDOW), jnp.float32),
+            pltpu.VMEM((2, depth, half), jnp.bfloat16),
+            pltpu.VMEM((2, depth, half), jnp.bfloat16),
+            pltpu.VMEM((2, hops, depth, half), jnp.bfloat16),
+            pltpu.VMEM((2, STATE_SIZE, half), jnp.float32),
+            pltpu.VMEM((2, 8, half), jnp.float32),
+            pltpu.VMEM((2, STATE_SIZE, half), jnp.bfloat16),
+            pltpu.VMEM((2, STATE_SIZE, half), jnp.bfloat16),
+            dma((2,)), dma((2,)), dma((2, hops)), dma((2, hops)), dma((2,)), dma((2,)),
+        ],
+        compiler_params=pltpu.CompilerParams(collective_id=5, has_side_effects=True),
         cost_estimate=pl.CostEstimate(
-            flops=4 * rows * 3 * WINDOW * width, bytes_accessed=4 * rows * width,
-            transcendentals=rows * 3 * WINDOW * width // head_size,
+            flops=4 * rows * span * width, bytes_accessed=4 * rows * width,
+            transcendentals=rows * span * heads,
         ),
-        name="attend",
-    )(place, sink_logit, query, rimmed)
+        name="middle",
+    )(sink_logit, query, rimmed, pack_forward, pack_backward)
 
 
 def combine_kernel(
@@ -389,9 +536,10 @@
     total, heads, chunks = rimmed.shape[1], decay[0].shape[1], rows // CHUNK
     small = pl.BlockSpec((CHUNK, heads), lambda i: (i, 0))
     fresh = pl.BlockSpec((1, STATE_SIZE, inner), lambda i: (i, 0, 0))
-    end = pl.BlockSpec((STATE_SIZE, inner), lambda i: (0, 0))
+    packed = (2, STATE_SIZE + PACK_ROWS, inner // 2)
+    end = pl.BlockSpec(packed, lambda i: (0, 0, 0))
     fresh_shape = jax.ShapeDtypeStruct((chunks, STATE_SIZE, inner), jnp.float32)
-    end_shape = jax.ShapeDtypeStruct((STATE_SIZE, inner), jnp.float32)
+    end_shape = jax.ShapeDtypeStruct(packed, jnp.bfloat16)
     return pl.pallas_call(
         functools.partial(states_kernel, tap_count, inner, maps),
         grid=(chunks,),
@@ -408,6 +556,9 @@
         scratch_shapes=[
             pltpu.VMEM((CHUNK + 2 * HALO, total), jnp.float32),
             pltpu.VMEM((8, inner), jnp.float32),
+            pltpu.VMEM((STATE_SIZE, inner), jnp.float32),
+            pltpu.VMEM((STATE_SIZE, inner), jnp.float32),
+            pltpu.VMEM((2, 8, heads), jnp.float32),
         ],
         cost_estimate=pl.CostEstimate(
             flops=8 * rows * inner * STATE_SIZE, bytes_accessed=16 * rows * inner,
@@ -422,7 +573,6 @@
     heads, chunks = decay[0].shape[1], rows // CHUNK
     small = pl.BlockSpec((CHUNK, heads), lambda i: (i, 0))
     turned = pl.BlockSpec((heads, CHUNK), lambda i: (0, i))
-    whole = pl.BlockSpec((STATE_SIZE, inner), lambda i: (0, 0))
     return pl.pallas_call(
         functools.partial(outputs_kernel, head_size, inner, maps),
         grid=(chunks,),
@@ -432,7 +582,7 @@
             pl.BlockSpec((rows, heads), lambda i: (0, 0)),
             pl.BlockSpec((1, STATE_SIZE, inner), lambda i: (i, 0, 0)),
             pl.BlockSpec((chunks, STATE_SIZE, inner), lambda i: (0, 0, 0)),
-            whole, whole,
+            pl.BlockSpec(incoming.shape, lambda i: (0, 0, 0, 0)),
             pl.BlockSpec((CHUNK, inner), lambda i: (i, 0)),
             pl.BlockSpec((1, inner), lambda i: (0, 0)),
         ],
@@ -450,32 +600,8 @@
         name="chunk_outputs",
     )(
         act, *decay, *step, decay[0].T, decay[1].T, step[0].T, step[1].T, decay[1],
-        fresh[0], fresh[1], incoming[0], incoming[1], gate, gain,
+        fresh[0], fresh[1], incoming, gate, gain,
     )
-
-
-def entering_state(end, total, axis, head_size, reverse):
-    count = lax.axis_size(axis)
-    states = end.shape[0]
-
-    def moved(packet, distance):
-        pairs = [(i, i + distance) for i in range(count - distance)]
-        if reverse:
-            pairs = [(target, source) for source, target in pairs]
-        return lax.ppermute(packet, axis, pairs)
-
-    decay = jnp.broadcast_to(jnp.repeat(jnp.exp(total), head_size)[None, :], (16, end.shape[1]))
-    packet = jnp.concatenate([end, decay], axis=0).astype(jnp.bfloat16)
-    packet = moved(packet, 1)
-    distance = 1
-    held = packet.astype(jnp.float32)
-    while distance < count - 1:
-        arrived = moved(held.astype(jnp.bfloat16), distance).astype(jnp.float32)
-        factor = held[states : states + 1]
-        added = jnp.concatenate([held[:states], jnp.zeros_like(held[states:])], axis=0)
-        held = added + factor * arrived
-        distance *= 2
-    return held[:states]
 
 
 def local(
@@ -501,7 +627,6 @@
     ssm_out_weight,
 ):
     row_total = tokens.shape[0]
-    seq_total = row_total * lax.axis_size("sp")
     seq_first = lax.axis_index("sp") * row_total
     positions = seq_first + jnp.arange(row_total, dtype=jnp.int32)
     normed = rms_rows(tokens.astype(jnp.float32), norm_gain.astype(jnp.float32)).astype(
@@ -536,19 +661,17 @@
     heads_here = inner_width // head_size
     steps = (step[:, :heads_here], step[:, heads_here:])
     decays = (log_decay[:, :heads_here], log_decay[:, heads_here:])
-    act, fresh_forward, fresh_backward, end_forward, end_backward = chunk_states(
+    act, fresh_forward, fresh_backward, pack_forward, pack_backward = chunk_states(
         rimmed_rows, conv_table, tap_count, inner_width, map_width, decays, steps
     )
-    from_lower = entering_state(end_forward, jnp.sum(decays[0], axis=0), "sp", head_size, False)
-    from_higher = entering_state(end_backward, jnp.sum(decays[1], axis=0), "sp", head_size, True)
-    attn_out = attend(
-        query.reshape(row_total, -1), rimmed_keys, sink_logit, seq_first, seq_total, head_size,
-        key_heads,
+    attn_out, incoming = middle(
+        query.reshape(row_total, -1), rimmed_keys, sink_logit, pack_forward, pack_backward,
+        head_size, key_heads,
     )
     gate_rows = project(gate_weight)
     ssm_out = chunk_outputs(
         head_size, inner_width, map_width, act, decays, steps, (fresh_forward, fresh_backward),
-        (from_lower, from_higher), gate_rows, inner_gain.astype(jnp.float32)[None, :],
+        incoming, gate_rows, inner_gain.astype(jnp.float32)[None, :],
     )
     return combine(attn_out, ssm_out, attn_out_weight, ssm_out_weight)
 

time: 228 us -> 179 us (0.79)
  starting transfers between devices: 40.4 us -> 12.9 us
  waiting for transfers between devices: 18.2 us -> 0.01 us
  other arithmetic: 26 us -> 14.5 us
  Pallas kernels: 94.5 us -> 102 us
    ppermute x8 -> x0, starting transfers between devices: 26.7 us -> none  [moved(): return lax.ppermute(packet, axis, pairs)]
    ppermute x8 -> x0, waiting for transfers between devices: 18.2 us -> none  [moved(): return lax.ppermute(packet, axis, pairs)]
    pallas_call x1, Pallas kernels: 26 us -> 33.2 us  [middle(): pl.pallas_call(functools.partial(middle_kernel, head_size, key_heads, cou...]
    another operation x7 -> x2, other arithmetic: 3.16 us -> 0.41 us
    convert_element_type x2 -> x0, other arithmetic: 2.54 us -> none  [entering_state(): arrived = moved(held.astype(jnp.bfloat16), distance).astype(jnp.float32)]
    unnamed x56 -> x54, local copies, waits for them, and re-layouts: 5.82 us -> 8.3 us
    transpose x1 -> x2, local copies, waits for them, and re-layouts: 1.83 us -> 4.16 us  [chunk_outputs(): step[1]]
  transfers between devices with their start and end apart: 12 -> 4, of which waited for: 3 -> 0; matrix products, arithmetic and copies ran while one was open for 25% -> 25% of each run, Pallas kernels for 19% -> 10%
where the time goes in v2:
time: 179 us; the launch traced here: 178 us
  Pallas kernels  102 us (57%)
  matrix products  26.9 us (15%)
  local copies, waits for them, and re-layouts  21.6 us (12%)
  other arithmetic  14.5 us (8%)
  starting transfers between devices  12.9 us (7%)
    pallas_call x1, Pallas kernels, middle(): pl.pallas_call(functools.partial(middle_kernel, head_size, key_heads, cou...  33.2 us
    pallas_call x1, Pallas kernels, combine(): pl.pallas_call(functools.partial(combine_kernel, count), in_specs=[vmem]...  32.8 us
    dot_general x8, matrix products, project(): result = jnp.dot(normed, weight, preferred_element_type=jnp.float32)  26.9 us
    pallas_call x1, Pallas kernels, chunk_states(): pl.pallas_call(functools.partial(states_kernel, tap_count, inner, maps),...  18.3 us
    pallas_call x1, Pallas kernels, chunk_outputs(): pl.pallas_call(functools.partial(outputs_kernel, head_size, inner, maps),...  17.9 us
    ppermute x2, starting transfers between devices, extended(): lax.ppermute(lax.slice_in_dim(block, block.shape[dim] - width, None, axis...  10.3 us
    unnamed x54, local copies, waits for them, and re-layouts  8.3 us
    concatenate x2, other arithmetic, extended(): block = jnp.concatenate([low, block, high], axis=dim)  5.41 us
  transfers between devices with their start and end apart: 4, of which 0 were waited for; matrix products, arithmetic and copies ran while one was open for 25% of the time, Pallas kernels for 10%

profile of v2, /device:TPU:0, one launch (start us, length us, event | category | flops | bytes accessed | tf_op | source)
XLA Modules:
  0.0 178.5 jit_solution(10427667670384828947)
XLA Ops:
  0.0 3.2 %fusion = f32[1024]{0:T(1024)S(1)} fusion(bf16[1024,2048]{1,0:T(8,128)(2,1)} %param.20), kind=kLoop, calls=%fused_computation.2 | loop fusion | flops 6290432 | bytes 4198400 | tf_op jit(solution)/shard_map/reduce_sum | solution.py:37
  3.3 0.3 copy-done.5
  3.6 1.0 fusion.2
  4.7 1.3 convolution_convert_fusion.5
  5.9 0.7 copy-done.2
  6.6 1.2 convolution_convert_fusion.6
  7.9 0.1 copy.38
  8.1 0.5 multiply_cosine_fusion
  8.7 0.1 multiply_multiply_fusion.1
  8.9 0.2 copy.39
  9.1 0.7 pad_maximum_fusion.5
  9.8 5.2 %collective-permute-start = (bf16[128,256]{1,0:T(8,128)(2,1)}, bf16[128,256]{1,0:T(8,128)(2,1)S(1)}, u32[]{:S(2)}, u32[]{:S(2)}) collective-permute-start(bf16[128,256]{1,0:T(8,128)(2,1)} %get-tuple-element.33), channel_id=1, source_target_pairs={{0,4},{4,8},{8,12},{12,16},{16,20},{20,24},{24,28},{1,5},{5,9},{9,... | collective-permute-start | bytes 196616 | tf_op jit(solution)/shard_map/ppermute | solution.py:28
  14.9 1.3 collective-permute-start.1
  16.2 3.7 %convolution_convert_fusion.3 = bf16[1024,256]{1,0:T(8,128)(2,1)S(1)} fusion(bf16[1024,2048]{1,0:T(8,128)(2,1)} %copy-done.2, bf16[2048,256]{1,0:T(8,128)(2,1)} %param.31), kind=kOutput, calls=%fused_computation.12 | convolution fusion | flops 1074003968 | bytes 5767168 | tf_op jit(solution)/shard_map/dot_general | solution.py:637
  20.0 1.2 convolution_convert_fusion.4
  21.3 1.1 copy-done.21
  22.4 4.7 %convolution_convert_fusion.1 = bf16[1024,1024]{1,0:T(8,128)(2,1)S(1)} fusion(bf16[1024,2048]{1,0:T(8,128)(2,1)S(1)} %copy-done.3, bf16[2048,1024]{1,0:T(8,128)(2,1)S(1)} %copy-done.21), kind=kOutput, calls=%fused_computation.9 | convolution fusion | flops 4296015872 | bytes 10485760 | tf_op jit(solution)/shard_map/dot_general | solution.py:637
  27.1 1.4 copy-done.6
  28.5 0.6 pad_maximum_fusion.8
  29.1 5.2 %collective-permute-start.2 = (bf16[16,1536]{1,0:T(8,128)(2,1)}, bf16[16,1536]{1,0:T(8,128)(2,1)}, u32[]{:S(2)}, u32[]{:S(2)}) collective-permute-start(bf16[16,1536]{1,0:T(8,128)(2,1)} %get-tuple-element.19), channel_id=1, source_target_pairs={{0,4},{4,8},{8,12},{12,16},{16,20},{20,24},{24,28},{1,5},{5,9},{9,... | collective-permute-start | bytes 147464 | tf_op jit(solution)/shard_map/ppermute | solution.py:28
  34.3 1.3 collective-permute-start.3
  35.7 0.2 copy.41
  35.9 3.5 %convolution_convert_fusion.7 = bf16[1024,32]{0,1:T(8,128)(2,1)S(1)} fusion(bf16[1024,2048]{1,0:T(8,128)(2,1)} %copy-done.2, bf16[2048,32]{0,1:T(8,128)(2,1)S(1)} %bitcast.40), kind=kOutput, calls=%fused_computation.16 | convolution fusion | flops 134250496 | bytes 4390912 | tf_op jit(solution)/shard_map/dot_general | solution.py:637
  39.4 0.2 copy.40
  39.6 5.5 %convolution_convert_fusion.2 = bf16[1024,512]{1,0:T(8,128)(2,1)} fusion(bf16[1024,2048]{1,0:T(8,128)(2,1)} %copy-done.2, bf16[2048,512]{1,0:T(8,128)(2,1)S(1)} %copy-done), kind=kOutput, calls=%fused_computation.11 | convolution fusion | flops 2148007936 | bytes 7340032 | tf_op jit(solution)/shard_map/dot_general | solution.py:637
  45.1 1.5 copy.37
  46.6 0.3 multiply_reduce_fusion
  46.9 0.5 multiply_multiply_fusion
  47.4 0.3 subtract_convert_fusion
  47.7 1.1 copy-done.22
  48.8 1.4 copy-done.4
  50.1 5.7 %convolution_convert_fusion.gate_ref = bf16[1024,1024]{1,0:T(8,128)(2,1)} fusion(bf16[1024,2048]{1,0:T(8,128)(2,1)S(1)} %copy-done.4, bf16[2048,1024]{1,0:T(8,128)(2,1)S(1)} %copy-done.22), kind=kOutput, calls=%fused_computation.8 | convolution fusion | flops 4296015872 | bytes 10485760 | tf_op jit(solution)/shard_map/dot_general | solution.py:637
  55.8 0.6 maximum_convert_fusion.taps_ref
  56.5 0.3 compare_select_fusion
  56.8 2.3 %slice_bitcast_fusion = (f32[16,1024]{0,1:T(8,128)}, f32[1024,16]{1,0:T(8,128)}, f32[1024,16]{1,0:T(8,128)}, f32[16,1024]{0,1:T(8,128)}, f32[1024,16]{1,0:T(8,12...) fusion(f32[1024,32]{1,0:T(8,128)S(1)} %get-tuple-element.35, f32[1024,32]{1,0:T(8,128)S(1)} %get-tuple-element.36), kind=kLoop, calls=%fused_computation.46 | loop fusion | bytes 786432 | tf_op jit(solution)/shard_map/transpose | solution.py:602
  59.2 0.6 broadcast_in_dim.6
  59.8 1.3 copy.42.query_ref
  61.1 1.8 %copy.46.stbt_ref = f32[16,1024]{1,0:T(8,128)} copy(f32[16,1024]{0,1:T(8,128)} %get-tuple-element.25) | data formatting | bytes 131072 | tf_op jit(solution)/shard_map/transpose | solution.py:602
  63.0 1.8 %copy.45.stft_ref = f32[16,1024]{1,0:T(8,128)} copy(f32[16,1024]{0,1:T(8,128)} %get-tuple-element.28) | data formatting | bytes 131072 | tf_op jit(solution)/shard_map/transpose | solution.py:602
  64.8 1.8 %copy.43.ldft_ref = f32[16,1024]{1,0:T(8,128)} copy(f32[16,1024]{0,1:T(8,128)} %get-tuple-element.41) | data formatting | bytes 131072 | tf_op jit(solution)/shard_map/transpose | solution.py:602
  66.7 1.8 %copy.44.ldbt_ref = f32[16,1024]{1,0:T(8,128)} copy(f32[16,1024]{0,1:T(8,128)} %get-tuple-element.42) | data formatting | bytes 131072 | tf_op jit(solution)/shard_map/transpose | solution.py:602
  68.5 3.6 %pad_maximum_fusion.rows_ref = bf16[1056,1536]{1,0:T(8,128)(2,1)} fusion(bf16[16,1536]{1,0:T(8,128)(2,1)} %collective-permute-done.3, bf16[1024,256]{1,0:T(8,128)(2,1)} %copy-done.8, bf16[1024,256]{1,0:T(8,128)(2,1)} %copy-done.9, bf16[1024,1024]{1,0:T(8,128)(2,1)S(1)} %copy-done.7, bf16[16,1536]{1,0:T(8,128)(2,1)} %collective-permute-done.2), kind=kLoop, calls=%fused_computation.5 | loop fusion | flops 16220160 | bytes 6488064 | tf_op jit(solution)/shard_map/concatenate | solution.py:32
  72.1 18.3 %chunk_states.1 = (bf16[1024,1536]{1,0:T(8,128)(2,1)}, f32[8,128,1024]{2,1,0:T(8,128)}, f32[8,128,1024]{2,1,0:T(8,128)}, bf16[2,144,512]{2,1,0:T(8,128)(2,1)}, bf16[2,144,512]{2,1,0:T(8,128)(2,1)}) custom-call(bf16[1056,1536]{1,0:T(8,128)(2,1)} %pad_maximum_fusion.rows_ref, f32[5,1536]{1,0:T(8,128)} %maximum_convert_fusion.taps_ref, ...), custom_call_target="tpu_custom_call" | custom-call | flops 1073741824 | bytes 16777216 | tf_op jit(solution)/shard_map/chunk_states/pallas_call | solution.py:543
  90.4 1.8 %pad_maximum_fusion.2.rim_ref = bf16[1280,256]{1,0:T(8,128)(2,1)} fusion(bf16[128,256]{1,0:T(8,128)(2,1)} %collective-permute-done.1, bf16[1024,128]{1,0:T(8,128)(2,1)S(1)} %copy-done.11, bf16[1024,128]{1,0:T(8,128)(2,1)S(1)} %copy.39, bf16[128,256]{1,0:T(8,128)(2,1)S(1)} %collective-permute-done), kind=kLoop, calls=%fused_computation.22 | loop fusion | flops 2621440 | bytes 1310720 | tf_op jit(solution)/shard_map/concatenate | solution.py:32
  92.3 33.2 %middle.1 = (bf16[1024,512]{1,0:T(8,128)(2,1)}, f32[2,2,128,512]{3,2,1,0:T(8,128)}) custom-call(f32[8]{0:T(128)} %sink_ref.1, bf16[1024,512]{1,0:T(8,128)(2,1)} %copy.42.query_ref, bf16[1280,256]{1,0:T(8,128)(2,1)} %pad_maximum_fusion.2.rim_ref, bf16[2,144,512]{2,1,0:T(8,128)(2,1)} %get-tuple-element.12.packf_ref, ...), custom_call_target="tpu_custom_call" | custom-call | flops 805306368 | bytes 2097152 | tf_op jit(solution)/shard_map/middle/pallas_call | solution.py:381
  125.5 17.9 %chunk_outputs.1.ssm_ref = bf16[1024,1024]{1,0:T(8,128)(2,1)} custom-call(bf16[1024,1536]{1,0:T(8,128)(2,1)} %get-tuple-element.15.act_ref, f32[1024,16]{1,0:T(8,128)} %get-tuple-element.39.ldf_ref, f32[1024,16]{1,0:T(8,128)} %get-tuple-element.40.ldb_ref.ldball_ref, f32[1024,16]{1,0:T(8,128)} %get-tuple-element.27.stf_ref, ...), custom_call_target="tpu_custom_call" | custom-call | flops 1073741824 | bytes 16777216 | tf_op jit(solution)/shard_map/chunk_outputs/pallas_call | solution.py:576
  143.4 32.8 %combine.1 = bf16[256,2048]{1,0:T(8,128)(2,1)} custom-call(bf16[1024,512]{1,0:T(8,128)(2,1)} %get-tuple-element.14.attn_ref, bf16[1024,1024]{1,0:T(8,128)(2,1)} %chunk_outputs.1.ssm_ref, bf16[512,2048]{1,0:T(8,128)(2,1)} %attn_w_ref.1, bf16[1024,2048]{1,0:T(8,128)(2,1)} %ssm_w_ref.1), custom_call_target="tpu_custom_call" | custom-call | flops 6442450944 | bytes 6291456 | tf_op jit(solution)/shard_map/combine/pallas_call | solution.py:509
  176.2 2.3 %copy.49 = bf16[256,2048]{1,0:T(8,128)(2,1)} copy(bf16[256,2048]{1,0:T(8,128)(2,1)} %combine.1) | data formatting | bytes 2097152
  (63 shorter events, 0.5 us)
Async XLA Ops:
  0.0 39.6 %copy-start = (bf16[2048,512]{1,0:T(8,128)(2,1)S(1)}, bf16[2048,512]{1,0:T(8,128)(2,1)}, u32[]{:S(2)}) copy-start(bf16[2048,512]{1,0:T(8,128)(2,1)} %param.22) | copy-start | bytes 6291460
  0.0 3.3 %copy-start.16 = (bf16[2048]{0:T(1024)(128)(2,1)S(1)}, bf16[2048]{0:T(1024)(128)(2,1)}, u32[]{:S(2)}) copy-start(bf16[2048]{0:T(1024)(128)(2,1)} %param.21) | copy-start | bytes 12292
  0.0 3.6 %copy-start.5 = (bf16[1024,2048]{1,0:T(8,128)(2,1)S(1)}, bf16[1024,2048]{1,0:T(8,128)(2,1)}, u32[]{:S(2)}) copy-start(bf16[1024,2048]{1,0:T(8,128)(2,1)} %param.20) | copy-start | bytes 12582916
  3.6 1.0 copy-start.24
  4.7 2.0 %copy-start.2 = (bf16[1024,2048]{1,0:T(8,128)(2,1)}, bf16[1024,2048]{1,0:T(8,128)(2,1)S(1)}, u32[]{:S(2)}) copy-start(bf16[1024,2048]{1,0:T(8,128)(2,1)S(1)} %fusion.2) | copy-start | bytes 12582916
  4.7 2.0 %copy-start.25 = (bf16[2048,128]{1,0:T(8,128)(2,1)S(1)}, bf16[2048,128]{1,0:T(8,128)(2,1)}, u32[]{:S(2)}) copy-start(bf16[2048,128]{1,0:T(8,128)(2,1)} %param.23) | copy-start | bytes 1572868
  6.6 2.4 %copy-start.10 = (bf16[1024,128]{1,0:T(8,128)(2,1)}, bf16[1024,128]{1,0:T(8,128)(2,1)S(1)}, u32[]{:S(2)}) copy-start(bf16[1024,128]{1,0:T(8,128)(2,1)S(1)} %convolution_convert_fusion.5) | copy-start | bytes 786436
  6.6 2.0 %copy-start.19 = (f32[64]{0:T(128)S(1)}, f32[64]{0:T(128)}, u32[]{:S(2)}) copy-start(f32[64]{0:T(128)} %param.26) | copy-start | bytes 772
  9.1 10.9 %copy-start.3 = (bf16[1024,2048]{1,0:T(8,128)(2,1)S(1)}, bf16[1024,2048]{1,0:T(8,128)(2,1)}, u32[]{:S(2)}) copy-start(bf16[1024,2048]{1,0:T(8,128)(2,1)} %copy-done.2) | copy-start | bytes 12582916
  9.1 10.9 %copy-start.23 = (bf16[2048,256]{1,0:T(8,128)(2,1)S(1)}, bf16[2048,256]{1,0:T(8,128)(2,1)}, u32[]{:S(2)}) copy-start(bf16[2048,256]{1,0:T(8,128)(2,1)} %param.30) | copy-start | bytes 3145732
  9.8 80.7 %collective-permute-start = (bf16[128,256]{1,0:T(8,128)(2,1)}, bf16[128,256]{1,0:T(8,128)(2,1)S(1)}, u32[]{:S(2)}, u32[]{:S(2)}) collective-permute-start(bf16[128,256]{1,0:T(8,128)(2,1)} %get-tuple-element.33), channel_id=1, source_target_pairs={{0,4},{4,8},{8,12},{12,16},{16,20},{20,24},{24,28},{1,5},{5,9},{9,... | collective-permute-start | bytes 196616 | tf_op jit(solution)/shard_map/ppermute | solution.py:28
  14.9 75.5 %collective-permute-start.1 = (bf16[128,256]{1,0:T(8,128)(2,1)}, bf16[128,256]{1,0:T(8,128)(2,1)}, u32[]{:S(2)}, u32[]{:S(2)}) collective-permute-start(bf16[128,256]{1,0:T(8,128)(2,1)} %get-tuple-element.34), channel_id=1, source_target_pairs={{4,0},{8,4},{12,8},{16,12},{20,16},{24,20},{28,24},{5,1},{9,5},{13... | collective-permute-start | bytes 196616 | tf_op jit(solution)/shard_map/ppermute | solution.py:31
  20.0 7.1 %copy-start.8 = (bf16[1024,256]{1,0:T(8,128)(2,1)}, bf16[1024,256]{1,0:T(8,128)(2,1)S(1)}, u32[]{:S(2)}) copy-start(bf16[1024,256]{1,0:T(8,128)(2,1)S(1)} %convolution_convert_fusion.3) | copy-start | bytes 1572868
  20.0 2.4 %copy-start.21 = (bf16[2048,1024]{1,0:T(8,128)(2,1)S(1)}, bf16[2048,1024]{1,0:T(8,128)(2,1)}, u32[]{:S(2)}) copy-start(bf16[2048,1024]{1,0:T(8,128)(2,1)} %param.29) | copy-start | bytes 12582916
  22.4 4.8 %copy-start.9 = (bf16[1024,256]{1,0:T(8,128)(2,1)}, bf16[1024,256]{1,0:T(8,128)(2,1)S(1)}, u32[]{:S(2)}) copy-start(bf16[1024,256]{1,0:T(8,128)(2,1)S(1)} %convolution_convert_fusion.4) | copy-start | bytes 1572868
  22.4 13.2 %copy-start.18 = (f32[2,16]{1,0:T(2,128)S(1)}, f32[2,16]{1,0:T(2,128)}, u32[]{:S(2)}) copy-start(f32[2,16]{1,0:T(2,128)} %param.35) | copy-start | bytes 388
  22.4 13.3 %copy-start.15 = (bf16[5,2,256]{2,1,0:T(2,128)(2,1)S(1)}, bf16[5,2,256]{2,1,0:T(2,128)(2,1)}, u32[]{:S(2)}) copy-start(bf16[5,2,256]{2,1,0:T(2,128)(2,1)} %param.34) | copy-start | bytes 15364
  22.4 13.3 %copy-start.12 = (f32[1024,2,16]{0,2,1:T(8,128)S(1)}, f32[1024,2,16]{0,2,1:T(8,128)}, u32[]{:S(2)}) copy-start(f32[1024,2,16]{0,2,1:T(8,128)} %param.36) | copy-start | bytes 393220
  22.4 13.5 %copy-start.13 = (bf16[2048,2,16]{0,2,1:T(8,128)(2,1)S(1)}, bf16[2048,2,16]{0,2,1:T(8,128)(2,1)}, u32[]{:S(2)}) copy-start(bf16[2048,2,16]{0,2,1:T(8,128)(2,1)} %param.32) | copy-start | bytes 393220
  27.1 1.4 copy-start.6
  29.1 39.4 %collective-permute-start.2 = (bf16[16,1536]{1,0:T(8,128)(2,1)}, bf16[16,1536]{1,0:T(8,128)(2,1)}, u32[]{:S(2)}, u32[]{:S(2)}) collective-permute-start(bf16[16,1536]{1,0:T(8,128)(2,1)} %get-tuple-element.19), channel_id=1, source_target_pairs={{0,4},{4,8},{8,12},{12,16},{16,20},{20,24},{24,28},{1,5},{5,9},{9,... | collective-permute-start | bytes 147464 | tf_op jit(solution)/shard_map/ppermute | solution.py:28
  34.3 34.2 %collective-permute-start.3 = (bf16[16,1536]{1,0:T(8,128)(2,1)}, bf16[16,1536]{1,0:T(8,128)(2,1)}, u32[]{:S(2)}, u32[]{:S(2)}) collective-permute-start(bf16[16,1536]{1,0:T(8,128)(2,1)} %get-tuple-element.20), channel_id=1, source_target_pairs={{4,0},{8,4},{12,8},{16,12},{20,16},{24,20},{28,24},{5,1},{9,5},{13... | collective-permute-start | bytes 147464 | tf_op jit(solution)/shard_map/ppermute | solution.py:31
  45.1 1.8 %copy-start.20 = (f32[64]{0:T(128)S(1)}, f32[64]{0:T(128)}, u32[]{:S(2)}) copy-start(f32[64]{0:T(128)} %param.25) | copy-start | bytes 772
  46.6 2.2 %copy-start.22 = (bf16[2048,1024]{1,0:T(8,128)(2,1)S(1)}, bf16[2048,1024]{1,0:T(8,128)(2,1)}, u32[]{:S(2)}) copy-start(bf16[2048,1024]{1,0:T(8,128)(2,1)} %param.28) | copy-start | bytes 12582916
  46.9 3.2 %copy-start.4 = (bf16[1024,2048]{1,0:T(8,128)(2,1)S(1)}, bf16[1024,2048]{1,0:T(8,128)(2,1)}, u32[]{:S(2)}) copy-start(bf16[1024,2048]{1,0:T(8,128)(2,1)} %copy-done.2) | copy-start | bytes 12582916
  50.1 5.7 %copy-start.14 = (bf16[5,1024]{1,0:T(8,128)(2,1)S(1)}, bf16[5,1024]{1,0:T(8,128)(2,1)}, u32[]{:S(2)}) copy-start(bf16[5,1024]{1,0:T(8,128)(2,1)} %param.33) | copy-start | bytes 30724
  56.8 2.4 %copy-start.17 = (bf16[1024]{0:T(1024)(128)(2,1)S(1)}, bf16[1024]{0:T(1024)(128)(2,1)}, u32[]{:S(2)}) copy-start(bf16[1024]{0:T(1024)(128)(2,1)} %param.37) | copy-start | bytes 6148
  59.1 9.4 %copy-start.7 = (bf16[1024,1024]{1,0:T(8,128)(2,1)S(1)}, bf16[1024,1024]{1,0:T(8,128)(2,1)}, u32[]{:S(2)}) copy-start(bf16[1024,1024]{1,0:T(8,128)(2,1)} %copy-done.6) | copy-start | bytes 6291460
  72.1 18.3 %copy-start.11 = (bf16[1024,128]{1,0:T(8,128)(2,1)S(1)}, bf16[1024,128]{1,0:T(8,128)(2,1)}, u32[]{:S(2)}) copy-start(bf16[1024,128]{1,0:T(8,128)(2,1)} %copy-done.10) | copy-start | bytes 786436
  143.4 35.1 %copy-start.1 = (bf16[2048,512]{1,0:T(8,128)(2,1)S(1)}, bf16[2048,512]{1,0:T(8,128)(2,1)}, u32[]{:S(2)}) copy-start(bf16[2048,512]{1,0:T(8,128)(2,1)} %param.22) | copy-start | bytes 6291460

commit v3 on v2

--- a/solution.py
+++ b/solution.py
@@ -2,6 +2,7 @@
 
 import jax
 import jax.numpy as jnp
+import numpy as np
 from jax import lax
 from jax.experimental import pallas as pl
 from jax.experimental.pallas import tpu as pltpu
@@ -16,43 +17,10 @@
 ROPE_BASE = 500000.0
 NEG_FILL = -1e30
 PIECE = 256
+TILE = 512
+MIB = 1 << 20
 PACK_ROWS = 16
 MESH = pl.DeviceIdType.MESH
-
-
-def extended(block, sides, width):
-    for axis, dim in sides:
-        count = lax.axis_size(axis)
-        forward = [(i, i + 1) for i in range(count - 1)]
-        backward = [(target, source) for source, target in forward]
-        low = lax.ppermute(
-            lax.slice_in_dim(block, block.shape[dim] - width, None, axis=dim), axis, forward
-        )
-        high = lax.ppermute(lax.slice_in_dim(block, 0, width, axis=dim), axis, backward)
-        block = jnp.concatenate([low, block, high], axis=dim)
-    return block
-
-
-def rms_rows(values, scales):
-    return values * lax.rsqrt(jnp.mean(values * values, axis=-1, keepdims=True) + NORM_EPS) * scales
-
-
-def rotate(head_rows, positions):
-    head_size = head_rows.shape[-1]
-    half_size = head_size // 2
-    frequency = ROPE_BASE ** (-jnp.arange(0, head_size, 2, dtype=jnp.float32) / head_size)
-    angles = positions.astype(jnp.float32)[:, None] * frequency
-    cosine = jnp.cos(angles)[:, None, :]
-    sine_part = jnp.sin(angles)[:, None, :]
-    first_half = head_rows[..., :half_size]
-    second_half = head_rows[..., half_size:]
-    return jnp.concatenate(
-        [
-            first_half * cosine - second_half * sine_part,
-            second_half * cosine + first_half * sine_part,
-        ],
-        axis=-1,
-    )
 
 
 def spread(factor, width):
@@ -76,68 +44,397 @@
     return jnp.where(row >= column if lower else row <= column, 1.0, 0.0)
 
 
-def states_kernel(
-    tap_count, inner, maps, rows_ref, taps_ref, ldf_ref, ldb_ref, stf_ref, stb_ref,
-    act_ref, freshf_ref, freshb_ref, packf_ref, packb_ref, spare, reach, endf_ref, endb_ref, logs,
+def project_kernel(
+    head_size, heads, key_width, tokens_ref, inner_hbm, in_hbm, out_hbm, key_hbm, value_hbm,
+    query_hbm, gate_hbm, step_ref, small_ref, jump_ref, query_ref, keyed_ref, rows_ref, gate_ref,
+    table_ref, turned_ref, tokens, normed, inner_w, in_w, out_w, keyed_w, query_w, gate_w, raw,
+    cosine, sine, token_sems, weight_sems,
 ):
-    step = pl.program_id(0)
-    size = act_ref.shape[0]
-    start = pl.multiple_of(step * size, size)
-    spare[...] = rows_ref[pl.ds(start, size + 2 * HALO), :].astype(jnp.float32)
-    first = HALO - tap_count // 2
-    filtered = spare[first : first + size, :] * taps_ref[0:1, :]
-    for k in range(1, tap_count):
-        filtered = filtered + spare[first + k : first + k + size, :] * taps_ref[k : k + 1, :]
-    activated = filtered / (1.0 + jnp.exp(-filtered))
-    act_ref[...] = activated.astype(jnp.bfloat16)
-    signal = activated[:, :inner]
-    ldf, ldb = ldf_ref[...], ldb_ref[...]
-    cumf = exact_dot(triangle(size, True), ldf)
-    cumb = exact_dot(triangle(size, False), ldb)
-    wf = jnp.exp(cumf[size - 1 : size] - cumf) * stf_ref[...]
-    wb = jnp.exp(cumb[0:1] - cumb) * stb_ref[...]
-    xf = (signal * spread(wf, inner)).astype(jnp.bfloat16)
-    xb = (signal * spread(wb, inner)).astype(jnp.bfloat16)
-    totf = spread(jnp.exp(jnp.broadcast_to(cumf[size - 1 : size], (8, ldf.shape[1]))), inner)[0:1]
-    totb = spread(jnp.exp(jnp.broadcast_to(cumb[0:1], (8, ldb.shape[1]))), inner)[0:1]
-
-    @pl.when(step == 0)
+    total, depth = tokens.shape
+    parts = token_sems.shape[0]
+    size = total // parts
+    moves = [
+        pltpu.make_async_copy(
+            tokens_ref.at[pl.ds(i * size, size)], tokens.at[pl.ds(i * size, size)],
+            token_sems.at[i],
+        )
+        for i in range(parts)
+    ]
+    joined = key_width % 128 == 0
+    if joined:
+        key_w, value_w = keyed_w.at[:, :key_width], keyed_w.at[:, key_width:]
+    else:
+        key_w, value_w = keyed_w.at[0], keyed_w.at[1]
+    weights = (
+        (key_hbm, key_w), (value_hbm, value_w), (query_hbm, query_w), (in_hbm, in_w),
+        (out_hbm, out_w), (inner_hbm, inner_w), (gate_hbm, gate_w),
+    )
+    loads = [
+        pltpu.make_async_copy(source, target, weight_sems.at[i])
+        for i, (source, target) in enumerate(weights)
+    ]
+    for move in moves + loads:
+        move.start()
+    lanes = depth // 128
+    frequency, sign = small_ref[lanes + 2 : lanes + 3], small_ref[lanes + 3 : lanes + 4]
+    order = lax.broadcasted_iota(jnp.int32, (32, 128), 0)
+    first = lax.axis_index("sp") * total
+    near = order.astype(jnp.float32) * frequency
+    cos_near, sin_near = jnp.cos(near), jnp.sin(near)
+    for a in range(0, total, 1024):
+        far = (first + a + 32 * order).astype(jnp.float32) * frequency
+        cos_far, sin_far = jnp.cos(far), jnp.sin(far)
+        for r in range(min(32, (total - a) // 32)):
+            c, d = cos_far[r : r + 1], sin_far[r : r + 1]
+            span = slice(a + r * 32, a + (r + 1) * 32)
+            cosine[span, :] = c * cos_near - d * sin_near
+            sine[span, :] = (d * cos_near + c * sin_near) * sign
+    for i in range(parts):
+        moves[i].wait()
+
+        @pl.loop(0, size // 32)
+        def _(r, i=i):
+            span = pl.ds(pl.multiple_of(i * size + r * 32, 32), 32)
+            squares = jnp.zeros((32, 128), jnp.float32)
+            for j in range(lanes):
+                x = tokens[span, j * 128 : (j + 1) * 128].astype(jnp.float32)
+                squares = squares + x * x
+            mean = jnp.sum(squares, axis=-1, keepdims=True) * (1.0 / depth)
+            scale = lax.rsqrt(mean + NORM_EPS)
+            for j in range(lanes):
+                cols = slice(j * 128, (j + 1) * 128)
+                x = tokens[span, cols].astype(jnp.float32)
+                normed[span, cols] = (x * scale * small_ref[j : j + 1]).astype(jnp.bfloat16)
+
+    def run(weight, target, column, beside=None):
+        width = min(weight.shape[1], TILE)
+        count = weight.shape[1] // width
+
+        def tile(j):
+            at = j * width if count == 1 else pl.multiple_of(j * width, width)
+            target[:, pl.ds(column + at, width)] = jnp.dot(
+                normed[...], weight[:, pl.ds(at, width)], preferred_element_type=jnp.float32
+            ).astype(jnp.bfloat16)
+            if beside is not None:
+                beside(j, total // count)
+
+        if count == 1:
+            tile(0)
+        else:
+            pl.loop(0, count)(tile)
+
+    raw[:, 2 * heads :] = jnp.zeros((total, 128 - 2 * heads), jnp.float32)
+    raw[:, : 2 * heads] = lax.dot_general(
+        normed[...], step_ref[...], (((1,), (1,)), ((), ())), preferred_element_type=jnp.float32
+    ).astype(jnp.bfloat16).astype(jnp.float32)
+    rates = jnp.transpose(jnp.broadcast_to(small_ref[lanes + 4 : lanes + 5], (128, 128)))
+    rates = rates[: 2 * heads, 0:1]
+    upper, lower = triangle(CHUNK, False), triangle(CHUNK, True)
+
+    def steps(j, length):
+        for c in range(length // CHUNK):
+            at = pl.multiple_of(j * length + c * CHUNK, CHUNK)
+            span = pl.ds(at, CHUNK)
+            x = jnp.transpose(raw[span, :])[: 2 * heads]
+            step = jnp.maximum(x, 0.0) + jnp.log1p(jnp.exp(-jnp.abs(x)))
+            decay = jump_ref[:, span] - rates * step
+            filled = jnp.concatenate(
+                [
+                    exact_dot(decay[:heads], upper), exact_dot(decay[heads:], lower), step,
+                    jnp.zeros((128 - 4 * heads, CHUNK), jnp.float32),
+                ],
+                axis=0,
+            )
+            turned_ref[:, span] = filled
+            table_ref[span, :] = jnp.transpose(filled)
+
+    row = lax.broadcasted_iota(jnp.int32, (256, 128), 0)
+    column = lax.broadcasted_iota(jnp.int32, (256, 128), 1)
+    same_head = jnp.where(
+        lax.rem(row, 128) // head_size == column // head_size, 1.0, 0.0
+    ).astype(jnp.bfloat16)
+    lane = lax.broadcasted_iota(jnp.int32, (128, 128), 1)
+    half = head_size // 2
+    first_half = lax.rem(lane, head_size) < half
+
+    def rotate(value, gain_row, cos_here, sin_here):
+        square = value * value
+        high = square.astype(jnp.bfloat16)
+        low = (square - high.astype(jnp.float32)).astype(jnp.bfloat16)
+        sums = jnp.dot(
+            jnp.concatenate([high, low], axis=1), same_head, preferred_element_type=jnp.float32
+        )
+        value = value * lax.rsqrt(sums * (1.0 / head_size) + NORM_EPS) * gain_row
+        swapped = jnp.where(
+            first_half, pltpu.roll(value, 128 - half, 1), pltpu.roll(value, half, 1)
+        )
+        return (value * cos_here + swapped * sin_here).astype(jnp.bfloat16)
+
+    def heads_of(j, length):
+        for i in range(length // 128):
+            span = pl.ds(pl.multiple_of(j * length + i * 128, 128), 128)
+            cos_here, sin_here = cosine[span, :], sine[span, :]
+            for at in range(0, query_ref.shape[1], 128):
+                value = query_ref[span, at : at + 128].astype(jnp.float32)
+                query_ref[span, at : at + 128] = rotate(
+                    value, small_ref[lanes : lanes + 1], cos_here, sin_here
+                )
+            for at in range(0, key_width, 128):
+                packed = keyed_ref[span, at : at + 128]
+                keys = rotate(
+                    packed.astype(jnp.float32), small_ref[lanes + 1 : lanes + 2], cos_here, sin_here
+                )
+                keyed_ref[span, at : at + 128] = jnp.where(lane + at < key_width, keys, packed)
+
+    inner, maps = inner_w.shape[1], in_w.shape[1]
+    loads[0].wait()
+    loads[1].wait()
+    if joined:
+        run(keyed_w, keyed_ref, 0)
+    else:
+        run(keyed_w.at[0], keyed_ref, 0)
+        run(keyed_w.at[1], keyed_ref, key_width)
+    loads[2].wait()
+    run(query_w, query_ref, 0)
+    loads[3].wait()
+    run(in_w, rows_ref, inner)
+    loads[4].wait()
+    run(out_w, rows_ref, inner + maps)
+    loads[5].wait()
+    run(inner_w, rows_ref, 0, steps)
+    loads[6].wait()
+    run(gate_w, gate_ref, 0, heads_of)
+
+
+def project_all(
+    tokens, norm_gain, inner_weight, input_map, output_map, key_weight, value_weight, query_weight,
+    gate_weight, step_weight, query_gain, key_gain, decay_rate, decay_jump,
+):
+    total, depth = tokens.shape
+    head_size = query_gain.shape[0]
+    half = head_size // 2
+    lane = np.arange(128)
+    frequency = (ROPE_BASE ** (-2.0 * (lane % half) / head_size)).astype(np.float32)
+    sign = np.where(lane % head_size < half, -1.0, 1.0).astype(np.float32)
+    repeats = 128 // head_size
+    rates = decay_rate.reshape(-1)
+    small = jnp.concatenate(
+        [
+            norm_gain.astype(jnp.float32), jnp.tile(query_gain, repeats) * head_size ** (-0.5),
+            jnp.tile(key_gain, repeats), frequency, sign, rates,
+            jnp.zeros((4 * 128 - rates.shape[0],), jnp.float32),
+        ]
+    ).reshape(-1, 128)
+    turned_step = jnp.transpose(step_weight, (1, 2, 0)).reshape(-1, depth)
+    turned_jump = jnp.transpose(decay_jump, (1, 2, 0)).reshape(-1, total)
+    heads = step_weight.shape[2]
+    inner, maps = inner_weight.shape[1], input_map.shape[1]
+    width, key_width = query_weight.shape[1], key_weight.shape[1]
+    whole = pl.BlockSpec(memory_space=pltpu.HBM)
+    vmem = pl.BlockSpec(memory_space=pltpu.VMEM)
+    big = (inner_weight, input_map, output_map, key_weight, value_weight, query_weight, gate_weight)
+    columns = sum(w.shape[1] for w in big)
+    keyed_shape = (depth, 2 * key_width) if key_width % 128 == 0 else (2, depth, key_width)
+
+    def shape(*dims, kind=jnp.bfloat16):
+        return jax.ShapeDtypeStruct(dims, kind)
+
+    def room(*dims, kind=jnp.bfloat16):
+        return pltpu.VMEM(dims, kind)
+
+    return pl.pallas_call(
+        functools.partial(project_kernel, head_size, heads, key_width),
+        in_specs=[whole] * 8 + [vmem] * 3,
+        out_specs=[vmem] * 6,
+        out_shape=[
+            shape(total, width), shape(total, 2 * key_width), shape(total, inner + 2 * maps),
+            shape(total, inner), shape(total, 128, kind=jnp.float32),
+            shape(128, total, kind=jnp.float32),
+        ],
+        scratch_shapes=[
+            room(total, depth), room(total, depth), room(*inner_weight.shape),
+            room(*input_map.shape), room(*output_map.shape), room(*keyed_shape),
+            room(*query_weight.shape), room(*gate_weight.shape),
+            room(total, 128, kind=jnp.float32), room(total, 128, kind=jnp.float32),
+            room(total, 128, kind=jnp.float32),
+            pltpu.SemaphoreType.DMA((8,)), pltpu.SemaphoreType.DMA((7,)),
+        ],
+        compiler_params=pltpu.CompilerParams(vmem_limit_bytes=52 * MIB),
+        cost_estimate=pl.CostEstimate(
+            flops=2 * total * depth * columns, bytes_accessed=2 * depth * (columns + total),
+            transcendentals=total * 128,
+        ),
+        name="project",
+    )(tokens, *big, turned_step, small, turned_jump)
+
+
+def convolve_kernel(
+    tap_count, inner, maps, heads, count, rows_ref, keyed_ref, taps_ref, table_ref, act_ref,
+    freshf_ref, freshb_ref, packf_ref, packb_ref, rim_ref, spare, low_rows, high_rows, low_keys,
+    high_keys, endf, endb, sends, receives,
+):
+    me = lax.axis_index("sp")
+    total = rows_ref.shape[0]
+    size = CHUNK
+    chunks = total // size
+
+    def copies(up):
+        device = me + 1 if up else me - 1
+        slot = 0 if up else 2
+        edge = pl.ds(total - HALO if up else 0, HALO)
+        wide = pl.ds(total - WINDOW if up else 0, WINDOW)
+        pairs = (
+            (rows_ref.at[edge], low_rows if up else high_rows),
+            (keyed_ref.at[wide], low_keys if up else high_keys),
+        )
+        return [
+            pltpu.make_async_remote_copy(
+                src_ref=source, dst_ref=target, send_sem=sends.at[slot + i],
+                recv_sem=receives.at[slot + i], device_id={"sp": device}, device_id_type=MESH,
+            )
+            for i, (source, target) in enumerate(pairs)
+        ]
+
+    barrier = pltpu.get_barrier_semaphore()
+    for step in (1, count - 1):
+        pl.semaphore_signal(
+            barrier, inc=1, device_id={"sp": lax.rem(me + step, count)}, device_id_type=MESH
+        )
+    pl.semaphore_wait(barrier, 2)
+    has_low, has_high = me > 0, me < count - 1
+
+    @pl.when(has_high)
     def _():
-        endf_ref[...] = jnp.zeros_like(endf_ref)
-        endb_ref[...] = jnp.zeros_like(endb_ref)
-        reach[...] = jnp.ones_like(reach)
-        logs[...] = jnp.zeros_like(logs)
-
+        for copy in copies(True):
+            copy.start()
+
+    @pl.when(has_low)
+    def _():
+        for copy in copies(False):
+            copy.start()
+
+    @pl.when(jnp.logical_not(has_low))
+    def _():
+        low_rows[...] = jnp.zeros_like(low_rows)
+        low_keys[...] = jnp.zeros_like(low_keys)
+
+    @pl.when(jnp.logical_not(has_high))
+    def _():
+        high_rows[...] = jnp.zeros_like(high_rows)
+        high_keys[...] = jnp.zeros_like(high_keys)
+
+    rim_ref[WINDOW : WINDOW + total, :] = keyed_ref[...]
+
+    @pl.loop(0, chunks)
+    def _(turn):
+        c = lax.rem(turn + 1, chunks)
+        start = pl.multiple_of(c * size, size)
+        spare[HALO : HALO + size, :] = rows_ref[pl.ds(start, size), :].astype(jnp.float32)
+
+        @pl.when(turn == chunks - 2)
+        def _():
+            @pl.when(has_low)
+            def _():
+                for copy in copies(True):
+                    copy.wait_recv()
+
+            @pl.when(has_high)
+            def _():
+                for copy in copies(False):
+                    copy.wait_recv()
+
+        @pl.when(c == 0)
+        def _():
+            spare[:HALO, :] = low_rows[...].astype(jnp.float32)
+
+        @pl.when(c > 0)
+        def _():
+            at = pl.multiple_of(start - HALO, HALO)
+            spare[:HALO, :] = rows_ref[pl.ds(at, HALO), :].astype(jnp.float32)
+
+        @pl.when(c == chunks - 1)
+        def _():
+            spare[HALO + size :, :] = high_rows[...].astype(jnp.float32)
+
+        @pl.when(c < chunks - 1)
+        def _():
+            at = pl.multiple_of(start + size, HALO)
+            spare[HALO + size :, :] = rows_ref[pl.ds(at, HALO), :].astype(jnp.float32)
+
+        first = HALO - tap_count // 2
+        for at in range(0, inner + 2 * maps, 128):
+            cols = slice(at, at + 128)
+            filtered = spare[first : first + size, cols] * taps_ref[0:1, cols]
+            for k in range(1, tap_count):
+                filtered = (
+                    filtered + spare[first + k : first + k + size, cols] * taps_ref[k : k + 1, cols]
+                )
+            act_ref[pl.ds(start, size), cols] = (
+                filtered * (1.0 / (1.0 + jnp.exp(-filtered)))
+            ).astype(jnp.bfloat16)
+
+    rim_ref[:WINDOW, :] = low_keys[...]
+    rim_ref[WINDOW + total :, :] = high_keys[...]
     groups = maps // STATE_SIZE
     width = inner // groups
-    for g in range(groups):
-        entry = activated[:, inner + g * STATE_SIZE : inner + (g + 1) * STATE_SIZE]
-        entry = jnp.transpose(entry).astype(jnp.bfloat16)
-        cols = slice(g * width, (g + 1) * width)
-        ff = jnp.dot(entry, xf[:, cols], preferred_element_type=jnp.float32)
-        fb = jnp.dot(entry, xb[:, cols], preferred_element_type=jnp.float32)
-        freshf_ref[0, :, cols] = ff
-        freshb_ref[0, :, cols] = fb
-        endf_ref[:, cols] = endf_ref[:, cols] * totf[:, cols] + ff
-        endb_ref[:, cols] = endb_ref[:, cols] + reach[0:1, cols] * fb
-    reach[...] = reach[...] * totb
-    logs[0] = logs[0] + cumf[size - 1 : size]
-    logs[1] = logs[1] + cumb[0:1]
-
-    @pl.when(step == pl.num_programs(0) - 1)
+
+    @pl.loop(0, chunks)
+    def _(c):
+        span = pl.ds(pl.multiple_of(c * size, size), size)
+        table = table_ref[span, :]
+        cumf, cumb = table[:, :heads], table[:, heads : 2 * heads]
+        wf = jnp.exp(cumf[size - 1 : size] - cumf) * table[:, 2 * heads : 3 * heads]
+        wb = jnp.exp(cumb[0:1] - cumb) * table[:, 3 * heads : 4 * heads]
+        signal = act_ref[span, :inner].astype(jnp.float32)
+        xf = (signal * spread(wf, inner)).astype(jnp.bfloat16)
+        xb = (signal * spread(wb, inner)).astype(jnp.bfloat16)
+        for g in range(groups):
+            cols = slice(g * width, (g + 1) * width)
+            entry = act_ref[span, inner + g * STATE_SIZE : inner + (g + 1) * STATE_SIZE]
+            turned = jnp.transpose(entry)
+            freshf_ref[c, :, cols] = jnp.dot(turned, xf[:, cols], preferred_element_type=jnp.float32)
+            freshb_ref[c, :, cols] = jnp.dot(turned, xb[:, cols], preferred_element_type=jnp.float32)
+
+    endf[...] = jnp.zeros_like(endf)
+    endb[...] = jnp.zeros_like(endb)
+
+    def total_decay(c, forward):
+        row = c * size + size - 1 if forward else c * size
+        at = 0 if forward else heads
+        return table_ref[pl.ds(row, 1), :][:, at : at + heads]
+
+    def wide(log_row):
+        return spread(jnp.exp(jnp.broadcast_to(log_row, (8, heads))), inner)
+
+    for c in range(chunks):
+        endf[...] = endf[...] * wide(total_decay(c, True))[0:1] + freshf_ref[c]
+        r = chunks - 1 - c
+        endb[...] = endb[...] * wide(total_decay(r, False))[0:1] + freshb_ref[r]
+    half = inner // 2
+    for forward, end, pack_ref in ((True, endf, packf_ref), (False, endb, packb_ref)):
+        logs = total_decay(0, forward)
+        for c in range(1, chunks):
+            logs = logs + total_decay(c, forward)
+        decay = wide(logs).astype(jnp.bfloat16)
+        for side in range(2):
+            cols = slice(side * half, (side + 1) * half)
+            pack_ref[side, :STATE_SIZE, :] = end[:, cols].astype(jnp.bfloat16)
+            pack_ref[side, STATE_SIZE:, :] = jnp.concatenate([decay, decay], axis=0)[:, cols]
+
+    @pl.when(has_high)
     def _():
-        half = inner // 2
-        for d, (end_ref, pack_ref) in enumerate(((endf_ref, packf_ref), (endb_ref, packb_ref))):
-            decay = spread(jnp.exp(logs[d]), inner).astype(jnp.bfloat16)
-            for side in range(2):
-                cols = slice(side * half, (side + 1) * half)
-                pack_ref[side, :STATE_SIZE, :] = end_ref[:, cols].astype(jnp.bfloat16)
-                pack_ref[side, STATE_SIZE:, :] = jnp.concatenate([decay, decay], axis=0)[:, cols]
+        for copy in copies(True):
+            copy.wait_send()
+
+    @pl.when(has_low)
+    def _():
+        for copy in copies(False):
+            copy.wait_send()
 
 
 def outputs_kernel(
-    head_size, inner, maps, act_ref, ldf_ref, ldb_ref, stf_ref, stb_ref, ldft_ref, ldbt_ref,
-    stft_ref, stbt_ref, ldball_ref, freshf_ref, freshb_ref, enter_ref, gate_ref, gain_ref,
+    head_size, inner, maps, act_ref, table_ref, turned_ref, tables_ref, freshf_ref, freshb_ref,
+    enter_ref, gate_ref, gain_ref,
     out_ref, carryf, enterb, y,
 ):
     step = pl.program_id(0)
@@ -155,17 +452,14 @@
         @pl.loop(0, chunks - 1)
         def _(k):
             at = chunks - 1 - k
-            part = ldball_ref[pl.ds(pl.multiple_of(at * size, size), size), :]
-            tot = jnp.exp(jnp.sum(part, axis=0, keepdims=True))
+            part = tables_ref[pl.ds(pl.multiple_of(at * size, size), 8), :]
+            tot = jnp.exp(part[0:1, heads : 2 * heads])
             tot = spread(jnp.broadcast_to(tot, (8, heads)), inner)[0:1]
             enterb[at - 1] = enterb[at] * tot + freshb_ref[at]
 
-    lower, upper = triangle(size, True), triangle(size, False)
-    cumf = exact_dot(lower, ldf_ref[...])
-    cumb = exact_dot(upper, ldb_ref[...])
-    cumft = exact_dot(ldft_ref[...], upper)
-    cumbt = exact_dot(ldbt_ref[...], lower)
-    stft, stbt = stft_ref[...], stbt_ref[...]
+    cumf, cumb = table_ref[:, :heads], table_ref[:, heads : 2 * heads]
+    cumft, cumbt = turned_ref[:heads, :], turned_ref[heads : 2 * heads, :]
+    stft, stbt = turned_ref[2 * heads : 3 * heads, :], turned_ref[3 * heads : 4 * heads, :]
     row = lax.broadcasted_iota(jnp.int32, (size, size), 0)
     column = lax.broadcasted_iota(jnp.int32, (size, size), 1)
     is_lower, is_diagonal = row >= column, row == column
@@ -316,7 +610,6 @@
     ratio = heads // key_heads
     values_at = key_heads * head_size
     flipped[...] = jnp.transpose(rim_ref[:, values_at:])
-    scale = head_size ** (-0.5)
     key_row = lax.broadcasted_iota(jnp.int32, (span, block), 0)
     query_col = lax.broadcasted_iota(jnp.int32, (span, block), 1)
     in_band = (key_row >= query_col) & (key_row <= query_col + 2 * WINDOW)
@@ -343,7 +636,7 @@
                 rim_ref[pl.ds(start, span), k * head_size : (k + 1) * head_size],
                 query_ref[pl.ds(start, block), h * head_size : (h + 1) * head_size],
                 (((1,), (1,)), ((), ())), preferred_element_type=jnp.float32,
-            ) * scale + bias[...]
+            ) + bias[...]
         for h in range(heads):
             top = jnp.maximum(jnp.max(scores[h], axis=0, keepdims=True), sink_ref[h])
             lifted = jnp.exp(scores[h] - top)
@@ -402,7 +695,9 @@
             pltpu.VMEM((2, STATE_SIZE, half), jnp.bfloat16),
             dma((2,)), dma((2,)), dma((2, hops)), dma((2, hops)), dma((2,)), dma((2,)),
         ],
-        compiler_params=pltpu.CompilerParams(collective_id=5, has_side_effects=True),
+        compiler_params=pltpu.CompilerParams(
+            collective_id=5, has_side_effects=True, vmem_limit_bytes=20 * MIB
+        ),
         cost_estimate=pl.CostEstimate(
             flops=4 * rows * span * width, bytes_accessed=4 * rows * width,
             transcendentals=rows * span * heads,
@@ -523,7 +818,9 @@
             pltpu.SemaphoreType.DMA((far, pieces)),
             pltpu.SemaphoreType.DMA((far, pieces)),
         ],
-        compiler_params=pltpu.CompilerParams(collective_id=3, has_side_effects=True),
+        compiler_params=pltpu.CompilerParams(
+            collective_id=3, has_side_effects=True, vmem_limit_bytes=24 * MIB
+        ),
         cost_estimate=pl.CostEstimate(
             flops=2 * total * depth * width, bytes_accessed=2 * depth * width, transcendentals=0
         ),
@@ -531,55 +828,54 @@
     )(attn_out, ssm_out, attn_weight, ssm_weight)
 
 
-def chunk_states(rimmed, taps, tap_count, inner, maps, decay, step):
-    rows = rimmed.shape[0] - 2 * HALO
-    total, heads, chunks = rimmed.shape[1], decay[0].shape[1], rows // CHUNK
-    small = pl.BlockSpec((CHUNK, heads), lambda i: (i, 0))
-    fresh = pl.BlockSpec((1, STATE_SIZE, inner), lambda i: (i, 0, 0))
-    packed = (2, STATE_SIZE + PACK_ROWS, inner // 2)
-    end = pl.BlockSpec(packed, lambda i: (0, 0, 0))
-    fresh_shape = jax.ShapeDtypeStruct((chunks, STATE_SIZE, inner), jnp.float32)
-    end_shape = jax.ShapeDtypeStruct(packed, jnp.bfloat16)
+def convolve(rows, keyed, taps, table, tap_count, inner, maps, heads):
+    total, width = rows.shape
+    chunks = total // CHUNK
+    count = lax.axis_size("sp")
+    vmem = pl.BlockSpec(memory_space=pltpu.VMEM)
+    fresh = jax.ShapeDtypeStruct((chunks, STATE_SIZE, inner), jnp.float32)
+    pack = jax.ShapeDtypeStruct((2, STATE_SIZE + PACK_ROWS, inner // 2), jnp.bfloat16)
     return pl.pallas_call(
-        functools.partial(states_kernel, tap_count, inner, maps),
-        grid=(chunks,),
-        in_specs=[
-            pl.BlockSpec(rimmed.shape, lambda i: (0, 0)),
-            pl.BlockSpec(taps.shape, lambda i: (0, 0)),
-            small, small, small, small,
-        ],
-        out_specs=[pl.BlockSpec((CHUNK, total), lambda i: (i, 0)), fresh, fresh, end, end],
+        functools.partial(convolve_kernel, tap_count, inner, maps, heads, count),
+        in_specs=[vmem] * 4,
+        out_specs=[vmem] * 6,
         out_shape=[
-            jax.ShapeDtypeStruct((rows, total), jnp.bfloat16),
-            fresh_shape, fresh_shape, end_shape, end_shape,
+            jax.ShapeDtypeStruct((total, width), jnp.bfloat16), fresh, fresh, pack, pack,
+            jax.ShapeDtypeStruct((total + 2 * WINDOW, keyed.shape[1]), jnp.bfloat16),
         ],
         scratch_shapes=[
-            pltpu.VMEM((CHUNK + 2 * HALO, total), jnp.float32),
-            pltpu.VMEM((8, inner), jnp.float32),
+            pltpu.VMEM((CHUNK + 2 * HALO, width), jnp.float32),
+            pltpu.VMEM((HALO, width), jnp.bfloat16),
+            pltpu.VMEM((HALO, width), jnp.bfloat16),
+            pltpu.VMEM((WINDOW, keyed.shape[1]), jnp.bfloat16),
+            pltpu.VMEM((WINDOW, keyed.shape[1]), jnp.bfloat16),
             pltpu.VMEM((STATE_SIZE, inner), jnp.float32),
             pltpu.VMEM((STATE_SIZE, inner), jnp.float32),
-            pltpu.VMEM((2, 8, heads), jnp.float32),
+            pltpu.SemaphoreType.DMA((4,)),
+            pltpu.SemaphoreType.DMA((4,)),
         ],
+        compiler_params=pltpu.CompilerParams(
+            collective_id=4, has_side_effects=True, vmem_limit_bytes=24 * MIB
+        ),
         cost_estimate=pl.CostEstimate(
-            flops=8 * rows * inner * STATE_SIZE, bytes_accessed=16 * rows * inner,
-            transcendentals=rows * total,
+            flops=8 * total * inner * STATE_SIZE, bytes_accessed=8 * total * inner,
+            transcendentals=total * width,
         ),
-        name="chunk_states",
-    )(rimmed, taps, *decay, *step)
-
-
-def chunk_outputs(head_size, inner, maps, act, decay, step, fresh, incoming, gate, gain):
+        name="convolve",
+    )(rows, keyed, taps, table)
+
+
+def chunk_outputs(head_size, inner, maps, heads, act, table, turned, fresh, incoming, gate, gain):
     rows, total = act.shape
-    heads, chunks = decay[0].shape[1], rows // CHUNK
-    small = pl.BlockSpec((CHUNK, heads), lambda i: (i, 0))
-    turned = pl.BlockSpec((heads, CHUNK), lambda i: (0, i))
+    chunks = rows // CHUNK
     return pl.pallas_call(
         functools.partial(outputs_kernel, head_size, inner, maps),
         grid=(chunks,),
         in_specs=[
             pl.BlockSpec((CHUNK, total), lambda i: (i, 0)),
-            small, small, small, small, turned, turned, turned, turned,
-            pl.BlockSpec((rows, heads), lambda i: (0, 0)),
+            pl.BlockSpec((CHUNK, 128), lambda i: (i, 0)),
+            pl.BlockSpec((128, CHUNK), lambda i: (0, i)),
+            pl.BlockSpec((rows, 128), lambda i: (0, 0)),
             pl.BlockSpec((1, STATE_SIZE, inner), lambda i: (i, 0, 0)),
             pl.BlockSpec((chunks, STATE_SIZE, inner), lambda i: (0, 0, 0)),
             pl.BlockSpec(incoming.shape, lambda i: (0, 0, 0, 0)),
@@ -598,10 +894,7 @@
             transcendentals=rows * CHUNK * heads,
         ),
         name="chunk_outputs",
-    )(
-        act, *decay, *step, decay[0].T, decay[1].T, step[0].T, step[1].T, decay[1],
-        fresh[0], fresh[1], incoming, gate, gain,
-    )
+    )(act, table, turned, table, fresh[0], fresh[1], incoming, gate, gain)
 
 
 def local(
@@ -626,52 +919,27 @@
     attn_out_weight,
     ssm_out_weight,
 ):
-    row_total = tokens.shape[0]
-    seq_first = lax.axis_index("sp") * row_total
-    positions = seq_first + jnp.arange(row_total, dtype=jnp.int32)
-    normed = rms_rows(tokens.astype(jnp.float32), norm_gain.astype(jnp.float32)).astype(
-        jnp.bfloat16
+    head_size = query_gain.shape[0]
+    query, keyed, rows, gate_rows, table, turned = project_all(
+        tokens, norm_gain, inner_weight, input_map, output_map, key_weight, value_weight,
+        query_weight, gate_weight, step_weight, query_gain, key_gain, decay_rate, decay_jump,
     )
-
-    def project(weight):
-        result = jnp.dot(normed, weight, preferred_element_type=jnp.float32)
-        return lax.optimization_barrier(result.astype(jnp.bfloat16))
-
-    head_size = query_gain.shape[0]
-    query = project(query_weight).reshape(row_total, -1, head_size)
-    keyed = project(key_weight).reshape(row_total, -1, head_size)
-    value = project(value_weight)
-    query = rotate(rms_rows(query.astype(jnp.float32), query_gain), positions).astype(jnp.bfloat16)
-    keyed = rotate(rms_rows(keyed.astype(jnp.float32), key_gain), positions).astype(jnp.bfloat16)
-    key_heads = keyed.shape[1]
-    packed = jnp.concatenate([keyed.reshape(row_total, -1), value], axis=1)
-    rimmed_keys = extended(packed, (("sp", 0),), WINDOW)
-    inner_rows = project(inner_weight)
-    inner_width = inner_rows.shape[1]
-    map_width = input_map.shape[1]
-    carried_in = jnp.concatenate([inner_rows, project(input_map), project(output_map)], axis=1)
-    tap_count = conv_inner.shape[0]
+    tap_count, inner = conv_inner.shape
+    maps = input_map.shape[1]
+    heads = inner // head_size
+    key_heads = key_weight.shape[1] // head_size
     conv_table = jnp.concatenate([conv_inner, conv_pair.reshape(tap_count, -1)], axis=1).astype(
         jnp.float32
     )
-    rimmed_rows = extended(carried_in, (("sp", 0),), HALO)
-    step_rows = project(step_weight.reshape(step_weight.shape[0], -1))
-    step = jax.nn.softplus(step_rows.astype(jnp.float32))
-    log_decay = -decay_rate.reshape(1, -1) * step + decay_jump.reshape(row_total, -1)
-    heads_here = inner_width // head_size
-    steps = (step[:, :heads_here], step[:, heads_here:])
-    decays = (log_decay[:, :heads_here], log_decay[:, heads_here:])
-    act, fresh_forward, fresh_backward, pack_forward, pack_backward = chunk_states(
-        rimmed_rows, conv_table, tap_count, inner_width, map_width, decays, steps
+    act, fresh_forward, fresh_backward, pack_forward, pack_backward, rimmed = convolve(
+        rows, keyed, conv_table, table, tap_count, inner, maps, heads
     )
     attn_out, incoming = middle(
-        query.reshape(row_total, -1), rimmed_keys, sink_logit, pack_forward, pack_backward,
-        head_size, key_heads,
+        query, rimmed, sink_logit, pack_forward, pack_backward, head_size, key_heads
     )
-    gate_rows = project(gate_weight)
     ssm_out = chunk_outputs(
-        head_size, inner_width, map_width, act, decays, steps, (fresh_forward, fresh_backward),
-        incoming, gate_rows, inner_gain.astype(jnp.float32)[None, :],
+        head_size, inner, maps, heads, act, table, turned, (fresh_forward, fresh_backward), incoming,
+        gate_rows, inner_gain.astype(jnp.float32)[None, :],
     )
     return combine(attn_out, ssm_out, attn_out_weight, ssm_out_weight)
 

time: 179 us -> 144 us (0.80)
  matrix products: 26.9 us -> 0 us
  Pallas kernels: 102 us -> 126 us
  other arithmetic: 14.5 us -> 1.26 us
  starting transfers between devices: 12.9 us -> 0 us
  local copies, waits for them, and re-layouts: 21.6 us -> 16.5 us
    pallas_call x1 -> x2, Pallas kernels: 18.3 us -> 51.4 us  [the longest x1 32.9 us: project_all(): pl.pallas_call(functools.partial(project_kernel, head_size, heads, key_wi...]
    dot_general x8 -> x0, matrix products: 26.9 us -> none  [project(): result = jnp.dot(normed, weight, preferred_element_type=jnp.float32)]
    ppermute x4 -> x0, starting transfers between devices: 12.9 us -> none  [the longest x2 10.3 us: extended(): lax.ppermute(lax.slice_in_dim(block, block.shape[dim] - width, None, axis...]
    transpose x5 -> x0, local copies, waits for them, and re-layouts: 9.68 us -> none  [the longest x2 4.16 us: chunk_outputs(): step[1]]
    concatenate x4 -> x0, other arithmetic: 5.5 us -> none  [the longest x2 5.41 us: extended(): block = jnp.concatenate([low, block, high], axis=dim)]
    unnamed x54 -> x36, local copies, waits for them, and re-layouts: 8.3 us -> 13.5 us
    pallas_call x1, Pallas kernels: 32.8 us -> 27.9 us  [combine(): pl.pallas_call(functools.partial(combine_kernel, count), in_specs=[vmem]...]
    pallas_call x1, Pallas kernels: 33.2 us -> 28.9 us  [middle(): pl.pallas_call(functools.partial(middle_kernel, head_size, key_heads, cou...]
  transfers between devices with their start and end apart: 4 -> 0, of which waited for: 0 -> 0; matrix products, arithmetic and copies ran while one was open for 25% -> 0% of each run, Pallas kernels for 10% -> 0%
where the time goes in v3:
time: 144 us; the launch traced here: 143 us
  Pallas kernels  126 us (88%)
  local copies, waits for them, and re-layouts  16.5 us (11%)
    pallas_call x1, Pallas kernels, project_all(): pl.pallas_call(functools.partial(project_kernel, head_size, heads, key_wi...  32.9 us
    pallas_call x1, Pallas kernels, middle(): pl.pallas_call(functools.partial(middle_kernel, head_size, key_heads, cou...  28.9 us
    pallas_call x1, Pallas kernels, combine(): pl.pallas_call(functools.partial(combine_kernel, count), in_specs=[vmem]...  27.9 us
    pallas_call x1, Pallas kernels, convolve(): pl.pallas_call(functools.partial(convolve_kernel, tap_count, inner, maps,...  18.4 us
    pallas_call x1, Pallas kernels, chunk_outputs(): pl.pallas_call(functools.partial(outputs_kernel, head_size, inner, maps),...  17.4 us
    unnamed x36, local copies, waits for them, and re-layouts  13.5 us

profile of v3, /device:TPU:0, one launch (start us, length us, event | category | flops | bytes accessed | tf_op | source)
XLA Modules:
  0.0 143.5 jit_solution(17850637726309616643)
XLA Ops:
  0.0 0.7 broadcast_multiply_fusion
  0.7 0.1 mul.12
  0.7 0.7 tile.7
  1.4 0.1 tile.8
  1.5 0.8 reshape.20
  2.2 1.4 concatenate.6
  3.7 0.0 copy-start.10
  3.7 0.9 copy-done.10
  4.6 0.0 copy-start.11
  4.6 0.9 copy-done.11
  5.5 0.0 copy-start.15
  5.5 0.0 copy-start.14
  5.5 32.9 %project.1 = (bf16[1024,512]{1,0:T(8,128)(2,1)}, bf16[1024,256]{1,0:T(8,128)(2,1)S(1)}, bf16[1024,1536]{1,0:T(8,128)(2,1)}, bf16[1024,1024]{1,0:T(8,128)(2,1)}, ...) custom-call(bf16[1024,2048]{1,0:T(8,128)(2,1)} %tokens_ref.1, bf16[2048,1024]{1,0:T(8,128)(2,1)} %inner_hbm.1, ...), custom_call_target="tpu_custom_call" | custom-call | flops 13958643712 | bytes 17825792 | tf_op jit(solution)/shard_map/project/pallas_call | solution.py:245
  38.4 0.0 copy-start
  38.5 0.0 copy-start.7
  38.5 0.0 copy-start.12
  38.5 0.0 copy-done.15
  38.5 0.0 copy-done.14
  38.5 0.0 copy-start.4
  38.5 2.2 %copy-done.4 = bf16[1024,1536]{1,0:T(8,128)(2,1)S(1)} copy-done((bf16[1024,1536]{1,0:T(8,128)(2,1)S(1)}, bf16[1024,1536]{1,0:T(8,128)(2,1)}, u32[]{:S(2)}) %copy-start.4) | copy-done | bytes 3145752
  40.7 0.0 copy-start.13
  40.8 0.0 copy-start.16
  40.8 18.4 %convolve.1 = (bf16[1024,1536]{1,0:T(8,128)(2,1)S(1)}, f32[8,128,1024]{2,1,0:T(8,128)S(1)}, f32[8,128,1024]{2,1,0:T(8,128)S(1)}, bf16[2,144,512]{2,1,0:T(8,128)(...) custom-call(bf16[1024,1536]{1,0:T(8,128)(2,1)S(1)} %copy-done.4, ...), custom_call_target="tpu_custom_call" | custom-call | flops 1073741824 | bytes 8388608 | tf_op jit(solution)/shard_map/convolve/pallas_call | solution.py:838
  59.2 0.0 copy-start.2
  59.2 2.0 %copy-done.2 = f32[8,128,1024]{2,1,0:T(8,128)} copy-done((f32[8,128,1024]{2,1,0:T(8,128)}, f32[8,128,1024]{2,1,0:T(8,128)S(1)}, u32[]{:S(2)}) %copy-start.2) | copy-done | bytes 4194328
  61.2 0.0 copy-start.3
  61.2 1.7 %copy-done.3 = bf16[1024,1536]{1,0:T(8,128)(2,1)} copy-done((bf16[1024,1536]{1,0:T(8,128)(2,1)}, bf16[1024,1536]{1,0:T(8,128)(2,1)S(1)}, u32[]{:S(2)}) %copy-start.3) | copy-done | bytes 3145752
  62.9 0.0 copy-start.1
  62.9 0.0 copy-done.12
  62.9 0.0 copy-done.13
  62.9 28.9 %middle.1 = (bf16[1024,512]{1,0:T(8,128)(2,1)S(1)}, f32[2,2,128,512]{3,2,1,0:T(8,128)S(1)}) custom-call(f32[8]{0:T(128)S(1)} %copy-done.12, bf16[1024,512]{1,0:T(8,128)(2,1)S(1)} %copy-done.13, bf16[1280,256]{1,0:T(8,128)(2,1)S(1)} %get-tuple-element.23.rim_ref, bf16[2,144,512]{2,1,0:T(8,128)(2,1)S(1)} %get-tuple-element.24.packf_ref, ...), custom_call_target="tpu_custom_call" | custom-call | flops 805306368 | bytes 2097152 | tf_op jit(solution)/shard_map/middle/pallas_call | solution.py:674
  91.8 0.0 copy-done
  91.8 0.0 copy-done.7
  91.8 0.0 copy-start.6
  91.8 1.0 copy-done.6
  92.8 0.0 copy-done.1
  92.8 0.0 copy-done.16
  92.8 0.6 broadcast_in_dim.11
  93.4 0.0 copy-start.9
  93.4 17.4 %chunk_outputs.1.ssm_ref = bf16[1024,1024]{1,0:T(8,128)(2,1)} custom-call(bf16[1024,1536]{1,0:T(8,128)(2,1)} %copy-done.3, f32[1024,128]{1,0:T(8,128)} %copy-done, f32[128,1024]{1,0:T(8,128)} %copy-done.7, f32[1024,128]{1,0:T(8,128)} %copy-done, f32[8,128,1024]{2,1,0:T(8,128)} %copy-done.1, f32[8,128,1024]{2,1,0:T(8,128)} %copy-done.2, ...), custom_call_target="tpu_custom_call" | custom-call | flops 1073741824 | bytes 16777216 | tf_op jit(solution)/shard_map/chunk_outputs/pallas_call | solution.py:871
  110.8 0.0 copy-done.9
  110.8 0.0 copy-start.5
  110.8 1.6 %copy-done.5 = bf16[1024,1024]{1,0:T(8,128)(2,1)S(1)} copy-done((bf16[1024,1024]{1,0:T(8,128)(2,1)S(1)}, bf16[1024,1024]{1,0:T(8,128)(2,1)}, u32[]{:S(2)}) %copy-start.5) | copy-done | bytes 2097176
  112.4 0.0 copy-start.8
  112.4 2.2 %copy-done.8 = bf16[1024,2048]{1,0:T(8,128)(2,1)S(1)} copy-done((bf16[1024,2048]{1,0:T(8,128)(2,1)S(1)}, bf16[1024,2048]{1,0:T(8,128)(2,1)}, u32[]{:S(2)}) %copy-start.8) | copy-done | bytes 4194328
  114.6 27.9 %combine.1 = bf16[256,2048]{1,0:T(8,128)(2,1)S(1)} custom-call(bf16[1024,512]{1,0:T(8,128)(2,1)S(1)} %get-tuple-element.26.attn_ref, bf16[1024,1024]{1,0:T(8,128)(2,1)S(1)} %copy-done.5, bf16[512,2048]{1,0:T(8,128)(2,1)S(1)} %copy-done.9, bf16[1024,2048]{1,0:T(8,128)(2,1)S(1)} %copy-done.8), custom_call_target="tpu_custom_call" | custom-call | flops 6442450944 | bytes 6291456 | tf_op jit(solution)/shard_map/combine/pallas_call | solution.py:804
  142.5 1.0 copy.25
  (4 shorter events, 0.0 us)
Async XLA Ops:
  3.7 0.9 copy-start.10
  4.6 0.9 copy-start.11
  5.5 33.0 %copy-start.15 = (bf16[5,2,256]{2,1,0:T(2,128)(2,1)S(1)}, bf16[5,2,256]{2,1,0:T(2,128)(2,1)}, u32[]{:S(2)}) copy-start(bf16[5,2,256]{2,1,0:T(2,128)(2,1)} %param.36) | copy-start | bytes 15364
  5.5 33.0 %copy-start.14 = (bf16[5,1024]{1,0:T(8,128)(2,1)S(1)}, bf16[5,1024]{1,0:T(8,128)(2,1)}, u32[]{:S(2)}) copy-start(bf16[5,1024]{1,0:T(8,128)(2,1)} %param.35) | copy-start | bytes 30724
  38.4 53.4 %copy-start = (f32[1024,128]{1,0:T(8,128)}, f32[1024,128]{1,0:T(8,128)S(1)}, u32[]{:S(2)}) copy-start(f32[1024,128]{1,0:T(8,128)S(1)} %get-tuple-element.22.table_ref.tables_ref) | copy-start | bytes 1572868
  38.5 53.4 %copy-start.7 = (f32[128,1024]{1,0:T(8,128)}, f32[128,1024]{1,0:T(8,128)S(1)}, u32[]{:S(2)}) copy-start(f32[128,1024]{1,0:T(8,128)S(1)} %get-tuple-element.28.turned_ref) | copy-start | bytes 1572868
  38.5 24.4 %copy-start.12 = (f32[8]{0:T(128)S(1)}, f32[8]{0:T(128)}, u32[]{:S(2)}) copy-start(f32[8]{0:T(128)} %sink_ref.1) | copy-start | bytes 100
  38.5 2.2 %copy-start.4 = (bf16[1024,1536]{1,0:T(8,128)(2,1)S(1)}, bf16[1024,1536]{1,0:T(8,128)(2,1)}, u32[]{:S(2)}) copy-start(bf16[1024,1536]{1,0:T(8,128)(2,1)} %get-tuple-element.20.rows_ref) | copy-start | bytes 9437188
  40.7 22.1 %copy-start.13 = (bf16[1024,512]{1,0:T(8,128)(2,1)S(1)}, bf16[1024,512]{1,0:T(8,128)(2,1)}, u32[]{:S(2)}) copy-start(bf16[1024,512]{1,0:T(8,128)(2,1)} %get-tuple-element.19.query_ref) | copy-start | bytes 3145732
  40.8 52.1 %copy-start.16 = (bf16[1024]{0:T(1024)(128)(2,1)S(1)}, bf16[1024]{0:T(1024)(128)(2,1)}, u32[]{:S(2)}) copy-start(bf16[1024]{0:T(1024)(128)(2,1)} %param.39) | copy-start | bytes 6148
  59.2 2.0 %copy-start.2 = (f32[8,128,1024]{2,1,0:T(8,128)}, f32[8,128,1024]{2,1,0:T(8,128)S(1)}, u32[]{:S(2)}) copy-start(f32[8,128,1024]{2,1,0:T(8,128)S(1)} %get-tuple-element.30.freshb_ref) | copy-start | bytes 12582916
  61.2 1.7 %copy-start.3 = (bf16[1024,1536]{1,0:T(8,128)(2,1)}, bf16[1024,1536]{1,0:T(8,128)(2,1)S(1)}, u32[]{:S(2)}) copy-start(bf16[1024,1536]{1,0:T(8,128)(2,1)S(1)} %get-tuple-element.27.act_ref) | copy-start | bytes 9437188
  62.9 29.9 %copy-start.1 = (f32[8,128,1024]{2,1,0:T(8,128)}, f32[8,128,1024]{2,1,0:T(8,128)S(1)}, u32[]{:S(2)}) copy-start(f32[8,128,1024]{2,1,0:T(8,128)S(1)} %get-tuple-element.29.freshf_ref) | copy-start | bytes 12582916
  91.8 1.0 copy-start.6
  93.4 17.4 %copy-start.9 = (bf16[512,2048]{1,0:T(8,128)(2,1)S(1)}, bf16[512,2048]{1,0:T(8,128)(2,1)}, u32[]{:S(2)}) copy-start(bf16[512,2048]{1,0:T(8,128)(2,1)} %attn_w_ref.1) | copy-start | bytes 6291460
  110.8 1.6 %copy-start.5 = (bf16[1024,1024]{1,0:T(8,128)(2,1)S(1)}, bf16[1024,1024]{1,0:T(8,128)(2,1)}, u32[]{:S(2)}) copy-start(bf16[1024,1024]{1,0:T(8,128)(2,1)} %chunk_outputs.1.ssm_ref) | copy-start | bytes 6291460
  112.4 2.2 %copy-start.8 = (bf16[1024,2048]{1,0:T(8,128)(2,1)S(1)}, bf16[1024,2048]{1,0:T(8,128)(2,1)}, u32[]{:S(2)}) copy-start(bf16[1024,2048]{1,0:T(8,128)(2,1)} %ssm_w_ref.1) | copy-start | bytes 12582916

commit v4 on v3

--- a/solution.py
+++ b/solution.py
@@ -16,9 +16,12 @@
 NORM_EPS = 1e-05
 ROPE_BASE = 500000.0
 NEG_FILL = -1e30
-PIECE = 256
 TILE = 512
 MIB = 1 << 20
+PROJECT_MIB = 52
+CONVOLVE_MIB = 32
+MIDDLE_MIB = 30
+FINISH_MIB = 28
 PACK_ROWS = 16
 MESH = pl.DeviceIdType.MESH
 
@@ -46,8 +49,8 @@
 
 def project_kernel(
     head_size, heads, key_width, tokens_ref, inner_hbm, in_hbm, out_hbm, key_hbm, value_hbm,
-    query_hbm, gate_hbm, step_ref, small_ref, jump_ref, query_ref, keyed_ref, rows_ref, gate_ref,
-    table_ref, turned_ref, tokens, normed, inner_w, in_w, out_w, keyed_w, query_w, gate_w, raw,
+    query_hbm, gate_hbm, step_hbm, jump_hbm, small_ref, query_ref, keyed_ref, rows_ref, gate_ref,
+    table_ref, turned_ref, step_ref, jump_ref, tokens, normed, inner_w, in_w, out_w, keyed_w, query_w, gate_w, raw,
     cosine, sine, token_sems, weight_sems,
 ):
     total, depth = tokens.shape
@@ -67,13 +70,14 @@
         key_w, value_w = keyed_w.at[0], keyed_w.at[1]
     weights = (
         (key_hbm, key_w), (value_hbm, value_w), (query_hbm, query_w), (in_hbm, in_w),
-        (out_hbm, out_w), (inner_hbm, inner_w), (gate_hbm, gate_w),
+        (out_hbm, out_w), (inner_hbm, inner_w), (gate_hbm, gate_w), (step_hbm, step_ref),
+        (jump_hbm, jump_ref),
     )
     loads = [
         pltpu.make_async_copy(source, target, weight_sems.at[i])
         for i, (source, target) in enumerate(weights)
     ]
-    for move in moves + loads:
+    for move in moves + loads[7:] + loads[:7]:
         move.start()
     lanes = depth // 128
     frequency, sign = small_ref[lanes + 2 : lanes + 3], small_ref[lanes + 3 : lanes + 4]
@@ -123,6 +127,8 @@
         else:
             pl.loop(0, count)(tile)
 
+    loads[7].wait()
+    loads[8].wait()
     raw[:, 2 * heads :] = jnp.zeros((total, 128 - 2 * heads), jnp.float32)
     raw[:, : 2 * heads] = lax.dot_general(
         normed[...], step_ref[...], (((1,), (1,)), ((), ())), preferred_element_type=jnp.float32
@@ -244,7 +250,7 @@
 
     return pl.pallas_call(
         functools.partial(project_kernel, head_size, heads, key_width),
-        in_specs=[whole] * 8 + [vmem] * 3,
+        in_specs=[whole] * 10 + [vmem],
         out_specs=[vmem] * 6,
         out_shape=[
             shape(total, width), shape(total, 2 * key_width), shape(total, inner + 2 * maps),
@@ -252,25 +258,26 @@
             shape(128, total, kind=jnp.float32),
         ],
         scratch_shapes=[
+            room(*turned_step.shape), room(*turned_jump.shape, kind=jnp.float32),
             room(total, depth), room(total, depth), room(*inner_weight.shape),
             room(*input_map.shape), room(*output_map.shape), room(*keyed_shape),
             room(*query_weight.shape), room(*gate_weight.shape),
             room(total, 128, kind=jnp.float32), room(total, 128, kind=jnp.float32),
             room(total, 128, kind=jnp.float32),
-            pltpu.SemaphoreType.DMA((8,)), pltpu.SemaphoreType.DMA((7,)),
+            pltpu.SemaphoreType.DMA((8,)), pltpu.SemaphoreType.DMA((9,)),
         ],
-        compiler_params=pltpu.CompilerParams(vmem_limit_bytes=52 * MIB),
+        compiler_params=pltpu.CompilerParams(vmem_limit_bytes=PROJECT_MIB * MIB),
         cost_estimate=pl.CostEstimate(
             flops=2 * total * depth * columns, bytes_accessed=2 * depth * (columns + total),
             transcendentals=total * 128,
         ),
         name="project",
-    )(tokens, *big, turned_step, small, turned_jump)
+    )(tokens, *big, turned_step, turned_jump, small)
 
 
 def convolve_kernel(
     tap_count, inner, maps, heads, count, rows_ref, keyed_ref, taps_ref, table_ref, act_ref,
-    freshf_ref, freshb_ref, packf_ref, packb_ref, rim_ref, spare, low_rows, high_rows, low_keys,
+    local_ref, reach_ref, packf_ref, packb_ref, rim_ref, freshf_ref, freshb_ref, spare, low_rows, high_rows, low_keys,
     high_keys, endf, endb, sends, receives,
 ):
     me = lax.axis_index("sp")
@@ -406,15 +413,19 @@
     def wide(log_row):
         return spread(jnp.exp(jnp.broadcast_to(log_row, (8, heads))), inner)
 
+    logsf, logsb = jnp.zeros((1, heads), jnp.float32), jnp.zeros((1, heads), jnp.float32)
     for c in range(chunks):
+        local_ref[0, c] = endf[...].astype(jnp.bfloat16)
+        reach_ref[0, c] = wide(logsf)
+        logsf = logsf + total_decay(c, True)
         endf[...] = endf[...] * wide(total_decay(c, True))[0:1] + freshf_ref[c]
         r = chunks - 1 - c
+        local_ref[1, r] = endb[...].astype(jnp.bfloat16)
+        reach_ref[1, r] = wide(logsb)
+        logsb = logsb + total_decay(r, False)
         endb[...] = endb[...] * wide(total_decay(r, False))[0:1] + freshb_ref[r]
     half = inner // 2
-    for forward, end, pack_ref in ((True, endf, packf_ref), (False, endb, packb_ref)):
-        logs = total_decay(0, forward)
-        for c in range(1, chunks):
-            logs = logs + total_decay(c, forward)
+    for logs, end, pack_ref in ((logsf, endf, packf_ref), (logsb, endb, packb_ref)):
         decay = wide(logs).astype(jnp.bfloat16)
         for side in range(2):
             cols = slice(side * half, (side + 1) * half)
@@ -432,91 +443,9 @@
             copy.wait_send()
 
 
-def outputs_kernel(
-    head_size, inner, maps, act_ref, table_ref, turned_ref, tables_ref, freshf_ref, freshb_ref,
-    enter_ref, gate_ref, gain_ref,
-    out_ref, carryf, enterb, y,
-):
-    step = pl.program_id(0)
-    chunks = pl.num_programs(0)
-    size = act_ref.shape[0]
-    heads = inner // head_size
-
-    @pl.when(step == 0)
-    def _():
-        half = inner // 2
-        for side in range(2):
-            carryf[:, side * half : (side + 1) * half] = enter_ref[0, side]
-            enterb[chunks - 1, :, side * half : (side + 1) * half] = enter_ref[1, side]
-
-        @pl.loop(0, chunks - 1)
-        def _(k):
-            at = chunks - 1 - k
-            part = tables_ref[pl.ds(pl.multiple_of(at * size, size), 8), :]
-            tot = jnp.exp(part[0:1, heads : 2 * heads])
-            tot = spread(jnp.broadcast_to(tot, (8, heads)), inner)[0:1]
-            enterb[at - 1] = enterb[at] * tot + freshb_ref[at]
-
-    cumf, cumb = table_ref[:, :heads], table_ref[:, heads : 2 * heads]
-    cumft, cumbt = turned_ref[:heads, :], turned_ref[heads : 2 * heads, :]
-    stft, stbt = turned_ref[2 * heads : 3 * heads, :], turned_ref[3 * heads : 4 * heads, :]
-    row = lax.broadcasted_iota(jnp.int32, (size, size), 0)
-    column = lax.broadcasted_iota(jnp.int32, (size, size), 1)
-    is_lower, is_diagonal = row >= column, row == column
-    groups = maps // STATE_SIZE
-    width = inner // groups
-    group_heads = heads // groups
-    expf = spread(jnp.exp(cumf), inner)
-    expb = spread(jnp.exp(cumb), inner)
-    lane = lax.broadcasted_iota(jnp.int32, (size, 2 * head_size), 1)
-    for g in range(groups):
-        cols = slice(g * width, (g + 1) * width)
-        entry = act_ref[:, inner + g * STATE_SIZE : inner + (g + 1) * STATE_SIZE]
-        leave = act_ref[:, inner + maps + g * STATE_SIZE : inner + maps + (g + 1) * STATE_SIZE]
-        crossed = lax.dot_general(
-            leave, entry, (((1,), (1,)), ((), ())), preferred_element_type=jnp.float32
-        )
-        y[:, cols] = (
-            jnp.dot(leave, carryf[:, cols].astype(jnp.bfloat16), preferred_element_type=jnp.float32)
-            * expf[:, cols]
-            + jnp.dot(
-                leave, enterb[step, :, cols].astype(jnp.bfloat16),
-                preferred_element_type=jnp.float32,
-            )
-            * expb[:, cols]
-        )
-        for pair in range(group_heads // 2):
-            mats = []
-            base = g * group_heads + 2 * pair
-            for h in (base, base + 1):
-                gap = jnp.where(
-                    is_lower,
-                    cumf[:, h : h + 1] - cumft[h : h + 1, :],
-                    cumb[:, h : h + 1] - cumbt[h : h + 1, :],
-                )
-                sf, sb = stft[h : h + 1, :], stbt[h : h + 1, :]
-                amount = jnp.where(is_diagonal, sf + sb, jnp.where(is_lower, sf, sb))
-                mats.append((crossed * jnp.exp(gap) * amount).astype(jnp.bfloat16))
-            two = slice(base * head_size, (base + 2) * head_size)
-            x = act_ref[:, two]
-            zero = jnp.zeros_like(x)
-            stacked = jnp.concatenate(
-                [jnp.where(lane < head_size, x, zero), jnp.where(lane < head_size, zero, x)], axis=0
-            )
-            y[:, two] += jnp.dot(
-                jnp.concatenate(mats, axis=1), stacked, preferred_element_type=jnp.float32
-            )
-        gate = gate_ref[:, cols].astype(jnp.float32)
-        mixed = y[:, cols] * (gate / (1.0 + jnp.exp(-gate)))
-        scale = lax.rsqrt(jnp.mean(mixed * mixed, axis=1, keepdims=True) + NORM_EPS)
-        out_ref[:, cols] = (mixed * scale * gain_ref[:, cols]).astype(jnp.bfloat16)
-    totf = spread(jnp.exp(jnp.broadcast_to(cumf[size - 1 : size], (8, heads))), inner)[0:1]
-    carryf[...] = carryf[...] * totf + freshf_ref[0]
-
-
 def middle_kernel(
-    head_size, key_heads, count, sink_ref, query_ref, rim_ref, packf_ref, packb_ref, out_ref,
-    enter_ref, scores, raised, bottoms, flipped, turned, bias, mate_in, pair_out, pair_in, gathered,
+    head_size, key_heads, count, inner, maps, sink_ref, query_ref, rim_ref, packf_ref, packb_ref,
+    act_ref, table_ref, turned_ref, out_ref, enter_ref, inside_ref, scores, raised, bottoms, flipped, turned, bias, mate_in, pair_out, pair_in, gathered,
     reach, back_out, back_in, mate_send, mate_recv, pair_send, pair_recv, back_send, back_recv,
 ):
     me = lax.axis_index("sp")
@@ -614,8 +543,55 @@
     query_col = lax.broadcasted_iota(jnp.int32, (span, block), 1)
     in_band = (key_row >= query_col) & (key_row <= query_col + 2 * WINDOW)
 
+    groups = maps // STATE_SIZE
+    ssm_heads = inner // head_size
+    chunk_row = lax.broadcasted_iota(jnp.int32, (CHUNK, CHUNK), 0)
+    chunk_col = lax.broadcasted_iota(jnp.int32, (CHUNK, CHUNK), 1)
+    is_lower, is_diagonal = chunk_row >= chunk_col, chunk_row == chunk_col
+    lane = lax.broadcasted_iota(jnp.int32, (CHUNK, 2 * head_size), 1)
+
+    def inside_chunk(c):
+        at = pl.multiple_of(c * CHUNK, CHUNK)
+        span = pl.ds(at, CHUNK)
+        table = table_ref[span, :]
+        for g in range(groups):
+            entry = act_ref[span, inner + g * STATE_SIZE : inner + (g + 1) * STATE_SIZE]
+            leave = act_ref[
+                span, inner + maps + g * STATE_SIZE : inner + maps + (g + 1) * STATE_SIZE
+            ]
+            crossed = lax.dot_general(
+                leave, entry, (((1,), (1,)), ((), ())), preferred_element_type=jnp.float32
+            )
+            each = ssm_heads // groups
+            for pair in range(each // 2):
+                mats = []
+                base = g * each + 2 * pair
+                for h in (base, base + 1):
+                    low, high = h, ssm_heads + h
+                    gap = jnp.where(
+                        is_lower,
+                        table[:, low : low + 1] - turned_ref[low : low + 1, span],
+                        table[:, high : high + 1] - turned_ref[high : high + 1, span],
+                    )
+                    sf = turned_ref[2 * ssm_heads + h : 2 * ssm_heads + h + 1, span]
+                    sb = turned_ref[3 * ssm_heads + h : 3 * ssm_heads + h + 1, span]
+                    amount = jnp.where(is_diagonal, sf + sb, jnp.where(is_lower, sf, sb))
+                    mats.append((crossed * jnp.exp(gap) * amount).astype(jnp.bfloat16))
+                two = slice(base * head_size, (base + 2) * head_size)
+                x = act_ref[span, two]
+                zero = jnp.zeros_like(x)
+                stacked = jnp.concatenate(
+                    [jnp.where(lane < head_size, x, zero), jnp.where(lane < head_size, zero, x)],
+                    axis=0,
+                )
+                inside_ref[span, two] = jnp.dot(
+                    jnp.concatenate(mats, axis=1), stacked, preferred_element_type=jnp.float32
+                )
+
     @pl.loop(0, blocks)
     def _(step):
+        inside_chunk(step)
+
         @pl.when(step == (3 * blocks) // 8)
         def _():
             join_pair()
@@ -662,7 +638,10 @@
                 to_pair(d, k).wait_send()
 
 
-def middle(query, rimmed, sink_logit, pack_forward, pack_backward, head_size, key_heads):
+def middle(
+    query, rimmed, sink_logit, pack_forward, pack_backward, act, table, turned, head_size, key_heads,
+    inner, maps,
+):
     rows, width = query.shape
     heads = width // head_size
     count = lax.axis_size("sp")
@@ -672,12 +651,13 @@
     vmem = pl.BlockSpec(memory_space=pltpu.VMEM)
     dma = pltpu.SemaphoreType.DMA
     return pl.pallas_call(
-        functools.partial(middle_kernel, head_size, key_heads, count),
-        in_specs=[pl.BlockSpec(memory_space=pltpu.SMEM), vmem, vmem, vmem, vmem],
-        out_specs=[vmem, vmem],
+        functools.partial(middle_kernel, head_size, key_heads, count, inner, maps),
+        in_specs=[pl.BlockSpec(memory_space=pltpu.SMEM)] + [vmem] * 7,
+        out_specs=[vmem] * 3,
         out_shape=[
             jax.ShapeDtypeStruct((rows, width), jnp.bfloat16),
             jax.ShapeDtypeStruct((2, 2, STATE_SIZE, half), jnp.float32),
+            jax.ShapeDtypeStruct((rows, inner), jnp.float32),
         ],
         scratch_shapes=[
             pltpu.VMEM((heads, span, WINDOW), jnp.float32),
@@ -696,136 +676,14 @@
             dma((2,)), dma((2,)), dma((2, hops)), dma((2, hops)), dma((2,)), dma((2,)),
         ],
         compiler_params=pltpu.CompilerParams(
-            collective_id=5, has_side_effects=True, vmem_limit_bytes=20 * MIB
+            collective_id=5, has_side_effects=True, vmem_limit_bytes=MIDDLE_MIB * MIB
         ),
         cost_estimate=pl.CostEstimate(
             flops=4 * rows * span * width, bytes_accessed=4 * rows * width,
             transcendentals=rows * span * heads,
         ),
         name="middle",
-    )(sink_logit, query, rimmed, pack_forward, pack_backward)
-
-
-def combine_kernel(
-    count, attn_ref, ssm_ref, attn_w_ref, ssm_w_ref, out_ref, acc, own, mate_out, mate_in,
-    far_out, far_in, mate_send, mate_recv, far_send, far_recv,
-):
-    me = lax.axis_index("tp")
-    core = lax.rem(me, 2)
-    chip = lax.div(me, 2)
-    chips = count // 2
-    mate = me + 1 - 2 * core
-    rows = out_ref.shape[0]
-    pieces, width = own.shape[1], own.shape[3]
-
-    def chip_of(slot):
-        return lax.rem(chip + 1 + slot, chips)
-
-    def to_mate(slot, j):
-        return pltpu.make_async_remote_copy(
-            src_ref=mate_out.at[slot, j], dst_ref=mate_in.at[slot, j],
-            send_sem=mate_send.at[slot, j], recv_sem=mate_recv.at[slot, j],
-            device_id={"tp": mate}, device_id_type=MESH,
-        )
-
-    def to_far(slot, j):
-        return pltpu.make_async_remote_copy(
-            src_ref=far_out.at[slot, j], dst_ref=far_in.at[slot, j],
-            send_sem=far_send.at[slot, j], recv_sem=far_recv.at[slot, j],
-            device_id={"tp": 2 * chip_of(slot) + core}, device_id_type=MESH,
-        )
-
-    barrier = pltpu.get_barrier_semaphore()
-    pl.semaphore_signal(barrier, inc=1, device_id={"tp": mate}, device_id_type=MESH)
-    for slot in range(chips - 1):
-        pl.semaphore_signal(
-            barrier, inc=1, device_id={"tp": 2 * chip_of(slot) + core}, device_id_type=MESH
-        )
-    pl.semaphore_wait(barrier, chips)
-
-    def compute(slot, j):
-        cols = pl.ds(pl.multiple_of(j * width, width), width)
-        first = pl.multiple_of(chip_of(slot) * 2 * rows, rows)
-        span = pl.ds(first, 2 * rows)
-        acc[...] = jnp.dot(
-            attn_ref[span, :], attn_w_ref[:, cols], preferred_element_type=jnp.float32
-        ) + jnp.dot(ssm_ref[span, :], ssm_w_ref[:, cols], preferred_element_type=jnp.float32)
-        other = acc[pl.ds(pl.multiple_of((1 - core) * rows, rows), rows), :]
-        mate_out[slot, j] = other.astype(jnp.bfloat16)
-        to_mate(slot, j).start()
-        mine = acc[pl.ds(pl.multiple_of(core * rows, rows), rows), :]
-        own[slot, j] = mine.astype(jnp.bfloat16)
-
-    def forward(slot, j):
-        to_mate(slot, j).wait_recv()
-        far_out[slot, j] = (
-            own[slot, j].astype(jnp.float32) + mate_in[slot, j].astype(jnp.float32)
-        ).astype(jnp.bfloat16)
-        to_far(slot, j).start()
-
-    last = chips - 1
-    for slot in range(chips):
-        compute(slot, 0)
-        if slot > 0:
-            forward(slot - 1, pieces - 1)
-
-        @pl.loop(1, pieces)
-        def _(j, slot=slot):
-            compute(slot, j)
-            if slot < last:
-                forward(slot, j - 1)
-
-    @pl.loop(0, pieces)
-    def _(j):
-        to_mate(last, j).wait_recv()
-        total = own[last, j].astype(jnp.float32) + mate_in[last, j].astype(jnp.float32)
-        for slot in range(last):
-            to_far(slot, j).wait_recv()
-            total = total + far_in[slot, j].astype(jnp.float32)
-        out_ref[:, pl.ds(pl.multiple_of(j * width, width), width)] = total.astype(jnp.bfloat16)
-
-    @pl.loop(0, pieces)
-    def _(j):
-        for slot in range(chips):
-            to_mate(slot, j).wait_send()
-        for slot in range(last):
-            to_far(slot, j).wait_send()
-
-
-def combine(attn_out, ssm_out, attn_weight, ssm_weight):
-    count = lax.axis_size("tp")
-    chips = count // 2
-    total, width = attn_out.shape[0], attn_weight.shape[1]
-    rows = total // count
-    pieces = width // PIECE
-    far = max(chips - 1, 1)
-    vmem = pl.BlockSpec(memory_space=pltpu.VMEM)
-    depth = attn_out.shape[1] + ssm_out.shape[1]
-    return pl.pallas_call(
-        functools.partial(combine_kernel, count),
-        in_specs=[vmem] * 4,
-        out_specs=vmem,
-        out_shape=jax.ShapeDtypeStruct((rows, width), jnp.bfloat16),
-        scratch_shapes=[
-            pltpu.VMEM((2 * rows, PIECE), jnp.float32),
-            pltpu.VMEM((chips, pieces, rows, PIECE), jnp.bfloat16),
-            pltpu.VMEM((chips, pieces, rows, PIECE), jnp.bfloat16),
-            pltpu.VMEM((chips, pieces, rows, PIECE), jnp.bfloat16),
-            pltpu.VMEM((far, pieces, rows, PIECE), jnp.bfloat16),
-            pltpu.VMEM((far, pieces, rows, PIECE), jnp.bfloat16),
-            pltpu.SemaphoreType.DMA((chips, pieces)),
-            pltpu.SemaphoreType.DMA((chips, pieces)),
-            pltpu.SemaphoreType.DMA((far, pieces)),
-            pltpu.SemaphoreType.DMA((far, pieces)),
-        ],
-        compiler_params=pltpu.CompilerParams(
-            collective_id=3, has_side_effects=True, vmem_limit_bytes=24 * MIB
-        ),
-        cost_estimate=pl.CostEstimate(
-            flops=2 * total * depth * width, bytes_accessed=2 * depth * width, transcendentals=0
-        ),
-        name="combine",
-    )(attn_out, ssm_out, attn_weight, ssm_weight)
+    )(sink_logit, query, rimmed, pack_forward, pack_backward, act, table, turned)
 
 
 def convolve(rows, keyed, taps, table, tap_count, inner, maps, heads):
@@ -833,17 +691,20 @@
     chunks = total // CHUNK
     count = lax.axis_size("sp")
     vmem = pl.BlockSpec(memory_space=pltpu.VMEM)
-    fresh = jax.ShapeDtypeStruct((chunks, STATE_SIZE, inner), jnp.float32)
+    local_shape = jax.ShapeDtypeStruct((2, chunks, STATE_SIZE, inner), jnp.bfloat16)
+    reach_shape = jax.ShapeDtypeStruct((2, chunks, 8, inner), jnp.float32)
     pack = jax.ShapeDtypeStruct((2, STATE_SIZE + PACK_ROWS, inner // 2), jnp.bfloat16)
     return pl.pallas_call(
         functools.partial(convolve_kernel, tap_count, inner, maps, heads, count),
         in_specs=[vmem] * 4,
         out_specs=[vmem] * 6,
         out_shape=[
-            jax.ShapeDtypeStruct((total, width), jnp.bfloat16), fresh, fresh, pack, pack,
+            jax.ShapeDtypeStruct((total, width), jnp.bfloat16), local_shape, reach_shape, pack, pack,
             jax.ShapeDtypeStruct((total + 2 * WINDOW, keyed.shape[1]), jnp.bfloat16),
         ],
         scratch_shapes=[
+            pltpu.VMEM((chunks, STATE_SIZE, inner), jnp.float32),
+            pltpu.VMEM((chunks, STATE_SIZE, inner), jnp.float32),
             pltpu.VMEM((CHUNK + 2 * HALO, width), jnp.float32),
             pltpu.VMEM((HALO, width), jnp.bfloat16),
             pltpu.VMEM((HALO, width), jnp.bfloat16),
@@ -855,7 +716,7 @@
             pltpu.SemaphoreType.DMA((4,)),
         ],
         compiler_params=pltpu.CompilerParams(
-            collective_id=4, has_side_effects=True, vmem_limit_bytes=24 * MIB
+            collective_id=4, has_side_effects=True, vmem_limit_bytes=CONVOLVE_MIB * MIB
         ),
         cost_estimate=pl.CostEstimate(
             flops=8 * total * inner * STATE_SIZE, bytes_accessed=8 * total * inner,
@@ -865,36 +726,208 @@
     )(rows, keyed, taps, table)
 
 
-def chunk_outputs(head_size, inner, maps, heads, act, table, turned, fresh, incoming, gate, gain):
-    rows, total = act.shape
-    chunks = rows // CHUNK
+def finish_kernel(
+    head_size, inner, maps, heads, count, act_ref, table_ref, local_ref, reach_ref, enter_ref,
+    inside_ref, gate_ref, gain_ref, attn_ref, attn_hbm, ssm_hbm, out_ref, attn_w, ssm_w, ssm,
+    carries, own, mate_out, mate_in, far_out, far_in, home, home_out, home_in, load_sems, mate_send,
+    mate_recv, far_send, far_recv, home_send, home_recv,
+):
+    loads = [
+        pltpu.make_async_copy(attn_hbm, attn_w, load_sems.at[0]),
+        pltpu.make_async_copy(ssm_hbm, ssm_w, load_sems.at[1]),
+    ]
+    for load in loads:
+        load.start()
+    me = lax.axis_index("tp")
+    core = lax.rem(me, 2)
+    chip = lax.div(me, 2)
+    chips = count // 2
+    mate = me + 1 - 2 * core
+    size = CHUNK
+    wide = ssm_w.shape[1]
+    side = wide // 2
+    each = home.shape[0]
+    per_chip = 2 * each
+    far_steps = (chips - 1) * per_chip
+    groups = maps // STATE_SIZE
+    width = inner // groups
+    half = inner // 2
+
+    def chip_of(slot):
+        return lax.rem(chip + 1 + slot, chips)
+
+    def remote(source, target, sends, receives, device):
+        return pltpu.make_async_remote_copy(
+            src_ref=source, dst_ref=target, send_sem=sends, recv_sem=receives,
+            device_id={"tp": device}, device_id_type=MESH,
+        )
+
+    def to_mate(t):
+        return remote(mate_out.at[t], mate_in.at[t], mate_send.at[t], mate_recv.at[t], mate)
+
+    def to_far(t):
+        slot, i = lax.div(t, per_chip), lax.rem(t, per_chip)
+        owner, at = lax.div(i, each), lax.rem(i, each)
+        return remote(
+            far_out.at[t], far_in.at[slot, core, at], far_send.at[t], far_recv.at[slot, core, at],
+            2 * chip_of(slot) + owner,
+        )
+
+    def from_far(slot, part, at):
+        return remote(
+            far_out.at[0], far_in.at[slot, part, at], far_send.at[0], far_recv.at[slot, part, at],
+            mate,
+        )
+
+    def to_home(i):
+        return remote(home_out.at[i], home_in.at[i], home_send.at[i], home_recv.at[i], mate)
+
+    barrier = pltpu.get_barrier_semaphore()
+    pl.semaphore_signal(barrier, inc=1, device_id={"tp": mate}, device_id_type=MESH)
+    for slot in range(chips - 1):
+        for other in range(2):
+            pl.semaphore_signal(
+                barrier, inc=1, device_id={"tp": 2 * chip_of(slot) + other}, device_id_type=MESH
+            )
+    pl.semaphore_wait(barrier, 1 + 2 * (chips - 1))
+
+    def rows_of(c):
+        span = pl.ds(pl.multiple_of(c * size, size), size)
+        for d in range(2):
+            for part in range(2):
+                cols = slice(part * half, (part + 1) * half)
+                carries[d, :, cols] = (
+                    local_ref[d, c, :, cols].astype(jnp.float32)
+                    + reach_ref[d, c, 0:1, cols] * enter_ref[d, part]
+                ).astype(jnp.bfloat16)
+        table = table_ref[span, :]
+        expf = spread(jnp.exp(table[:, :heads]), inner)
+        expb = spread(jnp.exp(table[:, heads : 2 * heads]), inner)
+        for g in range(groups):
+            cols = slice(g * width, (g + 1) * width)
+            first = inner + maps + g * STATE_SIZE
+            leave = act_ref[span, first : first + STATE_SIZE]
+            y = (
+                inside_ref[span, cols]
+                + jnp.dot(leave, carries[0, :, cols], preferred_element_type=jnp.float32)
+                * expf[:, cols]
+                + jnp.dot(leave, carries[1, :, cols], preferred_element_type=jnp.float32)
+                * expb[:, cols]
+            )
+            gate = gate_ref[span, cols].astype(jnp.float32)
+            mixed = y * (gate * (1.0 / (1.0 + jnp.exp(-gate))))
+            scale = lax.rsqrt(jnp.mean(mixed * mixed, axis=1, keepdims=True) + NORM_EPS)
+            ssm[:, cols] = (mixed * scale * gain_ref[:, cols]).astype(jnp.bfloat16)
+        return span
+
+    def product(span, cols):
+        return (
+            jnp.dot(attn_ref[span, :], attn_w[:, cols], preferred_element_type=jnp.float32)
+            + jnp.dot(ssm[...], ssm_w[:, cols], preferred_element_type=jnp.float32)
+        ).astype(jnp.bfloat16)
+
+    def forward(t):
+        to_mate(t).wait_recv()
+        far_out[t] = (own[t].astype(jnp.float32) + mate_in[t].astype(jnp.float32)).astype(
+            jnp.bfloat16
+        )
+        to_far(t).start()
+
+    for load in loads:
+        load.wait()
+
+    @pl.loop(0, far_steps)
+    def _(t):
+        slot, i = lax.div(t, per_chip), lax.rem(t, per_chip)
+        span = rows_of(chip_of(slot) * per_chip + i)
+        mate_out[t] = product(span, pl.ds(pl.multiple_of((1 - core) * side, side), side))
+        to_mate(t).start()
+        own[t] = product(span, pl.ds(pl.multiple_of(core * side, side), side))
+
+        @pl.when(t > 0)
+        def _():
+            forward(t - 1)
+
+    @pl.loop(0, per_chip)
+    def _(u):
+        i = lax.rem(u, each)
+        owner = jnp.where(u < each, 1 - core, core)
+        span = rows_of((2 * chip + owner) * each + i)
+        for part in range(2):
+            cols = slice(part * side, (part + 1) * side)
+            home[i, :, cols] = product(span, cols)
+
+        if far_steps > 0:
+            @pl.when(u == 0)
+            def _():
+                forward(far_steps - 1)
+
+        @pl.when(u < each)
+        def _():
+            home_out[i] = home[i]
+            to_home(i).start()
+
+    for i in range(each):
+        to_home(i).wait_recv()
+        for part in range(2):
+            cols = slice(part * side, (part + 1) * side)
+            total = home[i, :, cols].astype(jnp.float32) + home_in[i, :, cols].astype(jnp.float32)
+            for slot in range(chips - 1):
+                from_far(slot, part, i).wait_recv()
+                total = total + far_in[slot, part, i].astype(jnp.float32)
+            out_ref[i * size : (i + 1) * size, cols] = total.astype(jnp.bfloat16)
+
+    @pl.loop(0, far_steps)
+    def _(t):
+        to_mate(t).wait_send()
+        to_far(t).wait_send()
+
+    for i in range(each):
+        to_home(i).wait_send()
+
+
+def finish(
+    head_size, inner, maps, heads, act, table, local_states, reach, incoming, inside, gate, gain,
+    attn_out, attn_weight, ssm_weight,
+):
+    count = lax.axis_size("tp")
+    chips = count // 2
+    total, width = attn_out.shape[0], attn_weight.shape[1]
+    each = total // count // CHUNK
+    far = max(chips - 1, 1)
+    steps = far * 2 * each
+    depth = attn_weight.shape[0] + ssm_weight.shape[0]
+    vmem = pl.BlockSpec(memory_space=pltpu.VMEM)
+    dma = pltpu.SemaphoreType.DMA
+
+    def room(*dims):
+        return pltpu.VMEM(dims, jnp.bfloat16)
+
     return pl.pallas_call(
-        functools.partial(outputs_kernel, head_size, inner, maps),
-        grid=(chunks,),
-        in_specs=[
-            pl.BlockSpec((CHUNK, total), lambda i: (i, 0)),
-            pl.BlockSpec((CHUNK, 128), lambda i: (i, 0)),
-            pl.BlockSpec((128, CHUNK), lambda i: (0, i)),
-            pl.BlockSpec((rows, 128), lambda i: (0, 0)),
-            pl.BlockSpec((1, STATE_SIZE, inner), lambda i: (i, 0, 0)),
-            pl.BlockSpec((chunks, STATE_SIZE, inner), lambda i: (0, 0, 0)),
-            pl.BlockSpec(incoming.shape, lambda i: (0, 0, 0, 0)),
-            pl.BlockSpec((CHUNK, inner), lambda i: (i, 0)),
-            pl.BlockSpec((1, inner), lambda i: (0, 0)),
+        functools.partial(finish_kernel, head_size, inner, maps, heads, count),
+        in_specs=[vmem] * 9 + [pl.BlockSpec(memory_space=pl.ANY)] * 2,
+        out_specs=vmem,
+        out_shape=jax.ShapeDtypeStruct((total // count, width), jnp.bfloat16),
+        scratch_shapes=[
+            room(*attn_weight.shape), room(*ssm_weight.shape), room(CHUNK, inner),
+            room(2, STATE_SIZE, inner), room(steps, CHUNK, width // 2),
+            room(steps, CHUNK, width // 2), room(steps, CHUNK, width // 2),
+            room(steps, CHUNK, width // 2), room(far, 2, each, CHUNK, width // 2),
+            room(each, CHUNK, width), room(each, CHUNK, width), room(each, CHUNK, width),
+            dma((2,)), dma((steps,)), dma((steps,)), dma((steps,)), dma((far, 2, each)),
+            dma((each,)), dma((each,)),
         ],
-        out_specs=pl.BlockSpec((CHUNK, inner), lambda i: (i, 0)),
-        out_shape=jax.ShapeDtypeStruct((rows, inner), jnp.bfloat16),
-        scratch_shapes=[
-            pltpu.VMEM((STATE_SIZE, inner), jnp.float32),
-            pltpu.VMEM((chunks, STATE_SIZE, inner), jnp.float32),
-            pltpu.VMEM((CHUNK, inner), jnp.float32),
-        ],
+        compiler_params=pltpu.CompilerParams(
+            collective_id=3, has_side_effects=True, vmem_limit_bytes=FINISH_MIB * MIB
+        ),
         cost_estimate=pl.CostEstimate(
-            flops=8 * rows * inner * STATE_SIZE, bytes_accessed=16 * rows * inner,
-            transcendentals=rows * CHUNK * heads,
+            flops=2 * total * depth * width, bytes_accessed=2 * depth * width, transcendentals=0
         ),
-        name="chunk_outputs",
-    )(act, table, turned, table, fresh[0], fresh[1], incoming, gate, gain)
+        name="finish",
+    )(
+        act, table, local_states, reach, incoming, inside, gate, gain, attn_out, attn_weight,
+        ssm_weight,
+    )
 
 
 def local(
@@ -931,17 +964,17 @@
     conv_table = jnp.concatenate([conv_inner, conv_pair.reshape(tap_count, -1)], axis=1).astype(
         jnp.float32
     )
-    act, fresh_forward, fresh_backward, pack_forward, pack_backward, rimmed = convolve(
+    act, local_states, reach, pack_forward, pack_backward, rimmed = convolve(
         rows, keyed, conv_table, table, tap_count, inner, maps, heads
     )
-    attn_out, incoming = middle(
-        query, rimmed, sink_logit, pack_forward, pack_backward, head_size, key_heads
+    attn_out, incoming, inside = middle(
+        query, rimmed, sink_logit, pack_forward, pack_backward, act, table, turned, head_size,
+        key_heads, inner, maps,
     )
-    ssm_out = chunk_outputs(
-        head_size, inner, maps, heads, act, table, turned, (fresh_forward, fresh_backward), incoming,
-        gate_rows, inner_gain.astype(jnp.float32)[None, :],
+    return finish(
+        head_size, inner, maps, heads, act, table, local_states, reach, incoming, inside, gate_rows,
+        inner_gain.astype(jnp.float32)[None, :], attn_out, attn_out_weight, ssm_out_weight,
     )
-    return combine(attn_out, ssm_out, attn_out_weight, ssm_out_weight)
 
 
 def solution(mesh):

time: 144 us -> 118 us (0.82)
  Pallas kernels: 126 us -> 109 us
  local copies, waits for them, and re-layouts: 16.5 us -> 7.73 us
    pallas_call x2 -> x1, Pallas kernels: 45.3 us -> 28.6 us  [finish(): pl.pallas_call(functools.partial(finish_kernel, head_size, inner, maps, h...]
    unnamed x36 -> x24, local copies, waits for them, and re-layouts: 13.5 us -> 4.71 us
where the time goes in v4:
time: 118 us
  Pallas kernels  109 us (92%)
  local copies, waits for them, and re-layouts  7.73 us (7%)
    pallas_call x1, Pallas kernels, project_all(): pl.pallas_call(functools.partial(project_kernel, head_size, heads, key_wi...  32.7 us
    pallas_call x1, Pallas kernels, middle(): pl.pallas_call(functools.partial(middle_kernel, head_size, key_heads, cou...  28.9 us
    pallas_call x1, Pallas kernels, finish(): pl.pallas_call(functools.partial(finish_kernel, head_size, inner, maps, h...  28.6 us
    pallas_call x1, Pallas kernels, convolve(): pl.pallas_call(functools.partial(convolve_kernel, tap_count, inner, maps,...  18.9 us
    unnamed x24, local copies, waits for them, and re-layouts  4.71 us

profile of v4, /device:TPU:0, one launch (start us, length us, event | category | flops | bytes accessed | tf_op | source)
XLA Modules:
  0.0 117.7 jit_solution(12842472731858285426)
XLA Ops:
  0.0 0.7 broadcast_multiply_fusion
  0.7 0.1 mul.12
  0.7 0.7 tile.7
  1.4 0.1 tile.8
  1.5 0.8 reshape.21
  2.2 1.4 %concatenate.6 = f32[3072]{0:T(1024)S(1)} concatenate(bf16[2048]{0:T(1024)(128)(2,1)} %param.23, f32[128]{0:T(128)S(1)} %mul.12, f32[128]{0:T(128)S(1)} %tile.8, f32[128]{0:T(128)} %constant.8.clone, f32[128]{0:T(128)} %constant.9.clone, f32[32]{0:T(128)S(1)} %reshape.21, f32[480]{0:T(512)S(1)} %broadcast_in_dim.8), dimensions={0} | concatenate | bytes 20480 | tf_op jit(solution)/shard_map/concatenate | solution.py:227
  3.7 0.0 copy-start.6
  3.7 0.9 copy-done.6
  4.6 0.0 copy-start.7
  4.6 0.9 copy-done.7
  5.5 0.0 copy-start.9
  5.5 0.0 copy-start.8
  5.5 32.7 %project.1 = (bf16[1024,512]{1,0:T(8,128)(2,1)}, bf16[1024,256]{1,0:T(8,128)(2,1)S(1)}, bf16[1024,1536]{1,0:T(8,128)(2,1)}, bf16[1024,1024]{1,0:T(8,128)(2,1)}, ...) custom-call(bf16[1024,2048]{1,0:T(8,128)(2,1)} %tokens_ref.1, bf16[2048,1024]{1,0:T(8,128)(2,1)} %inner_hbm.1, ...), custom_call_target="tpu_custom_call" | custom-call | flops 13958643712 | bytes 17825792 | tf_op jit(solution)/shard_map/project/pallas_call | solution.py:251
  38.2 0.0 copy-start.5
  38.3 0.0 copy-done.9
  38.3 0.0 copy-done.8
  38.3 0.0 copy-start.1
  38.3 1.9 %copy-done.1 = bf16[1024,1536]{1,0:T(8,128)(2,1)S(1)} copy-done((bf16[1024,1536]{1,0:T(8,128)(2,1)S(1)}, bf16[1024,1536]{1,0:T(8,128)(2,1)}, u32[]{:S(2)}) %copy-start.1) | copy-done | bytes 3145752
  40.2 0.0 copy-start.4
  40.2 0.0 copy-start.3
  40.2 18.9 %convolve.1 = (bf16[1024,1536]{1,0:T(8,128)(2,1)S(1)}, bf16[2,8,128,1024]{3,2,1,0:T(8,128)(2,1)S(1)}, f32[2,8,8,1024]{3,2,1,0:T(8,128)S(1)}, bf16[2,144,512]{2,1...) custom-call(bf16[1024,1536]{1,0:T(8,128)(2,1)S(1)} %copy-done.1, ...), custom_call_target="tpu_custom_call" | custom-call | flops 1073741824 | bytes 8388608 | tf_op jit(solution)/shard_map/convolve/pallas_call | solution.py:697
  59.1 0.0 copy-start.10
  59.1 0.0 copy-start
  59.1 0.0 copy-start.2
  59.2 0.0 copy-done.5
  59.2 0.0 copy-done.4
  59.2 28.9 %middle.1 = (bf16[1024,512]{1,0:T(8,128)(2,1)S(1)}, f32[2,2,128,512]{3,2,1,0:T(8,128)S(1)}, f32[1024,1024]{1,0:T(8,128)S(1)}) custom-call(f32[8]{0:T(128)S(1)} %copy-done.5, bf16[1024,512]{1,0:T(8,128)(2,1)S(1)} %copy-done.4, bf16[1280,256]{1,0:T(8,128)(2,1)S(1)} %get-tuple-element.27.rim_ref, bf16[2,144,512]{2,1,0:T(8,128)(2,1)S(1)} %get-tuple-element.28.packf_ref, ...), custom_call_target="tpu_custom_call" | custom-call | flops 805306368 | bytes 2097152 | tf_op jit(solution)/shard_map/middle/pallas_call | solution.py:653
  88.1 0.0 copy-done.10
  88.1 0.0 copy-done.3
  88.1 0.0 copy-done
  88.1 0.0 copy-done.2
  88.2 28.6 %finish.1 = bf16[256,2048]{1,0:T(8,128)(2,1)S(1)} custom-call(bf16[1024,1536]{1,0:T(8,128)(2,1)S(1)} %get-tuple-element.23.act_ref, f32[1024,128]{1,0:T(8,128)S(1)} %get-tuple-element.22.table_ref, bf16[2,8,128,1024]{3,2,1,0:T(8,128)(2,1)S(1)} %get-tuple-element.24.local_ref, f32[2,8,8,1024]{3,2,1,0:T(8,128)S(1)} %get-tuple-element.25.reach_ref, ...), custom_call_target="tpu_custom_call" | custom-call | flops 6442450944 | bytes 6291456 | tf_op jit(solution)/shard_map/finish/pallas_call | solution.py:906
  116.7 1.0 copy.25
  (5 shorter events, 0.0 us)
Async XLA Ops:
  3.7 0.9 copy-start.6
  4.6 0.9 copy-start.7
  5.5 32.8 %copy-start.9 = (bf16[5,2,256]{2,1,0:T(2,128)(2,1)S(1)}, bf16[5,2,256]{2,1,0:T(2,128)(2,1)}, u32[]{:S(2)}) copy-start(bf16[5,2,256]{2,1,0:T(2,128)(2,1)} %param.36) | copy-start | bytes 15364
  5.5 32.8 %copy-start.8 = (bf16[5,1024]{1,0:T(8,128)(2,1)S(1)}, bf16[5,1024]{1,0:T(8,128)(2,1)}, u32[]{:S(2)}) copy-start(bf16[5,1024]{1,0:T(8,128)(2,1)} %param.35) | copy-start | bytes 30724
  38.2 20.9 %copy-start.5 = (f32[8]{0:T(128)S(1)}, f32[8]{0:T(128)}, u32[]{:S(2)}) copy-start(f32[8]{0:T(128)} %sink_ref.1) | copy-start | bytes 100
  38.3 1.9 %copy-start.1 = (bf16[1024,1536]{1,0:T(8,128)(2,1)S(1)}, bf16[1024,1536]{1,0:T(8,128)(2,1)}, u32[]{:S(2)}) copy-start(bf16[1024,1536]{1,0:T(8,128)(2,1)} %get-tuple-element.20.rows_ref) | copy-start | bytes 9437188
  40.2 19.0 %copy-start.4 = (bf16[1024,512]{1,0:T(8,128)(2,1)S(1)}, bf16[1024,512]{1,0:T(8,128)(2,1)}, u32[]{:S(2)}) copy-start(bf16[1024,512]{1,0:T(8,128)(2,1)} %get-tuple-element.26.query_ref) | copy-start | bytes 3145732
  40.2 47.9 %copy-start.3 = (bf16[1024,1024]{1,0:T(8,128)(2,1)S(1)}, bf16[1024,1024]{1,0:T(8,128)(2,1)}, u32[]{:S(2)}) copy-start(bf16[1024,1024]{1,0:T(8,128)(2,1)} %get-tuple-element.33.gate_ref) | copy-start | bytes 6291460
  59.1 29.0 %copy-start.10 = (bf16[1024]{0:T(1024)(128)(2,1)S(1)}, bf16[1024]{0:T(1024)(128)(2,1)}, u32[]{:S(2)}) copy-start(bf16[1024]{0:T(1024)(128)(2,1)} %param.39) | copy-start | bytes 6148
  59.1 29.0 %copy-start = (bf16[1024,2048]{1,0:T(8,128)(2,1)S(1)}, bf16[1024,2048]{1,0:T(8,128)(2,1)}, u32[]{:S(2)}) copy-start(bf16[1024,2048]{1,0:T(8,128)(2,1)} %ssm_hbm.1) | copy-start | bytes 12582916
  59.1 29.0 %copy-start.2 = (bf16[512,2048]{1,0:T(8,128)(2,1)S(1)}, bf16[512,2048]{1,0:T(8,128)(2,1)}, u32[]{:S(2)}) copy-start(bf16[512,2048]{1,0:T(8,128)(2,1)} %attn_hbm.1) | copy-start | bytes 6291460

commit v5 on v4

--- a/solution.py
+++ b/solution.py
@@ -17,6 +17,7 @@
 ROPE_BASE = 500000.0
 NEG_FILL = -1e30
 TILE = 512
+ROWS = 256
 MIB = 1 << 20
 PROJECT_MIB = 52
 CONVOLVE_MIB = 32
@@ -49,7 +50,8 @@
 
 def project_kernel(
     head_size, heads, key_width, tokens_ref, inner_hbm, in_hbm, out_hbm, key_hbm, value_hbm,
-    query_hbm, gate_hbm, step_hbm, jump_hbm, small_ref, query_ref, keyed_ref, rows_ref, gate_ref,
+    query_hbm, gate_hbm, step_hbm, jump_hbm, small_ref,
+    waves_ref, query_gain_ref, key_gain_ref, rate_ref, query_ref, keyed_ref, rows_ref, gate_ref,
     table_ref, turned_ref, step_ref, jump_ref, tokens, normed, inner_w, in_w, out_w, keyed_w, query_w, gate_w, raw,
     cosine, sine, token_sems, weight_sems,
 ):
@@ -80,7 +82,10 @@
     for move in moves + loads[7:] + loads[:7]:
         move.start()
     lanes = depth // 128
-    frequency, sign = small_ref[lanes + 2 : lanes + 3], small_ref[lanes + 3 : lanes + 4]
+    frequency, sign = waves_ref[0:1], waves_ref[1:2]
+    repeats = 128 // head_size
+    query_gain = jnp.concatenate([query_gain_ref[...] * head_size ** (-0.5)] * repeats, axis=1)
+    key_gain = jnp.concatenate([key_gain_ref[...]] * repeats, axis=1)
     order = lax.broadcasted_iota(jnp.int32, (32, 128), 0)
     first = lax.axis_index("sp") * total
     near = order.astype(jnp.float32) * frequency
@@ -116,11 +121,14 @@
 
         def tile(j):
             at = j * width if count == 1 else pl.multiple_of(j * width, width)
-            target[:, pl.ds(column + at, width)] = jnp.dot(
-                normed[...], weight[:, pl.ds(at, width)], preferred_element_type=jnp.float32
-            ).astype(jnp.bfloat16)
-            if beside is not None:
-                beside(j, total // count)
+            share = total // count
+            for m in range(0, total, ROWS):
+                target[m : m + ROWS, pl.ds(column + at, width)] = jnp.dot(
+                    normed[m : m + ROWS, :], weight[:, pl.ds(at, width)],
+                    preferred_element_type=jnp.float32,
+                ).astype(jnp.bfloat16)
+                if beside is not None:
+                    beside(j * share + m // count, ROWS // count)
 
         if count == 1:
             tile(0)
@@ -133,13 +141,16 @@
     raw[:, : 2 * heads] = lax.dot_general(
         normed[...], step_ref[...], (((1,), (1,)), ((), ())), preferred_element_type=jnp.float32
     ).astype(jnp.bfloat16).astype(jnp.float32)
-    rates = jnp.transpose(jnp.broadcast_to(small_ref[lanes + 4 : lanes + 5], (128, 128)))
+    rates = jnp.concatenate(
+        [rate_ref[0:1], rate_ref[1:2], jnp.zeros((1, 128 - 2 * heads), jnp.float32)], axis=1
+    )
+    rates = jnp.transpose(jnp.broadcast_to(rates, (128, 128)))
     rates = rates[: 2 * heads, 0:1]
     upper, lower = triangle(CHUNK, False), triangle(CHUNK, True)
 
-    def steps(j, length):
+    def steps(first_row, length):
         for c in range(length // CHUNK):
-            at = pl.multiple_of(j * length + c * CHUNK, CHUNK)
+            at = pl.multiple_of(first_row + c * CHUNK, CHUNK)
             span = pl.ds(at, CHUNK)
             x = jnp.transpose(raw[span, :])[: 2 * heads]
             step = jnp.maximum(x, 0.0) + jnp.log1p(jnp.exp(-jnp.abs(x)))
@@ -176,19 +187,19 @@
         )
         return (value * cos_here + swapped * sin_here).astype(jnp.bfloat16)
 
-    def heads_of(j, length):
+    def heads_of(first_row, length):
         for i in range(length // 128):
-            span = pl.ds(pl.multiple_of(j * length + i * 128, 128), 128)
+            span = pl.ds(pl.multiple_of(first_row + i * 128, 128), 128)
             cos_here, sin_here = cosine[span, :], sine[span, :]
             for at in range(0, query_ref.shape[1], 128):
                 value = query_ref[span, at : at + 128].astype(jnp.float32)
                 query_ref[span, at : at + 128] = rotate(
-                    value, small_ref[lanes : lanes + 1], cos_here, sin_here
+                    value, query_gain, cos_here, sin_here
                 )
             for at in range(0, key_width, 128):
                 packed = keyed_ref[span, at : at + 128]
                 keys = rotate(
-                    packed.astype(jnp.float32), small_ref[lanes + 1 : lanes + 2], cos_here, sin_here
+                    packed.astype(jnp.float32), key_gain, cos_here, sin_here
                 )
                 keyed_ref[span, at : at + 128] = jnp.where(lane + at < key_width, keys, packed)
 
@@ -222,15 +233,8 @@
     lane = np.arange(128)
     frequency = (ROPE_BASE ** (-2.0 * (lane % half) / head_size)).astype(np.float32)
     sign = np.where(lane % head_size < half, -1.0, 1.0).astype(np.float32)
-    repeats = 128 // head_size
-    rates = decay_rate.reshape(-1)
-    small = jnp.concatenate(
-        [
-            norm_gain.astype(jnp.float32), jnp.tile(query_gain, repeats) * head_size ** (-0.5),
-            jnp.tile(key_gain, repeats), frequency, sign, rates,
-            jnp.zeros((4 * 128 - rates.shape[0],), jnp.float32),
-        ]
-    ).reshape(-1, 128)
+    waves = jnp.asarray(np.stack([frequency, sign]))
+    small = norm_gain.astype(jnp.float32).reshape(-1, 128)
     turned_step = jnp.transpose(step_weight, (1, 2, 0)).reshape(-1, depth)
     turned_jump = jnp.transpose(decay_jump, (1, 2, 0)).reshape(-1, total)
     heads = step_weight.shape[2]
@@ -250,7 +254,7 @@
 
     return pl.pallas_call(
         functools.partial(project_kernel, head_size, heads, key_width),
-        in_specs=[whole] * 10 + [vmem],
+        in_specs=[whole] * 10 + [vmem] * 5,
         out_specs=[vmem] * 6,
         out_shape=[
             shape(total, width), shape(total, 2 * key_width), shape(total, inner + 2 * maps),
@@ -272,7 +276,10 @@
             transcendentals=total * 128,
         ),
         name="project",
-    )(tokens, *big, turned_step, turned_jump, small)
+    )(
+        tokens, *big, turned_step, turned_jump, small, waves, query_gain[None], key_gain[None],
+        decay_rate,
+    )
 
 
 def convolve_kernel(

time: 118 us -> 115 us (0.975)
  Pallas kernels: 109 us -> 106 us
    pallas_call x1, Pallas kernels: 32.7 us -> 29.4 us  [project_all(): pl.pallas_call(functools.partial(project_kernel, head_size, heads, key_wi...]
    unnamed x24 -> x32, local copies, waits for them, and re-layouts: 4.71 us -> 7.37 us
    concatenate x1 -> x0, local copies, waits for them, and re-layouts: 1.43 us -> none  [project_all(): jnp.concatenate([norm_gain.astype(jnp.float32), jnp.tile(query_gain, repe...]
where the time goes in v5:
time: 115 us; the launch traced here: 114 us
  Pallas kernels  106 us (92%)
  local copies, waits for them, and re-layouts  7.37 us (6%)
    pallas_call x1, Pallas kernels, project_all(): pl.pallas_call(functools.partial(project_kernel, head_size, heads, key_wi...  29.4 us
    pallas_call x1, Pallas kernels, middle(): pl.pallas_call(functools.partial(middle_kernel, head_size, key_heads, cou...  28.9 us
    pallas_call x1, Pallas kernels, finish(): pl.pallas_call(functools.partial(finish_kernel, head_size, inner, maps, h...  28.6 us
    pallas_call x1, Pallas kernels, convolve(): pl.pallas_call(functools.partial(convolve_kernel, tap_count, inner, maps,...  18.9 us
    unnamed x32, local copies, waits for them, and re-layouts  7.37 us

profile of v5, /device:TPU:0, one launch (start us, length us, event | category | flops | bytes accessed | tf_op | source)
XLA Modules:
  0.0 114.0 jit_solution(2229047440753961557)
XLA Ops:
  0.0 0.7 bitcast_convert_fusion.small_ref
  0.7 0.0 copy-start.6
  0.7 0.9 copy-done.6
  1.6 0.0 copy-start.7
  1.6 0.9 copy-done.7
  2.5 0.0 copy-start.8
  2.5 0.7 copy-done.8
  3.2 0.0 copy-start.9
  3.2 0.7 copy-done.9
  3.8 0.0 copy-start.10
  3.8 0.7 copy-done.10
  4.5 0.0 copy-start.11
  4.5 0.7 copy-done.11
  5.2 0.0 copy-start.13
  5.2 0.0 copy-start.12
  5.2 29.4 %project.1 = (bf16[1024,512]{1,0:T(8,128)(2,1)}, bf16[1024,256]{1,0:T(8,128)(2,1)S(1)}, bf16[1024,1536]{1,0:T(8,128)(2,1)}, bf16[1024,1024]{1,0:T(8,128)(2,1)}, ...) custom-call(bf16[1024,2048]{1,0:T(8,128)(2,1)} %tokens_ref.1, bf16[2048,1024]{1,0:T(8,128)(2,1)} %inner_hbm.1, ...), custom_call_target="tpu_custom_call" | custom-call | flops 13958643712 | bytes 17825792 | tf_op jit(solution)/shard_map/project/pallas_call | solution.py:255
  34.6 0.0 copy-start.5
  34.6 0.0 copy-done.13
  34.6 0.0 copy-done.12
  34.6 0.0 copy-start.1
  34.6 1.9 %copy-done.1 = bf16[1024,1536]{1,0:T(8,128)(2,1)S(1)} copy-done((bf16[1024,1536]{1,0:T(8,128)(2,1)S(1)}, bf16[1024,1536]{1,0:T(8,128)(2,1)}, u32[]{:S(2)}) %copy-start.1) | copy-done | bytes 3145752
  36.5 0.0 copy-start.4
  36.5 0.0 copy-start.3
  36.5 18.9 %convolve.1 = (bf16[1024,1536]{1,0:T(8,128)(2,1)S(1)}, bf16[2,8,128,1024]{3,2,1,0:T(8,128)(2,1)S(1)}, f32[2,8,8,1024]{3,2,1,0:T(8,128)S(1)}, bf16[2,144,512]{2,1...) custom-call(bf16[1024,1536]{1,0:T(8,128)(2,1)S(1)} %copy-done.1, ...), custom_call_target="tpu_custom_call" | custom-call | flops 1073741824 | bytes 8388608 | tf_op jit(solution)/shard_map/convolve/pallas_call | solution.py:704
  55.4 0.0 copy-start.14
  55.4 0.0 copy-start
  55.4 0.0 copy-start.2
  55.5 0.0 copy-done.5
  55.5 0.0 copy-done.4
  55.5 28.9 %middle.1 = (bf16[1024,512]{1,0:T(8,128)(2,1)S(1)}, f32[2,2,128,512]{3,2,1,0:T(8,128)S(1)}, f32[1024,1024]{1,0:T(8,128)S(1)}) custom-call(f32[8]{0:T(128)S(1)} %copy-done.5, bf16[1024,512]{1,0:T(8,128)(2,1)S(1)} %copy-done.4, bf16[1280,256]{1,0:T(8,128)(2,1)S(1)} %get-tuple-element.27.rim_ref, bf16[2,144,512]{2,1,0:T(8,128)(2,1)S(1)} %get-tuple-element.28.packf_ref, ...), custom_call_target="tpu_custom_call" | custom-call | flops 805306368 | bytes 2097152 | tf_op jit(solution)/shard_map/middle/pallas_call | solution.py:660
  84.4 0.0 copy-done.14
  84.4 0.0 copy-done.3
  84.4 0.0 copy-done
  84.5 0.0 copy-done.2
  84.5 28.6 %finish.1 = bf16[256,2048]{1,0:T(8,128)(2,1)S(1)} custom-call(bf16[1024,1536]{1,0:T(8,128)(2,1)S(1)} %get-tuple-element.23.act_ref, f32[1024,128]{1,0:T(8,128)S(1)} %get-tuple-element.22.table_ref, bf16[2,8,128,1024]{3,2,1,0:T(8,128)(2,1)S(1)} %get-tuple-element.24.local_ref, f32[2,8,8,1024]{3,2,1,0:T(8,128)S(1)} %get-tuple-element.25.reach_ref, ...), custom_call_target="tpu_custom_call" | custom-call | flops 6442450944 | bytes 6291456 | tf_op jit(solution)/shard_map/finish/pallas_call | solution.py:913
  113.0 1.0 copy.24
  (3 shorter events, 0.0 us)
Async XLA Ops:
  0.7 0.9 copy-start.6
  1.6 0.9 copy-start.7
  2.5 0.7 copy-start.8
  3.2 0.7 copy-start.9
  3.8 0.7 copy-start.10
  4.5 0.7 copy-start.11
  5.2 29.4 %copy-start.13 = (bf16[5,2,256]{2,1,0:T(2,128)(2,1)S(1)}, bf16[5,2,256]{2,1,0:T(2,128)(2,1)}, u32[]{:S(2)}) copy-start(bf16[5,2,256]{2,1,0:T(2,128)(2,1)} %param.35) | copy-start | bytes 15364
  5.2 29.4 %copy-start.12 = (bf16[5,1024]{1,0:T(8,128)(2,1)S(1)}, bf16[5,1024]{1,0:T(8,128)(2,1)}, u32[]{:S(2)}) copy-start(bf16[5,1024]{1,0:T(8,128)(2,1)} %param.34) | copy-start | bytes 30724
  34.6 20.9 %copy-start.5 = (f32[8]{0:T(128)S(1)}, f32[8]{0:T(128)}, u32[]{:S(2)}) copy-start(f32[8]{0:T(128)} %sink_ref.1) | copy-start | bytes 100
  34.6 1.9 %copy-start.1 = (bf16[1024,1536]{1,0:T(8,128)(2,1)S(1)}, bf16[1024,1536]{1,0:T(8,128)(2,1)}, u32[]{:S(2)}) copy-start(bf16[1024,1536]{1,0:T(8,128)(2,1)} %get-tuple-element.20.rows_ref) | copy-start | bytes 9437188
  36.5 19.0 %copy-start.4 = (bf16[1024,512]{1,0:T(8,128)(2,1)S(1)}, bf16[1024,512]{1,0:T(8,128)(2,1)}, u32[]{:S(2)}) copy-start(bf16[1024,512]{1,0:T(8,128)(2,1)} %get-tuple-element.26.query_ref) | copy-start | bytes 3145732
  36.5 47.9 %copy-start.3 = (bf16[1024,1024]{1,0:T(8,128)(2,1)S(1)}, bf16[1024,1024]{1,0:T(8,128)(2,1)}, u32[]{:S(2)}) copy-start(bf16[1024,1024]{1,0:T(8,128)(2,1)} %get-tuple-element.33.gate_ref) | copy-start | bytes 6291460
  55.4 29.0 %copy-start.14 = (bf16[1024]{0:T(1024)(128)(2,1)S(1)}, bf16[1024]{0:T(1024)(128)(2,1)}, u32[]{:S(2)}) copy-start(bf16[1024]{0:T(1024)(128)(2,1)} %param.38) | copy-start | bytes 6148
  55.4 29.0 %copy-start = (bf16[1024,2048]{1,0:T(8,128)(2,1)S(1)}, bf16[1024,2048]{1,0:T(8,128)(2,1)}, u32[]{:S(2)}) copy-start(bf16[1024,2048]{1,0:T(8,128)(2,1)} %ssm_hbm.1) | copy-start | bytes 12582916
  55.4 29.0 %copy-start.2 = (bf16[512,2048]{1,0:T(8,128)(2,1)S(1)}, bf16[512,2048]{1,0:T(8,128)(2,1)}, u32[]{:S(2)}) copy-start(bf16[512,2048]{1,0:T(8,128)(2,1)} %attn_hbm.1) | copy-start | bytes 6291460
